TPU v7x, 32 devices: a whole 2x2x4 slice. The times are simulated.
32 devices in a mesh: sp: 16 (over z, y, x), tp: 2 (over core).
Axes of the slice: x: 2, y: 2, z: 4, core: 2. Of those that a mesh axis runs over, the one named last changes fastest.
Arguments:
- residual: bfloat16 [4096, 2048], P(('sp', 'tp')), may hold values from -6 to 6
- query_rows: bfloat16 [4096, 1024], P('sp', 'tp'), may hold values from -141 to 141
- key_rows: bfloat16 [4096, 1024], P('sp', 'tp'), may hold values from -7.8 to 7.8
- value_rows: bfloat16 [4096, 1024], P('sp', 'tp'), may hold values from -6 to 6
- mix_lambda: float32 [8], P('tp'), may hold values from 0.3 to 0.8
- documents: int32 [4096], P('sp'), may hold values from 0 to 7, never falling along the last dimension, each value on 1 to 768 neighbouring positions
- out_weight: bfloat16 [1024, 2048], replicated, may hold values from -0.1875 to 0.1875
- norm_gain: float32 [2048], replicated, may hold values from 0.1 to 1.9
- gate_weight: bfloat16 [16, 2048, 2048], P('sp', None, 'tp'), may hold values from -0.125 to 0.125
- up_weight: bfloat16 [16, 2048, 2048], P('sp', None, 'tp'), may hold values from -0.125 to 0.125
- down_weight: bfloat16 [16, 2048, 2048], P('sp', 'tp'), may hold values from -0.125 to 0.125
- routes: int32 [4096, 2], P(('sp', 'tp')), may hold values from 0 to 15, all different within a row; in each aligned block of 128 rows (0 to 127, 128 to 255, ...) at most 32 rows name the same one
- route_weights: float32 [4096, 2], P(('sp', 'tp')), may hold values from 0.25 to 1
Outputs:
- layer_out: bfloat16 [4096, 2048], P(('sp', 'tp'))
Inputs may be any that keep to these rules, and one draw needn't show every extreme that they name: `documents`: document numbers never fall along the sequence; a document covers at most 768 positions, and one covers exactly that many. `routes`: each row names two different experts. Among the rows of one index of sp+tp, no expert is named by more than 32 rows, and in every draw some expert is named by exactly 32 rows of some such block.
All inputs are finite; a program needn't handle non-finite values.
Results may differ from a plain program's by a relative error of at most 0.013.
Values may be sent and summed in bfloat16 or wider, within the bound.
No kernel may reach another device: no remote copies, remote signals or barrier semaphores. Data moves between devices by JAX's collectives and lax.ppermute only.
A program may use at most 128 MiB of HBM per device.

v0:
```python
import jax
import jax.numpy as jnp
from jax import lax
from jax.sharding import PartitionSpec as P

HD = 64
REACH = 3


def shifted(value, axis, steps):
    count = lax.axis_size(axis)
    first, last = (max(0, -steps), min(count, count - steps))
    return lax.ppermute(value, axis, [(source, source + steps) for source in range(first, last)])


def neighbour(pieces, offset):
    return shifted((pieces[0], pieces[1], pieces[2]), "sp", offset)


def slot_order(route_block, experts):
    flat_routes = route_block.reshape(-1)
    table = (flat_routes[:, None] == jnp.arange(experts, dtype=jnp.int32)[None, :]).astype(
        jnp.int32
    )
    earlier = jnp.cumsum(table, axis=0) - table
    return (flat_routes, jnp.sum(earlier * table, axis=1))


def head_attention(same_document, score_scale):

    def attend(operands):
        head_query, head_keys, head_values, second_weight = operands
        scores = (
            jnp.einsum("qcd,kcd->cqk", head_query, head_keys, preferred_element_type=jnp.float32)
            * score_scale
        )
        masked = jnp.where(same_document[None], scores, -1e30)
        largest = jnp.max(masked, axis=-1, keepdims=True)
        lifted = jnp.exp(masked - largest)
        probabilities = lifted / jnp.sum(lifted, axis=-1, keepdims=True)
        weights = (probabilities[0] - second_weight * probabilities[1]).astype(jnp.bfloat16)
        head_out = jnp.dot(weights, head_values, preferred_element_type=jnp.float32)
        scaled = head_out * lax.rsqrt(jnp.mean(head_out * head_out, axis=-1, keepdims=True) + 1e-06)
        return scaled.astype(jnp.bfloat16)

    return attend


def on_device(
    residual,
    query_rows,
    key_rows,
    value_rows,
    mix_lambda,
    documents,
    out_weight,
    norm_gain,
    gate_weight,
    up_weight,
    down_weight,
    routes,
    route_weights,
):
    length = query_rows.shape[0]
    local_heads = mix_lambda.shape[0]
    value_dim = value_rows.shape[1] // local_heads
    model_width = residual.shape[1]
    own_ids = documents + 1
    key_parts, value_parts, id_parts = ([key_rows], [value_rows], [own_ids])
    for distance in range(1, REACH + 1):
        for offset in (distance, -distance):
            far_keys, far_values, far_ids = neighbour((key_rows, value_rows, own_ids), offset)
            key_parts.append(far_keys)
            value_parts.append(far_values)
            id_parts.append(far_ids)
    all_keys = jnp.concatenate(key_parts, axis=0).reshape(-1, local_heads, 2, HD)
    all_values = jnp.concatenate(value_parts, axis=0).reshape(-1, local_heads, value_dim)
    all_ids = jnp.concatenate(id_parts, axis=0)
    same_document = own_ids[:, None] == all_ids[None, :]
    queries = query_rows.reshape(length, local_heads, 2, HD)
    per_head = lax.map(
        head_attention(same_document, HD ** (-0.5)),
        (
            jnp.moveaxis(queries, 1, 0),
            jnp.moveaxis(all_keys, 1, 0),
            jnp.moveaxis(all_values, 1, 0),
            mix_lambda,
        ),
    )
    merged = jnp.moveaxis(per_head, 0, 1).reshape(length, local_heads * value_dim)
    token_heads = lax.all_to_all(merged, "tp", split_axis=0, concat_axis=1, tiled=True)
    projected = jnp.dot(token_heads, out_weight, preferred_element_type=jnp.float32)
    mixed = (residual.astype(jnp.float32) + projected).astype(jnp.bfloat16)
    mixed_wide = mixed.astype(jnp.float32)
    normed = (
        mixed_wide
        * lax.rsqrt(jnp.mean(mixed_wide * mixed_wide, axis=-1, keepdims=True) + 1e-06)
        * norm_gain
    ).astype(jnp.bfloat16)
    experts = lax.axis_size("sp")
    capacity = 2 * length // experts
    top_count = routes.shape[1]
    flat_routes, slot_rank = slot_order(routes, experts)
    target_rows = flat_routes * capacity + slot_rank
    sources_all = jnp.repeat(normed, top_count, axis=0)
    outgoing = jnp.zeros((experts * capacity, model_width), jnp.bfloat16)
    outgoing = outgoing.at[target_rows].set(sources_all).reshape(experts, capacity, model_width)
    arrived = lax.all_to_all(outgoing, "sp", split_axis=0, concat_axis=0, tiled=True)
    rows_all = lax.all_gather(arrived.reshape(-1, model_width), "tp", axis=0, tiled=True)
    gate = jnp.dot(rows_all, gate_weight[0], preferred_element_type=jnp.float32)
    upward = jnp.dot(rows_all, up_weight[0], preferred_element_type=jnp.float32)
    hidden = (jax.nn.silu(gate) * upward).astype(jnp.bfloat16)
    summed = lax.psum_scatter(
        jnp.dot(hidden, down_weight[0], preferred_element_type=jnp.float32).astype(jnp.bfloat16),
        "tp",
        scatter_dimension=0,
        tiled=True,
    )
    answer = summed.reshape(arrived.shape[0], arrived.shape[1], model_width)
    returned = lax.all_to_all(answer, "sp", split_axis=0, concat_axis=0, tiled=True)
    picked = returned.reshape(experts * capacity, model_width)[target_rows]
    picked = picked.reshape(-1, top_count, model_width).astype(jnp.float32)
    weighted = jnp.sum(picked * route_weights[:, :, None], axis=1)
    return (mixed_wide + weighted).astype(jnp.bfloat16)


def solution(mesh):
    placed = (
        P(("sp", "tp"), None),
        P("sp", "tp"),
        P("sp", "tp"),
        P("sp", "tp"),
        P("tp"),
        P("sp"),
        P(),
        P(),
        P("sp", None, "tp"),
        P("sp", None, "tp"),
        P("sp", "tp", None),
        P(("sp", "tp"), None),
        P(("sp", "tp"), None),
    )
    return jax.shard_map(
        on_device, mesh=mesh, in_specs=placed, out_specs=P(("sp", "tp"), None), check_vma=False
    )
```

profile of v0, /device:TPU:12, one launch (start us, length us, event | category | flops | bytes accessed | tf_op | source)
XLA Modules:
  0.0 333.0 jit_solution(15591114638349226413)
XLA Ops:
  14.0 4.3 %collective-permute-start.2 = (s32[256]{0:T(256)S(1)}, s32[256]{0:T(256)S(1)}, u32[]{:S(2)}, u32[]{:S(2)}) collective-permute-start(s32[256]{0:T(256)S(1)} %get-tuple-element.167), channel_id=1, source_target_pairs={{0,4},{2,6},{4,8},{6,10},{8,12},{10,14},{12,16},{14,18},{16,20},{1... | collective-permute-start | bytes 3080 | tf_op jit(solution)/shard_map/ppermute | solution.py:13
  20.3 4.0 %collective-permute-start.4 = (s32[256]{0:T(256)S(1)}, s32[256]{0:T(256)S(1)}, u32[]{:S(2)}, u32[]{:S(2)}) collective-permute-start(s32[256]{0:T(256)S(1)} %get-tuple-element.167), channel_id=1, source_target_pairs={{0,6},{2,8},{4,10},{6,12},{8,14},{10,16},{12,18},{14,20},{16,22},{... | collective-permute-start | bytes 3080 | tf_op jit(solution)/shard_map/ppermute | solution.py:13
  35.4 4.4 %collective-permute-start.13 = (bf16[256,512]{0,1:T(8,128)(2,1)S(1)}, bf16[256,512]{0,1:T(8,128)(2,1)S(1)}, u32[]{:S(2)}, u32[]{:S(2)}) collective-permute-start(bf16[256,512]{0,1:T(8,128)(2,1)S(1)} %copy.40), channel_id=1, source_target_pairs={{2,0},{4,2},{6,4},{8,6},{10,8},{12,10},{14,12},{16,14},{18,16},{20... | collective-permute-start | bytes 786440 | tf_op jit(solution)/shard_map/ppermute | solution.py:13
  39.8 5.7 %collective-permute-start.14 = (bf16[256,512]{0,1:T(8,128)(2,1)S(1)}, bf16[256,512]{0,1:T(8,128)(2,1)S(1)}, u32[]{:S(2)}, u32[]{:S(2)}) collective-permute-start(bf16[256,512]{0,1:T(8,128)(2,1)S(1)} %copy.40), channel_id=1, source_target_pairs={{0,4},{2,6},{4,8},{6,10},{8,12},{10,14},{12,16},{14,18},{16,20},{1... | collective-permute-start | bytes 786440 | tf_op jit(solution)/shard_map/ppermute | solution.py:13
  50.6 3.8 %collective-permute-start.6 = (bf16[256,512]{1,0:T(8,128)(2,1)S(1)}, bf16[256,512]{1,0:T(8,128)(2,1)S(1)}, u32[]{:S(2)}, u32[]{:S(2)}) collective-permute-start(bf16[256,512]{1,0:T(8,128)(2,1)S(1)} %copy-done.2), channel_id=1, source_target_pairs={{0,2},{2,4},{4,6},{6,8},{8,10},{10,12},{12,14},{14,16},{16,18},{18... | collective-permute-start | bytes 786440 | tf_op jit(solution)/shard_map/ppermute | solution.py:13
  55.1 6.3 %collective-permute-start.7 = (bf16[256,512]{1,0:T(8,128)(2,1)S(1)}, bf16[256,512]{1,0:T(8,128)(2,1)S(1)}, u32[]{:S(2)}, u32[]{:S(2)}) collective-permute-start(bf16[256,512]{1,0:T(8,128)(2,1)S(1)} %copy-done.2), channel_id=1, source_target_pairs={{2,0},{4,2},{6,4},{8,6},{10,8},{12,10},{14,12},{16,14},{18,16},{20... | collective-permute-start | bytes 786440 | tf_op jit(solution)/shard_map/ppermute | solution.py:13
  64.9 6.3 %collective-permute-start.9 = (bf16[256,512]{1,0:T(8,128)(2,1)S(1)}, bf16[256,512]{1,0:T(8,128)(2,1)S(1)}, u32[]{:S(2)}, u32[]{:S(2)}) collective-permute-start(bf16[256,512]{1,0:T(8,128)(2,1)S(1)} %copy-done.2), channel_id=1, source_target_pairs={{4,0},{6,2},{8,4},{10,6},{12,8},{14,10},{16,12},{18,14},{20,16},{2... | collective-permute-start | bytes 786440 | tf_op jit(solution)/shard_map/ppermute | solution.py:13
  71.2 9.8 %collective-permute-start.10 = (bf16[256,512]{1,0:T(8,128)(2,1)S(1)}, bf16[256,512]{1,0:T(8,128)(2,1)S(1)}, u32[]{:S(2)}, u32[]{:S(2)}) collective-permute-start(bf16[256,512]{1,0:T(8,128)(2,1)S(1)} %copy-done.2), channel_id=1, source_target_pairs={{0,6},{2,8},{4,10},{6,12},{8,14},{10,16},{12,18},{14,20},{16,22},{... | collective-permute-start | bytes 786440 | tf_op jit(solution)/shard_map/ppermute | solution.py:13
  81.0 13.4 %collective-permute-start.11 = (bf16[256,512]{1,0:T(8,128)(2,1)S(1)}, bf16[256,512]{1,0:T(8,128)(2,1)S(1)}, u32[]{:S(2)}, u32[]{:S(2)}) collective-permute-start(bf16[256,512]{1,0:T(8,128)(2,1)S(1)} %copy-done.2), channel_id=1, source_target_pairs={{6,0},{8,2},{10,4},{12,6},{14,8},{16,10},{18,12},{20,14},{22,16},{... | collective-permute-start | bytes 786440 | tf_op jit(solution)/shard_map/ppermute | solution.py:13
  96.5 4.6 %collective-permute-done.11 = bf16[256,512]{1,0:T(8,128)(2,1)S(1)} collective-permute-done((bf16[256,512]{1,0:T(8,128)(2,1)S(1)}, bf16[256,512]{1,0:T(8,128)(2,1)S(1)}, u32[]{:S(2)}, u32[]{:S(2)}) %collective-permute-start.11) | collective-permute-done | bytes 262176 | tf_op jit(solution)/shard_map/ppermute | solution.py:13
  107.3 40.1 %while.11 = (s32[]{:T(128)}, bf16[4,256,128]{1,2,0:T(8,128)(2,1)S(1)}, bf16[4,256,2,64]{1,3,2,0:T(8,128)(2,1)S(1)}, bf16[4,1792,2,64]{1,3,2,0:T(8,128)(2,1)}, f3...) while((s32[]{:T(128)}, ...), condition=%wide.region_4.5_spmd.clone, body=%wide.region_0.4_spmd.clone.sunk | while | flops 241436672 | bytes 16926828 | solution.py:81
  107.6 4.2 %exponential_reduce_fusion.2 = (f32[2,256]{1,0:T(2,128)S(1)}, f32[2,256,1792]{2,1,0:T(8,128)}) fusion(pred[256,1792]{1,0:T(8,128)(4,1)S(1)} %broadcast_compare_fusion.2, bf16[4,1792,2,64]{1,3,2,0:T(8,128)(2,1)} %get-tuple-element.181, s32[]{:T(128)} %get-tuple-element.169, bf16[4,256,2,64]{1,3,2,0:T(8,128)(2,1)S(1)} %get-tuple-element.180), kind=kOutput, calls=%fused_computation.7.clone.1 | convolution fusion | flops 121112320 | bytes 4656128 | tf_op jit(solution)/shard_map/while/body/eval_jaxpr/sub | solution.py:39
  117.7 4.2 %exponential_reduce_fusion.2 = (f32[2,256]{1,0:T(2,128)S(1)}, f32[2,256,1792]{2,1,0:T(8,128)}) fusion(pred[256,1792]{1,0:T(8,128)(4,1)S(1)} %broadcast_compare_fusion.2, bf16[4,1792,2,64]{1,3,2,0:T(8,128)(2,1)} %get-tuple-element.181, s32[]{:T(128)} %get-tuple-element.169, bf16[4,256,2,64]{1,3,2,0:T(8,128)(2,1)S(1)} %get-tuple-element.180), kind=kOutput, calls=%fused_computation.7.clone.1 | convolution fusion | flops 121112320 | bytes 4656128 | tf_op jit(solution)/shard_map/while/body/eval_jaxpr/sub | solution.py:39
  127.7 4.2 %exponential_reduce_fusion.2 = (f32[2,256]{1,0:T(2,128)S(1)}, f32[2,256,1792]{2,1,0:T(8,128)}) fusion(pred[256,1792]{1,0:T(8,128)(4,1)S(1)} %broadcast_compare_fusion.2, bf16[4,1792,2,64]{1,3,2,0:T(8,128)(2,1)} %get-tuple-element.181, s32[]{:T(128)} %get-tuple-element.169, bf16[4,256,2,64]{1,3,2,0:T(8,128)(2,1)S(1)} %get-tuple-element.180), kind=kOutput, calls=%fused_computation.7.clone.1 | convolution fusion | flops 121112320 | bytes 4656128 | tf_op jit(solution)/shard_map/while/body/eval_jaxpr/sub | solution.py:39
  137.7 4.2 %exponential_reduce_fusion.2 = (f32[2,256]{1,0:T(2,128)S(1)}, f32[2,256,1792]{2,1,0:T(8,128)}) fusion(pred[256,1792]{1,0:T(8,128)(4,1)S(1)} %broadcast_compare_fusion.2, bf16[4,1792,2,64]{1,3,2,0:T(8,128)(2,1)} %get-tuple-element.181, s32[]{:T(128)} %get-tuple-element.169, bf16[4,256,2,64]{1,3,2,0:T(8,128)(2,1)S(1)} %get-tuple-element.180), kind=kOutput, calls=%fused_computation.7.clone.1 | convolution fusion | flops 121112320 | bytes 4656128 | tf_op jit(solution)/shard_map/while/body/eval_jaxpr/sub | solution.py:39
  147.7 3.9 %all_to_all.29 = bf16[2,128,512]{2,1,0:T(8,128)(2,1)S(1)} all-to-all(bf16[2,128,512]{2,1,0:T(8,128)(2,1)S(1)} %copy.49), channel_id=1, replica_groups=mesh['sp'=16,'tp'=2] {'tp'}, dimensions={0} | all-to-all | bytes 524288 | tf_op jit(solution)/shard_map/all_to_all | solution.py:91
  160.4 55.6 %all_to_all.30 = bf16[16,32,2048]{2,1,0:T(8,128)(2,1)} all-to-all(bf16[16,32,2048]{2,1,0:T(8,128)(2,1)S(1)} %bitcast.106), channel_id=1, replica_groups=mesh['sp'=16,'tp'=2] {'sp'}, dimensions={0} | all-to-all | bytes 4194304 | tf_op jit(solution)/shard_map/all_to_all | solution.py:108
  216.2 12.9 %all-gather.2.cloned.1.call-done = bf16[1024,2048]{1,0:T(8,128)(2,1)} async-done(((bf16[512,2048]{1,0:T(8,128)(2,1)}), bf16[1024,2048]{1,0:T(8,128)(2,1)}) %all-gather.2.cloned.1.call-update) | async-done | bytes 4194320 | tf_op jit(solution)/shard_map/all_gather | solution.py:109
  229.1 7.6 %fusion.36 = f32[1024,1024]{1,0:T(8,128)S(1)} fusion(bf16[1024,2048]{1,0:T(8,128)(2,1)} %all-gather.2.cloned.1.call-done, bf16[1,2048,1024]{2,1,0:T(8,128)(2,1)} %param.24), kind=kOutput, calls=%fused_computation.35 | convolution fusion | flops 4294967296 | bytes 12582912 | tf_op jit(solution)/shard_map/dot_general | solution.py:111
  236.8 5.4 %multiply_convert_fusion.1 = bf16[1024,1024]{1,0:T(8,128)(2,1)S(1)} fusion(f32[1024,1024]{1,0:T(8,128)S(1)} %fusion.36, bf16[1024,2048]{1,0:T(8,128)(2,1)S(1)} %copy-done.7, bf16[1,2048,1024]{2,1,0:T(8,128)(2,1)S(1)} %copy-done.5), kind=kOutput, calls=%fused_computation.39 | convolution fusion | flops 4301258752 | bytes 14680064 | tf_op jit(solution)/shard_map/dot_general | solution.py:110
  242.2 6.1 %fusion.40 = bf16[1024,2048]{1,0:T(8,128)(2,1)} fusion(bf16[1024,1024]{1,0:T(8,128)(2,1)S(1)} %multiply_convert_fusion.1, bf16[1,1024,2048]{2,1,0:T(8,128)(2,1)S(1)} %copy-done.6), kind=kOutput, calls=%fused_computation.40 | convolution fusion | flops 4297064448 | bytes 10485760 | tf_op jit(solution)/shard_map/dot_general | solution.py:114
  248.3 13.5 %reduce-scatter.2.cloned.1.call-done = bf16[512,2048]{1,0:T(8,128)(2,1)} async-done(((bf16[1024,2048]{1,0:T(8,128)(2,1)}), bf16[512,2048]{1,0:T(8,128)(2,1)}) %reduce-scatter.2.cloned.1.call-update) | async-done | bytes 2097168 | tf_op jit(solution)/shard_map/reduce_scatter | solution.py:113
  261.8 7.1 %all-to-all-start.2 = ((bf16[16,32,2048]{2,1,0:T(8,128)(2,1)}), bf16[16,32,2048]{2,1,0:T(8,128)(2,1)S(1)}, u32[]{:S(2)}, u32[]{:S(2)}) async-start(bf16[16,32,2048]{2,1,0:T(8,128)(2,1)} %bitcast.107), calls=%async_computation.3 | async-start | bytes 4194304 | tf_op jit(solution)/shard_map/all_to_all | solution.py:120
  269.1 48.3 %all-to-all-done.2 = bf16[16,32,2048]{2,1,0:T(8,128)(2,1)S(1)} async-done(((bf16[16,32,2048]{2,1,0:T(8,128)(2,1)}), bf16[16,32,2048]{2,1,0:T(8,128)(2,1)S(1)}, u32[]{:S(2)}, u32[]{:S(2)}) %all-to-all-start.2) | async-done | bytes 2097184 | tf_op jit(solution)/shard_map/all_to_all | solution.py:120
  (126 shorter events, 79.0 us)
Async XLA Ops:
  6.5 44.0 %copy-start.2 = (bf16[256,512]{1,0:T(8,128)(2,1)S(1)}, bf16[256,512]{1,0:T(8,128)(2,1)}, u32[]{:S(2)}) copy-start(bf16[256,512]{1,0:T(8,128)(2,1)} %param.17) | copy-start | bytes 786436
  6.5 23.4 %copy-start.1 = (bf16[256,512]{1,0:T(8,128)(2,1)S(1)}, bf16[256,512]{1,0:T(8,128)(2,1)}, u32[]{:S(2)}) copy-start(bf16[256,512]{1,0:T(8,128)(2,1)} %param.16) | copy-start | bytes 786436
  6.5 222.6 %all-gather.2.cloned.1.call-start = ((), (), s32[]{:S(2)}) async-start(), calls=%async_computation.4 | async-start | bytes 6291456 | tf_op jit(solution)/shard_map/all_gather | solution.py:109
  7.3 22.9 %collective-permute-start = (s32[256]{0:T(256)S(1)}, s32[256]{0:T(256)S(1)}, u32[]{:S(2)}, u32[]{:S(2)}) collective-permute-start(s32[256]{0:T(256)S(1)} %get-tuple-element.167), channel_id=1, source_target_pairs={{0,2},{2,4},{4,6},{6,8},{8,10},{10,12},{12,14},{14,16},{16,18},{18... | collective-permute-start | bytes 3080 | tf_op jit(solution)/shard_map/ppermute | solution.py:13
  10.7 22.3 %collective-permute-start.1 = (s32[256]{0:T(256)S(1)}, s32[256]{0:T(256)S(1)}, u32[]{:S(2)}, u32[]{:S(2)}) collective-permute-start(s32[256]{0:T(256)S(1)} %get-tuple-element.167), channel_id=1, source_target_pairs={{2,0},{4,2},{6,4},{8,6},{10,8},{12,10},{14,12},{16,14},{18,16},{20... | collective-permute-start | bytes 3080 | tf_op jit(solution)/shard_map/ppermute | solution.py:13
  14.0 21.3 %collective-permute-start.2 = (s32[256]{0:T(256)S(1)}, s32[256]{0:T(256)S(1)}, u32[]{:S(2)}, u32[]{:S(2)}) collective-permute-start(s32[256]{0:T(256)S(1)} %get-tuple-element.167), channel_id=1, source_target_pairs={{0,4},{2,6},{4,8},{6,10},{8,12},{10,14},{12,16},{14,18},{16,20},{1... | collective-permute-start | bytes 3080 | tf_op jit(solution)/shard_map/ppermute | solution.py:13
  18.4 21.4 %collective-permute-start.3 = (s32[256]{0:T(256)S(1)}, s32[256]{0:T(256)S(1)}, u32[]{:S(2)}, u32[]{:S(2)}) collective-permute-start(s32[256]{0:T(256)S(1)} %get-tuple-element.167), channel_id=1, source_target_pairs={{4,0},{6,2},{8,4},{10,6},{12,8},{14,10},{16,12},{18,14},{20,16},{2... | collective-permute-start | bytes 3080 | tf_op jit(solution)/shard_map/ppermute | solution.py:13
  20.3 25.2 %collective-permute-start.4 = (s32[256]{0:T(256)S(1)}, s32[256]{0:T(256)S(1)}, u32[]{:S(2)}, u32[]{:S(2)}) collective-permute-start(s32[256]{0:T(256)S(1)} %get-tuple-element.167), channel_id=1, source_target_pairs={{0,6},{2,8},{4,10},{6,12},{8,14},{10,16},{12,18},{14,20},{16,22},{... | collective-permute-start | bytes 3080 | tf_op jit(solution)/shard_map/ppermute | solution.py:13
  30.1 17.3 %collective-permute-start.5 = (s32[256]{0:T(256)S(1)}, s32[256]{0:T(256)S(1)}, u32[]{:S(2)}, u32[]{:S(2)}) collective-permute-start(s32[256]{0:T(256)S(1)} %get-tuple-element.167), channel_id=1, source_target_pairs={{6,0},{8,2},{10,4},{12,6},{14,8},{16,10},{18,12},{20,14},{22,16},{... | collective-permute-start | bytes 3080 | tf_op jit(solution)/shard_map/ppermute | solution.py:13
  33.0 17.6 %collective-permute-start.12 = (bf16[256,512]{0,1:T(8,128)(2,1)S(1)}, bf16[256,512]{0,1:T(8,128)(2,1)S(1)}, u32[]{:S(2)}, u32[]{:S(2)}) collective-permute-start(bf16[256,512]{0,1:T(8,128)(2,1)S(1)} %copy.40), channel_id=1, source_target_pairs={{0,2},{2,4},{4,6},{6,8},{8,10},{10,12},{12,14},{14,16},{16,18},{18... | collective-permute-start | bytes 786440 | tf_op jit(solution)/shard_map/ppermute | solution.py:13
  35.4 19.8 %collective-permute-start.13 = (bf16[256,512]{0,1:T(8,128)(2,1)S(1)}, bf16[256,512]{0,1:T(8,128)(2,1)S(1)}, u32[]{:S(2)}, u32[]{:S(2)}) collective-permute-start(bf16[256,512]{0,1:T(8,128)(2,1)S(1)} %copy.40), channel_id=1, source_target_pairs={{2,0},{4,2},{6,4},{8,6},{10,8},{12,10},{14,12},{16,14},{18,16},{20... | collective-permute-start | bytes 786440 | tf_op jit(solution)/shard_map/ppermute | solution.py:13
  39.8 22.4 %collective-permute-start.14 = (bf16[256,512]{0,1:T(8,128)(2,1)S(1)}, bf16[256,512]{0,1:T(8,128)(2,1)S(1)}, u32[]{:S(2)}, u32[]{:S(2)}) collective-permute-start(bf16[256,512]{0,1:T(8,128)(2,1)S(1)} %copy.40), channel_id=1, source_target_pairs={{0,4},{2,6},{4,8},{6,10},{8,12},{10,14},{12,16},{14,18},{16,20},{1... | collective-permute-start | bytes 786440 | tf_op jit(solution)/shard_map/ppermute | solution.py:13
  45.5 58.1 %collective-permute-start.15 = (bf16[256,512]{0,1:T(8,128)(2,1)S(1)}, bf16[256,512]{0,1:T(8,128)(2,1)S(1)}, u32[]{:S(2)}, u32[]{:S(2)}) collective-permute-start(bf16[256,512]{0,1:T(8,128)(2,1)S(1)} %copy.40), channel_id=1, source_target_pairs={{4,0},{6,2},{8,4},{10,6},{12,8},{14,10},{16,12},{18,14},{20,16},{2... | collective-permute-start | bytes 786440 | tf_op jit(solution)/shard_map/ppermute | solution.py:13
  47.5 57.0 %collective-permute-start.16 = (bf16[256,512]{0,1:T(8,128)(2,1)S(1)}, bf16[256,512]{0,1:T(8,128)(2,1)S(1)}, u32[]{:S(2)}, u32[]{:S(2)}) collective-permute-start(bf16[256,512]{0,1:T(8,128)(2,1)S(1)} %copy.40), channel_id=1, source_target_pairs={{0,6},{2,8},{4,10},{6,12},{8,14},{10,16},{12,18},{14,20},{16,22},{... | collective-permute-start | bytes 786440 | tf_op jit(solution)/shard_map/ppermute | solution.py:13
  50.6 14.3 %collective-permute-start.6 = (bf16[256,512]{1,0:T(8,128)(2,1)S(1)}, bf16[256,512]{1,0:T(8,128)(2,1)S(1)}, u32[]{:S(2)}, u32[]{:S(2)}) collective-permute-start(bf16[256,512]{1,0:T(8,128)(2,1)S(1)} %copy-done.2), channel_id=1, source_target_pairs={{0,2},{2,4},{4,6},{6,8},{8,10},{10,12},{12,14},{14,16},{16,18},{18... | collective-permute-start | bytes 786440 | tf_op jit(solution)/shard_map/ppermute | solution.py:13
  55.1 16.0 %collective-permute-start.7 = (bf16[256,512]{1,0:T(8,128)(2,1)S(1)}, bf16[256,512]{1,0:T(8,128)(2,1)S(1)}, u32[]{:S(2)}, u32[]{:S(2)}) collective-permute-start(bf16[256,512]{1,0:T(8,128)(2,1)S(1)} %copy-done.2), channel_id=1, source_target_pairs={{2,0},{4,2},{6,4},{8,6},{10,8},{12,10},{14,12},{16,14},{18,16},{20... | collective-permute-start | bytes 786440 | tf_op jit(solution)/shard_map/ppermute | solution.py:13
  62.2 18.8 %collective-permute-start.8 = (bf16[256,512]{1,0:T(8,128)(2,1)S(1)}, bf16[256,512]{1,0:T(8,128)(2,1)S(1)}, u32[]{:S(2)}, u32[]{:S(2)}) collective-permute-start(bf16[256,512]{1,0:T(8,128)(2,1)S(1)} %copy-done.2), channel_id=1, source_target_pairs={{0,4},{2,6},{4,8},{6,10},{8,12},{10,14},{12,16},{14,18},{16,20},{1... | collective-permute-start | bytes 786440 | tf_op jit(solution)/shard_map/ppermute | solution.py:13
  64.9 29.6 %collective-permute-start.9 = (bf16[256,512]{1,0:T(8,128)(2,1)S(1)}, bf16[256,512]{1,0:T(8,128)(2,1)S(1)}, u32[]{:S(2)}, u32[]{:S(2)}) collective-permute-start(bf16[256,512]{1,0:T(8,128)(2,1)S(1)} %copy-done.2), channel_id=1, source_target_pairs={{4,0},{6,2},{8,4},{10,6},{12,8},{14,10},{16,12},{18,14},{20,16},{2... | collective-permute-start | bytes 786440 | tf_op jit(solution)/shard_map/ppermute | solution.py:13
  71.2 25.3 %collective-permute-start.10 = (bf16[256,512]{1,0:T(8,128)(2,1)S(1)}, bf16[256,512]{1,0:T(8,128)(2,1)S(1)}, u32[]{:S(2)}, u32[]{:S(2)}) collective-permute-start(bf16[256,512]{1,0:T(8,128)(2,1)S(1)} %copy-done.2), channel_id=1, source_target_pairs={{0,6},{2,8},{4,10},{6,12},{8,14},{10,16},{12,18},{14,20},{16,22},{... | collective-permute-start | bytes 786440 | tf_op jit(solution)/shard_map/ppermute | solution.py:13
  81.0 20.1 %collective-permute-start.11 = (bf16[256,512]{1,0:T(8,128)(2,1)S(1)}, bf16[256,512]{1,0:T(8,128)(2,1)S(1)}, u32[]{:S(2)}, u32[]{:S(2)}) collective-permute-start(bf16[256,512]{1,0:T(8,128)(2,1)S(1)} %copy-done.2), channel_id=1, source_target_pairs={{6,0},{8,2},{10,4},{12,6},{14,8},{16,10},{18,12},{20,14},{22,16},{... | collective-permute-start | bytes 786440 | tf_op jit(solution)/shard_map/ppermute | solution.py:13
  94.5 11.1 %collective-permute-start.17 = (bf16[256,512]{0,1:T(8,128)(2,1)S(1)}, bf16[256,512]{0,1:T(8,128)(2,1)}, u32[]{:S(2)}, u32[]{:S(2)}) collective-permute-start(bf16[256,512]{0,1:T(8,128)(2,1)S(1)} %copy.40), channel_id=1, source_target_pairs={{6,0},{8,2},{10,4},{12,6},{14,8},{16,10},{18,12},{20,14},{22,16},{... | collective-permute-start | bytes 786440 | tf_op jit(solution)/shard_map/ppermute | solution.py:13
  216.0 45.8 %reduce-scatter.2.cloned.1.call-start = ((), (), s32[]{:S(2)}) async-start(), calls=%async_computation.5 | async-start | bytes 6291456 | tf_op jit(solution)/shard_map/reduce_scatter | solution.py:113
  229.1 7.7 %copy-start.7 = (bf16[1024,2048]{1,0:T(8,128)(2,1)S(1)}, bf16[1024,2048]{1,0:T(8,128)(2,1)}, u32[]{:S(2)}) copy-start(bf16[1024,2048]{1,0:T(8,128)(2,1)} %all-gather.2.cloned.1.call-done) | copy-start | bytes 12582916
  261.8 55.5 %all-to-all-start.2 = ((bf16[16,32,2048]{2,1,0:T(8,128)(2,1)}), bf16[16,32,2048]{2,1,0:T(8,128)(2,1)S(1)}, u32[]{:S(2)}, u32[]{:S(2)}) async-start(bf16[16,32,2048]{2,1,0:T(8,128)(2,1)} %bitcast.107), calls=%async_computation.3 | async-start | bytes 4194304 | tf_op jit(solution)/shard_map/all_to_all | solution.py:120
  (6 other events, 33.7 us)
Sparse Core Ops, SparseCore 0:
  216.1 12.9 all-gather.1
  248.5 13.3 reduce-scatter.1
where the time goes:
time: 334 us; the launch traced here: 333 us
  starting transfers between devices  87.9 us (26%)
  waiting for transfers between devices  79.8 us (24%)
  blocking collectives  59.5 us (18%)
  matrix products  47.7 us (14%)
  local copies, waits for them, and re-layouts  25.8 us (8%)
  other arithmetic  18.1 us (5%)
  between operations  13.9 us (4%)
    ppermute x18, starting transfers between devices, shifted(): lax.ppermute(value, axis, [(source, source + steps) for source in range(f...  80.6 us
    all_to_all x1, blocking collectives, on_device(): lax.all_to_all(outgoing, 'sp', split_axis=0, concat_axis=0, tiled=True)  55.6 us
    all_to_all x1, waiting for transfers between devices, on_device(): lax.all_to_all(answer, 'sp', split_axis=0, concat_axis=0, tiled=True)  48.3 us
    sub x4, matrix products, attend(): lifted = jnp.exp(masked - largest)  16.8 us
    reduce_scatter x1, waiting for transfers between devices, on_device(): lax.psum_scatter(jnp.dot(hidden, down_weight[0], preferred_element_type=j...  13.5 us
    all_gather x1, waiting for transfers between devices, on_device(): lax.all_gather(arrived.reshape(-1, model_width), 'tp', axis=0, tiled=True)  12.9 us
    div x4, other arithmetic, attend(): probabilities = lifted / jnp.sum(lifted, axis=-1, keepdims=True)  10.3 us
    dot_general x4, matrix products, attend(): head_out = jnp.dot(weights, head_values, preferred_element_type=jnp.float32)  8.81 us
  transfers between devices with their start and end apart: 21, of which 5 were waited for; matrix products, arithmetic and copies ran while one was open for 4% of the time, Pallas kernels for 0%

commit v1 on v0

v1 whole, which is shorter than its diff:
```python
import functools

import jax
import jax.numpy as jnp
from jax import lax
from jax.experimental import pallas as pl
from jax.experimental.pallas import tpu as pltpu
from jax.sharding import PartitionSpec as P

HD = 64
REACH = 3
EPS = 1e-06
BF = jnp.bfloat16
F32 = jnp.float32
VM = pl.BlockSpec(memory_space=pltpu.VMEM)
SM = pl.BlockSpec(memory_space=pltpu.SMEM)
ANY = pl.BlockSpec(memory_space=pl.ANY)
PARAMS = pltpu.CompilerParams(vmem_limit_bytes=56 * 1024 * 1024)


def cost(flops, bytes_accessed):
    return pl.CostEstimate(flops=flops, bytes_accessed=bytes_accessed, transcendentals=0)


def pack_kernel(q_ref, k_ref, v_ref, id_ref, qo_ref, kv_ref):
    heads, length, width = qo_ref.shape
    for h in range(heads):
        columns = slice(h * width, (h + 1) * width)
        qo_ref[h] = (q_ref[:, columns].astype(F32) * (HD**-0.5)).astype(BF)
        kv_ref[h, :length, :width] = k_ref[:, columns]
        kv_ref[h, :length, width:] = v_ref[:, columns]
        kv_ref[h, length:, :] = jnp.broadcast_to(id_ref[...], kv_ref[h, length:, :].shape)


def pack(query_rows, key_rows, value_rows, id_row, heads):
    length = query_rows.shape[0]
    width = query_rows.shape[1] // heads
    return pl.pallas_call(
        pack_kernel,
        in_specs=[VM] * 4,
        out_specs=[VM, VM],
        out_shape=[
            jax.ShapeDtypeStruct((heads, length, width), BF),
            jax.ShapeDtypeStruct((heads, length + 16, 2 * width), BF),
        ],
        compiler_params=PARAMS,
        name="pack",
    )(query_rows, key_rows, value_rows, id_row)


def attention_kernel(
    lam_ref, q_ref, prev_ref, own_ref, next_ref, o_ref, kv_ref, id_ref, s_ref, m_ref, l_ref, a_ref
):
    b = pl.program_id(0)
    length, width = o_ref.shape[1:]
    before, group, after = prev_ref.shape[0], own_ref.shape[0], next_ref.shape[0]
    span = before + 1 + after

    @pl.when(b == 0)
    def _():
        id_ref[...] = jnp.zeros_like(id_ref)
        for first, ref in ((0, prev_ref), (before, own_ref), (before + group, next_ref)):
            for i in range(ref.shape[0]):
                kv_ref[first + i] = ref[i, :length, :]
                id_ref[first + i : first + i + 1, :] = ref[i, length : length + 16, :].astype(F32)[:1]

    query_ids = id_ref[pl.ds(b + before, 1), :]
    low = jnp.min(query_ids, axis=1, keepdims=True)
    high = jnp.max(query_ids, axis=1, keepdims=True)
    ids = id_ref[...]
    smallest = jnp.min(ids, axis=1, keepdims=True)
    largest = jnp.max(ids, axis=1, keepdims=True)
    place = lax.broadcasted_iota(jnp.int32, smallest.shape, 0) - b
    apart = (largest < low) | (smallest > high)
    left = jnp.sum(jnp.where(apart & (place >= 0) & (place < before), 1.0, 0.0))
    right = jnp.sum(jnp.where(apart & (place > before) & (place < span), 1.0, 0.0))
    start = left.astype(jnp.int32)
    stop = span - right.astype(jnp.int32)
    query_column = jnp.transpose(jnp.broadcast_to(query_ids, (128, length)))

    q = q_ref[b]
    zero = jnp.zeros((length, HD), BF)
    stacked = jnp.concatenate(
        [
            jnp.concatenate([q[:, :HD], zero], axis=1),
            jnp.concatenate([zero, q[:, HD:]], axis=1),
        ],
        axis=0,
    )
    m_ref[...] = jnp.full_like(m_ref, -1e30)
    l_ref[...] = jnp.zeros_like(l_ref)
    a_ref[...] = jnp.zeros_like(a_ref)

    def score(j, carry):
        keys = kv_ref[b + j, :, :width]
        scores = lax.dot_general(
            stacked, keys, (((1,), (1,)), ((), ())), preferred_element_type=F32
        )
        key_ids = id_ref[pl.ds(b + j, 1), :]
        for c in range(2):
            rows = slice(c * length, (c + 1) * length)
            best = m_ref[rows, :]
            for part in range(length // 128):
                columns = slice(part * 128, (part + 1) * 128)
                piece = jnp.where(
                    query_column == key_ids[:, columns], scores[rows, columns], -1e30
                )
                s_ref[j, rows, columns] = piece
                best = jnp.maximum(best, piece)
            m_ref[rows, :] = best
        return carry

    lax.fori_loop(start, stop, score, 0)
    top = jnp.max(m_ref[...], axis=1, keepdims=True)

    def lift(j, carry):
        lifted = jnp.exp(s_ref[j] - top)
        s_ref[j] = lifted
        total = l_ref[...]
        for part in range(length // 128):
            total = total + lifted[:, part * 128 : (part + 1) * 128]
        l_ref[...] = total
        return carry

    lax.fori_loop(start, stop, lift, 0)
    total = jnp.sum(l_ref[...], axis=1, keepdims=True)
    first = 1.0 / total[:length]
    second = lam_ref[0] / total[length:]

    def gather(j, carry):
        weights = (s_ref[j, :length, :] * first - s_ref[j, length:, :] * second).astype(BF)
        a_ref[...] += jnp.dot(weights, kv_ref[b + j, :, width:], preferred_element_type=F32)
        return carry

    lax.fori_loop(start, stop, gather, 0)
    out = a_ref[...]
    scale = lax.rsqrt(jnp.mean(out * out, axis=1, keepdims=True) + EPS)
    o_ref[b] = (out * scale).astype(BF)


def attention(lam, q, prev, own, following):
    group, length, width = q.shape
    before, after = prev.shape[0], following.shape[0]
    span = before + 1 + after
    return pl.pallas_call(
        attention_kernel,
        grid=(group,),
        in_specs=[SM] + [VM] * 4,
        out_specs=VM,
        out_shape=jax.ShapeDtypeStruct((group, length, width), BF),
        scratch_shapes=[
            pltpu.VMEM((before + group + after, length, 2 * width), BF),
            pltpu.VMEM((-(-(before + group + after) // 8) * 8, length), F32),
            pltpu.VMEM((span, 2 * length, length), F32),
            pltpu.VMEM((2 * length, 128), F32),
            pltpu.VMEM((2 * length, 128), F32),
            pltpu.VMEM((length, width), F32),
        ],
        compiler_params=PARAMS,
        cost_estimate=cost(8 * 10**9, 4 * 10**6),
        name="attention",
    )(lam, q, prev, own, following)


def project_kernel(
    heads_ref, residual_ref, gain_ref, meta_ref, weight_ref, mixed_ref, rows_ref, left_ref
):
    n = pl.program_id(0)
    tile = weight_ref.shape[1]
    tokens, width = mixed_ref.shape
    members = heads_ref.shape[0]
    value_dim = heads_ref.shape[2]

    @pl.when(n == 0)
    def _():
        for source in range(members):
            head = (source % 2) * (members // 2) + source // 2
            left_ref[:, head * value_dim : (head + 1) * value_dim] = heads_ref[source]

    columns = pl.ds(pl.multiple_of(n * tile, tile), tile)
    projected = jnp.dot(left_ref[...], weight_ref[...], preferred_element_type=F32)
    mixed_ref[:, columns] = (residual_ref[:, columns].astype(F32) + projected).astype(BF)

    @pl.when(n == pl.num_programs(0) - 1)
    def _():
        wide = mixed_ref[...].astype(F32)
        scale = lax.rsqrt(jnp.mean(wide * wide, axis=1, keepdims=True) + EPS)
        normed = (wide * scale * gain_ref[...]).astype(BF)
        slots = rows_ref.shape[0]
        place = lax.broadcasted_iota(jnp.int32, (slots, tokens), 0).astype(F32)
        pick = (place == meta_ref[0:1, :]) | (place == meta_ref[1:2, :])
        rows_ref[...] = jnp.dot(
            jnp.where(pick, 1.0, 0.0).astype(BF), normed, preferred_element_type=F32
        ).astype(BF)


def project(heads, residual, gain, meta, out_weight, slots, tile=512):
    members, tokens, value_dim = heads.shape
    depth, width = out_weight.shape
    return pl.pallas_call(
        project_kernel,
        grid=(width // tile,),
        in_specs=[VM, VM, VM, VM, pl.BlockSpec((depth, tile), lambda n: (0, n))],
        out_specs=[VM, VM],
        out_shape=[
            jax.ShapeDtypeStruct((tokens, width), BF),
            jax.ShapeDtypeStruct((slots, width), BF),
        ],
        scratch_shapes=[pltpu.VMEM((tokens, depth), BF)],
        compiler_params=PARAMS,
        cost_estimate=cost(3 * 10**9, 8 * 10**6),
        name="project",
    )(heads, residual, gain, meta, out_weight)


def expert_kernel(
    x_ref, g0, u0, d0, g1, u1, d1, y_ref, gb, ub, db, acc_ref, half_ref, sems, *, tile, slots
):
    per_half = g0.shape[1] // tile
    steps = 2 * per_half
    sources = ((g0, u0, d0), (g1, u1, d1))

    def copies(step):
        g, u, d = sources[step // per_half]
        at = (step % per_half) * tile
        slot = step % slots
        return (
            pltpu.make_async_copy(g.at[:, pl.ds(at, tile)], gb.at[slot], sems.at[slot, 0]),
            pltpu.make_async_copy(u.at[:, pl.ds(at, tile)], ub.at[slot], sems.at[slot, 1]),
            pltpu.make_async_copy(d.at[pl.ds(at, tile), :], db.at[slot], sems.at[slot, 2]),
        )

    for step in range(min(slots - 1, steps)):
        for copy in copies(step):
            copy.start()
    for step in range(steps):
        if step + slots - 1 < steps:
            for copy in copies(step + slots - 1):
                copy.start()
        for copy in copies(step):
            copy.wait()
        slot = step % slots
        x = x_ref[...]
        gate = jnp.dot(x, gb[slot], preferred_element_type=F32)
        upward = jnp.dot(x, ub[slot], preferred_element_type=F32)
        hidden = (gate / (1.0 + jnp.exp(-gate)) * upward).astype(BF)
        part = jnp.dot(hidden, db[slot], preferred_element_type=F32)
        if step % per_half == 0:
            acc_ref[...] = part
        else:
            acc_ref[...] += part
        if step == per_half - 1:
            half_ref[...] = acc_ref[...].astype(BF)
    y_ref[...] = (
        half_ref[...].astype(F32) + acc_ref[...].astype(BF).astype(F32)
    ).astype(BF)


def experts_of(x, own, other, tile=256, slots=3):
    rows, width = x.shape
    return pl.pallas_call(
        functools.partial(expert_kernel, tile=tile, slots=slots),
        in_specs=[VM] + [ANY] * 6,
        out_specs=VM,
        out_shape=jax.ShapeDtypeStruct((rows, width), BF),
        scratch_shapes=[
            pltpu.VMEM((slots, width, tile), BF),
            pltpu.VMEM((slots, width, tile), BF),
            pltpu.VMEM((slots, tile, width), BF),
            pltpu.VMEM((rows, width), F32),
            pltpu.VMEM((rows, width), BF),
            pltpu.SemaphoreType.DMA((slots, 3)),
        ],
        compiler_params=PARAMS,
        cost_estimate=cost(9 * 10**9, 26 * 10**6),
        name="experts",
    )(x, *own, *other)


def picked(meta_ref, rows_ref):
    slots = rows_ref.shape[0]
    tokens = meta_ref.shape[1]
    columns = jnp.transpose(meta_ref[...])
    place = lax.broadcasted_iota(jnp.int32, (tokens, slots), 1).astype(F32)
    total = None
    for k in range(2):
        pick = jnp.where(place == columns[:, k : k + 1], 1.0, 0.0).astype(BF)
        rows = jnp.dot(pick, rows_ref[...], preferred_element_type=F32)
        part = rows * columns[:, 2 + k : 3 + k]
        total = part if total is None else total + part
    return total


def partial_kernel(meta_ref, rows_ref, o_ref):
    o_ref[...] = picked(meta_ref, rows_ref).astype(BF)


def final_kernel(meta_ref, rows_ref, mixed_ref, far_ref, o_ref):
    total = picked(meta_ref, rows_ref) + far_ref[...].astype(F32)
    o_ref[...] = (mixed_ref[...].astype(F32) + total).astype(BF)


def partial_sum(meta, rows):
    return pl.pallas_call(
        partial_kernel,
        in_specs=[VM] * 2,
        out_specs=VM,
        out_shape=jax.ShapeDtypeStruct((meta.shape[1], rows.shape[1]), BF),
        compiler_params=PARAMS,
        cost_estimate=cost(10**9, 2 * 10**6),
        name="partial_sum",
    )(meta, rows)


def final_sum(meta, rows, mixed, far):
    return pl.pallas_call(
        final_kernel,
        in_specs=[VM] * 4,
        out_specs=VM,
        out_shape=jax.ShapeDtypeStruct(mixed.shape, BF),
        compiler_params=PARAMS,
        cost_estimate=cost(10**9, 3 * 10**6),
        name="final_sum",
    )(meta, rows, mixed, far)


def ranks_of(routes, experts):
    tokens = routes.shape[0]
    table = (routes[:, :, None] == jnp.arange(experts, dtype=jnp.int32)).astype(F32)
    named = jnp.sum(table, axis=1)
    order = jnp.arange(tokens)
    below = (order[:, None] > order[None, :]).astype(BF)
    earlier = jnp.dot(below, named.astype(BF), preferred_element_type=F32)
    return jnp.sum(earlier[:, None, :] * table, axis=2)


def meta_of(routes, ranks, route_weights, first, count, capacity):
    local = routes - first
    inside = (local >= 0) & (local < count)
    target = jnp.where(inside, local.astype(F32) * capacity + ranks, -1.0)
    rows = jnp.concatenate([target.T, route_weights.T], axis=0)
    return jnp.concatenate([rows, jnp.zeros((8 - rows.shape[0], rows.shape[1]), F32)], axis=0)


def on_device(
    residual,
    query_rows,
    key_rows,
    value_rows,
    mix_lambda,
    documents,
    out_weight,
    norm_gain,
    gate_weight,
    up_weight,
    down_weight,
    routes,
    route_weights,
):
    length = query_rows.shape[0]
    heads = mix_lambda.shape[0]
    width = residual.shape[1]
    count = lax.axis_size("sp")
    twins = lax.axis_size("tp")
    here = lax.axis_index("sp")
    half = count // 2
    capacity = 2 * length // count
    planes = [[g * heads + j for j in range(heads)] for g in range(count // heads)]
    halves = [[h * half + j for j in range(half)] for h in range(2)]
    mirror = [(i, (i + half) % count) for i in range(count)]
    swap = [(i, twins - 1 - i) for i in range(twins)]

    id_row = (documents + 1).astype(BF).reshape(1, length)
    queries, pairs = pack(query_rows, key_rows, value_rows, id_row, heads)
    pairs = lax.all_to_all(pairs, "sp", 0, 0, tiled=True, axis_index_groups=planes)
    prev = lax.ppermute(
        pairs[heads - REACH :], "sp", [(i, i + heads) for i in range(count - heads)]
    )
    following = lax.ppermute(
        pairs[:REACH], "sp", [(i + heads, i) for i in range(count - heads)]
    )
    queries = lax.all_to_all(queries, "sp", 0, 0, tiled=True, axis_index_groups=planes)

    ranks = ranks_of(routes, count)
    my_half = here // half
    meta_own = meta_of(routes, ranks, route_weights, my_half * half, half, capacity)
    meta_far = meta_of(routes, ranks, route_weights, (1 - my_half) * half, half, capacity)
    meta_far = lax.ppermute(meta_far, "sp", mirror)
    residual_late, _ = lax.optimization_barrier((residual, pairs))
    residual_far = lax.ppermute(residual_late, "sp", mirror)

    own = (gate_weight[0], up_weight[0], down_weight[0])
    other = tuple(lax.ppermute(weight, "tp", swap) for weight in own)

    lam = lax.dynamic_slice(mix_lambda, (here % heads,), (1,))
    outs = attention(lam, queries, prev, pairs, following)
    outs = outs.reshape(heads * twins, length // twins, outs.shape[2])
    both = [[g * heads * twins + j for j in range(heads * twins)] for g in range(count // heads)]
    token_heads = lax.all_to_all(
        outs, ("sp", "tp"), 0, 0, tiled=True, axis_index_groups=both
    )
    heads_far = lax.ppermute(token_heads, "sp", mirror)

    gain = norm_gain.reshape(1, width)
    slots = half * capacity

    def exchange(rows):
        rows = rows.reshape(half, capacity, width)
        rows = lax.all_to_all(rows, "sp", 0, 0, tiled=True, axis_index_groups=halves)
        return rows.reshape(slots, width)

    mixed, rows_own = project(token_heads, residual, gain, meta_own, out_weight, slots)
    rows_own = exchange(rows_own)
    _, rows_far = project(heads_far, residual_far, gain, meta_far, out_weight, slots)
    rows_far = exchange(rows_far)
    answer_own = experts_of(rows_own, own, other)
    answer_far = experts_of(rows_far, own, other)
    back_far = exchange(answer_far)
    part_far = partial_sum(meta_far, back_far)
    part = lax.ppermute(part_far, "sp", mirror)
    back_own = exchange(answer_own)
    return final_sum(meta_own, back_own, mixed, part)


def solution(mesh):
    placed = (
        P(("sp", "tp"), None),
        P("sp", "tp"),
        P("sp", "tp"),
        P("sp", "tp"),
        P("tp"),
        P("sp"),
        P(),
        P(),
        P("sp", None, "tp"),
        P("sp", None, "tp"),
        P("sp", "tp", None),
        P(("sp", "tp"), None),
        P(("sp", "tp"), None),
    )
    return jax.shard_map(
        on_device, mesh=mesh, in_specs=placed, out_specs=P(("sp", "tp"), None), check_vma=False
    )
```

time: 334 us -> 184 us (0.55)
  blocking collectives: 59.5 us -> 0 us
  Pallas kernels: 0 us -> 58.3 us
  matrix products: 47.7 us -> 0.14 us
  starting transfers between devices: 87.9 us -> 46.5 us
  local copies, waits for them, and re-layouts: 25.8 us -> 2.92 us
  other arithmetic: 18.1 us -> 2.12 us
  between operations: 13.9 us -> 0.16 us
  waiting for transfers between devices: 79.8 us -> 70.8 us
    ppermute x18 -> x9, starting transfers between devices: 80.6 us -> 13 us  [the longest x1 4 us: on_device(): part = lax.ppermute(part_far, 'sp', mirror)]
    all_to_all x2 -> x0, blocking collectives: 59.5 us -> none  [the longest x1 55.6 us: on_device(): lax.all_to_all(outgoing, 'sp', split_axis=0, concat_axis=0, tiled=True)]
    pallas_call x0 -> x8, Pallas kernels: none -> 58.3 us  [the longest x2 25.2 us: experts_of(): pl.pallas_call(functools.partial(expert_kernel, tile=tile, slots=slots),...]
    ppermute x18 -> x9, waiting for transfers between devices: 5.1 us -> 43.9 us  [the longest x1 14.7 us: on_device(): lax.ppermute(pairs[:REACH], 'sp', [(i + heads, i) for i in range(count -...]
    dot_general x8 -> x1, matrix products: 30.9 us -> 0.14 us  [ranks_of(): earlier = jnp.dot(below, named.astype(BF), preferred_element_type=F32)]
    all_to_all x1 -> x7, starting transfers between devices: 7.1 us -> 33.5 us  [the longest x4 21.2 us: exchange(): lax.all_to_all(rows, 'sp', 0, 0, tiled=True, axis_index_groups=halves)]
    all_to_all x1 -> x7, waiting for transfers between devices: 48.3 us -> 26.9 us  [the longest x4 19.5 us: exchange(): lax.all_to_all(rows, 'sp', 0, 0, tiled=True, axis_index_groups=halves)]
    sub x4 -> x0, matrix products: 16.8 us -> none  [attend(): lifted = jnp.exp(masked - largest)]
  transfers between devices with their start and end apart: 21 -> 16, of which waited for: 5 -> 9; matrix products, arithmetic and copies ran while one was open for 4% -> 1% of each run, Pallas kernels for 0% -> 29%
where the time goes in v1:
time: 184 us; the launch traced here: 181 us
  waiting for transfers between devices  70.8 us (38%)
  Pallas kernels  58.3 us (32%)
  starting transfers between devices  46.5 us (25%)
  local copies, waits for them, and re-layouts  2.92 us (2%)
  other arithmetic  2.12 us (1%)
    pallas_call x2, Pallas kernels, experts_of(): pl.pallas_call(functools.partial(expert_kernel, tile=tile, slots=slots),...  25.2 us
    all_to_all x4, starting transfers between devices, exchange(): lax.all_to_all(rows, 'sp', 0, 0, tiled=True, axis_index_groups=halves)  21.2 us
    all_to_all x4, waiting for transfers between devices, exchange(): lax.all_to_all(rows, 'sp', 0, 0, tiled=True, axis_index_groups=halves)  19.5 us
    ppermute x1, waiting for transfers between devices, on_device(): lax.ppermute(pairs[:REACH], 'sp', [(i + heads, i) for i in range(count -...  14.7 us
    pallas_call x1, Pallas kernels, attention(): pl.pallas_call(attention_kernel, grid=(group,), in_specs=[SM] + [VM] * 4,...  14.1 us
    pallas_call x2, Pallas kernels, project(): pl.pallas_call(project_kernel, grid=(width // tile,), in_specs=[VM, VM, V...  11.1 us
    ppermute x1, waiting for transfers between devices, on_device(): heads_far = lax.ppermute(token_heads, 'sp', mirror)  10.9 us
    ppermute x1, waiting for transfers between devices, on_device(): part = lax.ppermute(part_far, 'sp', mirror)  9.18 us
  transfers between devices with their start and end apart: 16, of which 9 were waited for; matrix products, arithmetic and copies ran while one was open for 1% of the time, Pallas kernels for 29%

profile of v1, /device:TPU:12, one launch (start us, length us, event | category | flops | bytes accessed | tf_op | source)
XLA Modules:
  0.0 180.9 jit_solution(4491867187693223785)
XLA Ops:
  3.5 4.2 %all-to-all-start.1 = ((bf16[4,272,256]{2,1,0:T(8,128)(2,1)}), bf16[4,272,256]{2,1,0:T(8,128)(2,1)S(1)}, u32[]{:S(2)}, u32[]{:S(2)}) async-start(bf16[4,272,256]{2,1,0:T(8,128)(2,1)} %get-tuple-element.12), calls=%async_computation.1 | async-start | bytes 1114112 | tf_op jit(solution)/shard_map/all_to_all | solution.py:375
  8.2 7.3 %all-to-all-done.1.own_ref = bf16[4,272,256]{2,1,0:T(8,128)(2,1)S(1)} async-done(((bf16[4,272,256]{2,1,0:T(8,128)(2,1)}), bf16[4,272,256]{2,1,0:T(8,128)(2,1)S(1)}, u32[]{:S(2)}, u32[]{:S(2)}) %all-to-all-start.1) | async-done | bytes 557088 | tf_op jit(solution)/shard_map/all_to_all | solution.py:375
  15.5 3.9 %all-to-all-start = ((bf16[4,256,128]{2,1,0:T(8,128)(2,1)}), bf16[4,256,128]{2,1,0:T(8,128)(2,1)S(1)}, u32[]{:S(2)}, u32[]{:S(2)}) async-start(bf16[4,256,128]{2,1,0:T(8,128)(2,1)} %get-tuple-element.11), calls=%async_computation | async-start | bytes 524288 | tf_op jit(solution)/shard_map/all_to_all | solution.py:382
  19.5 3.5 %collective-permute-start = (bf16[3,272,256]{2,1,0:T(8,128)(2,1)S(1)}, bf16[3,272,256]{2,1,0:T(8,128)(2,1)S(1)}, u32[]{:S(2)}, u32[]{:S(2)}) collective-permute-start(bf16[3,272,256]{2,1,0:T(8,128)(2,1)S(1)} %get-tuple-element.18), channel_id=1, source_target_pairs={{0,8},{2,10},{4,12},{6,14},{8,16},{10,18},{12,20},{14,22},{16,24},... | collective-permute-start | bytes 1253384 | tf_op jit(solution)/shard_map/ppermute | solution.py:376
  27.0 4.5 %collective-permute-done.prev_ref = bf16[3,272,256]{2,1,0:T(8,128)(2,1)S(1)} collective-permute-done((bf16[3,272,256]{2,1,0:T(8,128)(2,1)S(1)}, bf16[3,272,256]{2,1,0:T(8,128)(2,1)S(1)}, u32[]{:S(2)}, u32[]{:S(2)}) %collective-permute-start) | collective-permute-done | bytes 417824 | tf_op jit(solution)/shard_map/ppermute | solution.py:376
  31.5 2.6 %collective-permute-start.7 = (bf16[128,2048]{1,0:T(8,128)(2,1)S(1)}, bf16[128,2048]{1,0:T(8,128)(2,1)S(1)}, u32[]{:S(2)}, u32[]{:S(2)}) collective-permute-start(bf16[128,2048]{1,0:T(8,128)(2,1)S(1)} %copy-done.9), channel_id=1, source_target_pairs={{0,16},{2,18},{4,20},{6,22},{8,24},{10,26},{12,28},{14,30},{16,0},... | collective-permute-start | bytes 1572872 | tf_op jit(solution)/shard_map/ppermute | solution.py:390
  34.0 14.7 %collective-permute-done.1.next_ref = bf16[3,272,256]{2,1,0:T(8,128)(2,1)} collective-permute-done((bf16[3,272,256]{2,1,0:T(8,128)(2,1)S(1)}, bf16[3,272,256]{2,1,0:T(8,128)(2,1)}, u32[]{:S(2)}, u32[]{:S(2)}) %collective-permute-start.1) | collective-permute-done | bytes 417824 | tf_op jit(solution)/shard_map/ppermute | solution.py:379
  48.8 14.1 %attention.1 = bf16[4,256,128]{2,1,0:T(8,128)(2,1)} custom-call(f32[1]{0:T(128)} %dynamic_slice.3.lam_ref, bf16[4,256,128]{2,1,0:T(8,128)(2,1)} %copy-done.5, bf16[3,272,256]{2,1,0:T(8,128)(2,1)} %copy-done.12, bf16[4,272,256]{2,1,0:T(8,128)(2,1)} %copy-done, bf16[3,272,256]{2,1,0:T(8,128)(2,1)} %collective-permute-done.1.next_ref), custom_call_target="tpu_custom_call" | custom-call | flops 8000000000 | bytes 4000000 | tf_op jit(solution)/shard_map/attention/pallas_call | solution.py:145
  62.9 4.2 %all-to-all-start.2 = ((bf16[8,128,128]{2,1,0:T(8,128)(2,1)}), bf16[8,128,128]{2,1,0:T(8,128)(2,1)S(1)}, u32[]{:S(2)}, u32[]{:S(2)}) async-start(bf16[8,128,128]{2,1,0:T(8,128)(2,1)} %bitcast.27), calls=%async_computation.2 | async-start | bytes 524288 | tf_op jit(solution)/shard_map/all_to_all | solution.py:399
  67.8 4.6 %collective-permute-done.5.meta_ref = f32[8,128]{1,0:T(8,128)S(1)} collective-permute-done((f32[8,128]{1,0:T(8,128)S(1)}, f32[8,128]{1,0:T(8,128)S(1)}, u32[]{:S(2)}, u32[]{:S(2)}) %collective-permute-start.5) | collective-permute-done | bytes 4128 | tf_op jit(solution)/shard_map/ppermute | solution.py:388
  72.6 10.9 %collective-permute-done.6.heads_ref = bf16[8,128,128]{2,1,0:T(8,128)(2,1)S(1)} collective-permute-done((bf16[8,128,128]{2,1,0:T(8,128)(2,1)S(1)}, bf16[8,128,128]{2,1,0:T(8,128)(2,1)S(1)}, u32[]{:S(2)}, u32[]{:S(2)}) %collective-permute-start.6) | collective-permute-done | bytes 262176 | tf_op jit(solution)/shard_map/ppermute | solution.py:402
  84.1 5.6 %project.3 = (bf16[128,2048]{1,0:T(8,128)(2,1)}, bf16[256,2048]{1,0:T(8,128)(2,1)}) custom-call(bf16[8,128,128]{2,1,0:T(8,128)(2,1)} %copy-done.13, bf16[128,2048]{1,0:T(8,128)(2,1)} %copy-done.10, f32[1,2048]{1,0:T(1,128)} %bitcast.38, f32[8,128]{1,0:T(8,128)} %copy-done.14, bf16[1024,2048]{1,0:T(8,128)(2,1)} %weight_ref.3), custom_call_target="tpu_custom_call" | custom-call | flops 3000000000 | bytes 8000000 | tf_op jit(solution)/shard_map/project/pallas_call | solution.py:200
  89.7 5.7 %all-to-all-start.5 = ((bf16[8,32,2048]{2,1,0:T(8,128)(2,1)}), bf16[8,32,2048]{2,1,0:T(8,128)(2,1)S(1)}, u32[]{:S(2)}, u32[]{:S(2)}) async-start(bf16[8,32,2048]{2,1,0:T(8,128)(2,1)} %bitcast.26), calls=%async_computation.5 | async-start | bytes 2097152 | tf_op jit(solution)/shard_map/all_to_all | solution.py:409
  95.5 5.6 %project.2 = (bf16[128,2048]{1,0:T(8,128)(2,1)}, bf16[256,2048]{1,0:T(8,128)(2,1)}) custom-call(bf16[8,128,128]{2,1,0:T(8,128)(2,1)} %copy-done.6, bf16[128,2048]{1,0:T(8,128)(2,1)} %residual_ref.1, f32[1,2048]{1,0:T(1,128)} %bitcast.39, f32[8,128]{1,0:T(8,128)} %get-tuple-element.22.meta_ref, bf16[1024,2048]{1,0:T(8,128)(2,1)} %weight_ref.3), custom_call_target="tpu_custom_call" | custom-call | flops 3000000000 | bytes 8000000 | tf_op jit(solution)/shard_map/project/pallas_call | solution.py:200
  101.0 6.6 %all-to-all-done.5 = bf16[8,32,2048]{2,1,0:T(8,128)(2,1)S(1)} async-done(((bf16[8,32,2048]{2,1,0:T(8,128)(2,1)}), bf16[8,32,2048]{2,1,0:T(8,128)(2,1)S(1)}, u32[]{:S(2)}, u32[]{:S(2)}) %all-to-all-start.5) | async-done | bytes 1048608 | tf_op jit(solution)/shard_map/all_to_all | solution.py:409
  107.7 5.2 %all-to-all-start.3 = ((bf16[8,32,2048]{2,1,0:T(8,128)(2,1)}), bf16[8,32,2048]{2,1,0:T(8,128)(2,1)S(1)}, u32[]{:S(2)}, u32[]{:S(2)}) async-start(bf16[8,32,2048]{2,1,0:T(8,128)(2,1)} %bitcast.21), calls=%async_computation.3 | async-start | bytes 2097152 | tf_op jit(solution)/shard_map/all_to_all | solution.py:409
  112.9 12.6 %experts.3 = bf16[256,2048]{1,0:T(8,128)(2,1)} custom-call(bf16[256,2048]{1,0:T(8,128)(2,1)} %bitcast.19, bf16[2048,1024]{1,0:T(8,128)(2,1)} %bitcast.30, bf16[2048,1024]{1,0:T(8,128)(2,1)} %bitcast.33, bf16[1024,2048]{1,0:T(8,128)(2,1)} %bitcast.36, bf16[2048,1024]{1,0:T(8,128)(2,1)} %collective-permute-done.2.g1, ...), custom_call_target="tpu_custom_call" | custom-call | flops 8999999488 | bytes 26000000 | tf_op jit(solution)/shard_map/experts/pallas_call | solution.py:261
  125.6 5.1 %all-to-all-start.6 = ((bf16[8,32,2048]{2,1,0:T(8,128)(2,1)}), bf16[8,32,2048]{2,1,0:T(8,128)(2,1)S(1)}, u32[]{:S(2)}, u32[]{:S(2)}) async-start(bf16[8,32,2048]{2,1,0:T(8,128)(2,1)} %bitcast.25), calls=%async_computation.6 | async-start | bytes 2097152 | tf_op jit(solution)/shard_map/all_to_all | solution.py:409
  130.7 12.6 %experts.2 = bf16[256,2048]{1,0:T(8,128)(2,1)} custom-call(bf16[256,2048]{1,0:T(8,128)(2,1)} %bitcast.20, bf16[2048,1024]{1,0:T(8,128)(2,1)} %bitcast.31, bf16[2048,1024]{1,0:T(8,128)(2,1)} %bitcast.34, bf16[1024,2048]{1,0:T(8,128)(2,1)} %bitcast.37, bf16[2048,1024]{1,0:T(8,128)(2,1)} %collective-permute-done.2.g1, ...), custom_call_target="tpu_custom_call" | custom-call | flops 8999999488 | bytes 26000000 | tf_op jit(solution)/shard_map/experts/pallas_call | solution.py:261
  143.4 5.1 %all-to-all-start.4 = ((bf16[8,32,2048]{2,1,0:T(8,128)(2,1)}), bf16[8,32,2048]{2,1,0:T(8,128)(2,1)S(1)}, u32[]{:S(2)}, u32[]{:S(2)}) async-start(bf16[8,32,2048]{2,1,0:T(8,128)(2,1)} %bitcast.24), calls=%async_computation.4 | async-start | bytes 2097152 | tf_op jit(solution)/shard_map/all_to_all | solution.py:409
  151.0 4.0 %collective-permute-start.8 = (bf16[128,2048]{1,0:T(8,128)(2,1)}, bf16[128,2048]{1,0:T(8,128)(2,1)S(1)}, u32[]{:S(2)}, u32[]{:S(2)}) collective-permute-start(bf16[128,2048]{1,0:T(8,128)(2,1)} %partial_sum.1), channel_id=1, source_target_pairs={{0,16},{2,18},{4,20},{6,22},{8,24},{10,26},{12,28},{14,30},{16,0},... | collective-permute-start | bytes 1572872 | tf_op jit(solution)/shard_map/ppermute | solution.py:420
  155.0 12.9 %all-to-all-done.4 = bf16[8,32,2048]{2,1,0:T(8,128)(2,1)S(1)} async-done(((bf16[8,32,2048]{2,1,0:T(8,128)(2,1)}), bf16[8,32,2048]{2,1,0:T(8,128)(2,1)S(1)}, u32[]{:S(2)}, u32[]{:S(2)}) %all-to-all-start.4) | async-done | bytes 1048608 | tf_op jit(solution)/shard_map/all_to_all | solution.py:409
  167.9 9.2 %collective-permute-done.8.far_ref = bf16[128,2048]{1,0:T(8,128)(2,1)S(1)} collective-permute-done((bf16[128,2048]{1,0:T(8,128)(2,1)}, bf16[128,2048]{1,0:T(8,128)(2,1)S(1)}, u32[]{:S(2)}, u32[]{:S(2)}) %collective-permute-start.8) | collective-permute-done | bytes 524320 | tf_op jit(solution)/shard_map/ppermute | solution.py:420
  177.9 3.0 %final_sum.1 = bf16[128,2048]{1,0:T(8,128)(2,1)} custom-call(f32[8,128]{1,0:T(8,128)} %get-tuple-element.22.meta_ref, bf16[256,2048]{1,0:T(8,128)(2,1)} %bitcast.22, bf16[128,2048]{1,0:T(8,128)(2,1)} %get-tuple-element.14.mixed_ref, bf16[128,2048]{1,0:T(8,128)(2,1)} %copy-done.11), custom_call_target="tpu_custom_call" | custom-call | flops 1000000000 | bytes 3000000 | tf_op jit(solution)/shard_map/final_sum/pallas_call | solution.py:316
  (59 shorter events, 12.9 us)
Async XLA Ops:
  0.0 26.9 %copy-start.7 = (s32[128,2]{0,1:T(2,128)S(1)}, s32[128,2]{0,1:T(2,128)}, u32[]{:S(2)}) copy-start(s32[128,2]{0,1:T(2,128)} %param.24) | copy-start | bytes 3076
  0.0 26.2 %copy-start.15 = (f32[4]{0:T(128)S(1)}, f32[4]{0:T(128)}, u32[]{:S(2)}) copy-start(f32[4]{0:T(128)} %param.17) | copy-start | bytes 52
  0.0 31.4 %copy-start.9 = (bf16[128,2048]{1,0:T(8,128)(2,1)S(1)}, bf16[128,2048]{1,0:T(8,128)(2,1)}, u32[]{:S(2)}) copy-start(bf16[128,2048]{1,0:T(8,128)(2,1)} %residual_ref.1) | copy-start | bytes 1572868
  3.5 12.0 %all-to-all-start.1 = ((bf16[4,272,256]{2,1,0:T(8,128)(2,1)}), bf16[4,272,256]{2,1,0:T(8,128)(2,1)S(1)}, u32[]{:S(2)}, u32[]{:S(2)}) async-start(bf16[4,272,256]{2,1,0:T(8,128)(2,1)} %get-tuple-element.12), calls=%async_computation.1 | async-start | bytes 1114112 | tf_op jit(solution)/shard_map/all_to_all | solution.py:375
  7.7 105.2 %collective-permute-start.2 = (bf16[2048,1024]{1,0:T(8,128)(2,1)}, bf16[2048,1024]{1,0:T(8,128)(2,1)}, u32[]{:S(2)}, u32[]{:S(2)}) collective-permute-start(bf16[2048,1024]{1,0:T(8,128)(2,1)} %bitcast.29), channel_id=1, source_target_pairs={{0,1},{1,0},{2,3},{3,2},{4,5},{5,4},{6,7},{7,6},{8,9},{9,8},{10,11... | collective-permute-start | bytes 12582920 | tf_op jit(solution)/shard_map/ppermute | solution.py:393
  7.7 105.2 %collective-permute-start.3 = (bf16[2048,1024]{1,0:T(8,128)(2,1)}, bf16[2048,1024]{1,0:T(8,128)(2,1)}, u32[]{:S(2)}, u32[]{:S(2)}) collective-permute-start(bf16[2048,1024]{1,0:T(8,128)(2,1)} %bitcast.32), channel_id=1, source_target_pairs={{0,1},{1,0},{2,3},{3,2},{4,5},{5,4},{6,7},{7,6},{8,9},{9,8},{10,11... | collective-permute-start | bytes 12582920 | tf_op jit(solution)/shard_map/ppermute | solution.py:393
  8.2 104.7 %collective-permute-start.4 = (bf16[1024,2048]{1,0:T(8,128)(2,1)}, bf16[1024,2048]{1,0:T(8,128)(2,1)}, u32[]{:S(2)}, u32[]{:S(2)}) collective-permute-start(bf16[1024,2048]{1,0:T(8,128)(2,1)} %bitcast.35), channel_id=1, source_target_pairs={{0,1},{1,0},{2,3},{3,2},{4,5},{5,4},{6,7},{7,6},{8,9},{9,8},{10,11... | collective-permute-start | bytes 12582920 | tf_op jit(solution)/shard_map/ppermute | solution.py:393
  15.5 33.2 %copy-start = (bf16[4,272,256]{2,1,0:T(8,128)(2,1)}, bf16[4,272,256]{2,1,0:T(8,128)(2,1)S(1)}, u32[]{:S(2)}) copy-start(bf16[4,272,256]{2,1,0:T(8,128)(2,1)S(1)} %all-to-all-done.1.own_ref) | copy-start | bytes 1671172
  15.5 18.5 %all-to-all-start = ((bf16[4,256,128]{2,1,0:T(8,128)(2,1)}), bf16[4,256,128]{2,1,0:T(8,128)(2,1)S(1)}, u32[]{:S(2)}, u32[]{:S(2)}) async-start(bf16[4,256,128]{2,1,0:T(8,128)(2,1)} %get-tuple-element.11), calls=%async_computation | async-start | bytes 524288 | tf_op jit(solution)/shard_map/all_to_all | solution.py:382
  19.5 11.9 %collective-permute-start = (bf16[3,272,256]{2,1,0:T(8,128)(2,1)S(1)}, bf16[3,272,256]{2,1,0:T(8,128)(2,1)S(1)}, u32[]{:S(2)}, u32[]{:S(2)}) collective-permute-start(bf16[3,272,256]{2,1,0:T(8,128)(2,1)S(1)} %get-tuple-element.18), channel_id=1, source_target_pairs={{0,8},{2,10},{4,12},{6,14},{8,16},{10,18},{12,20},{14,22},{16,24},... | collective-permute-start | bytes 1253384 | tf_op jit(solution)/shard_map/ppermute | solution.py:376
  23.0 25.7 %collective-permute-start.1 = (bf16[3,272,256]{2,1,0:T(8,128)(2,1)S(1)}, bf16[3,272,256]{2,1,0:T(8,128)(2,1)}, u32[]{:S(2)}, u32[]{:S(2)}) collective-permute-start(bf16[3,272,256]{2,1,0:T(8,128)(2,1)S(1)} %get-tuple-element.17), channel_id=1, source_target_pairs={{8,0},{10,2},{12,4},{14,6},{16,8},{18,10},{20,12},{22,14},{24,16},... | collective-permute-start | bytes 1253384 | tf_op jit(solution)/shard_map/ppermute | solution.py:379
  26.9 40.2 %copy-start.8 = (f32[128,2]{0,1:T(2,128)S(1)}, f32[128,2]{0,1:T(2,128)}, u32[]{:S(2)}) copy-start(f32[128,2]{0,1:T(2,128)} %param.25) | copy-start | bytes 3076
  31.4 17.3 %copy-start.12 = (bf16[3,272,256]{2,1,0:T(8,128)(2,1)}, bf16[3,272,256]{2,1,0:T(8,128)(2,1)S(1)}, u32[]{:S(2)}) copy-start(bf16[3,272,256]{2,1,0:T(8,128)(2,1)S(1)} %collective-permute-done.prev_ref) | copy-start | bytes 1253380
  31.5 41.1 %collective-permute-start.7 = (bf16[128,2048]{1,0:T(8,128)(2,1)S(1)}, bf16[128,2048]{1,0:T(8,128)(2,1)S(1)}, u32[]{:S(2)}, u32[]{:S(2)}) collective-permute-start(bf16[128,2048]{1,0:T(8,128)(2,1)S(1)} %copy-done.9), channel_id=1, source_target_pairs={{0,16},{2,18},{4,20},{6,22},{8,24},{10,26},{12,28},{14,30},{16,0},... | collective-permute-start | bytes 1572872 | tf_op jit(solution)/shard_map/ppermute | solution.py:390
  34.0 14.7 %copy-start.5 = (bf16[4,256,128]{2,1,0:T(8,128)(2,1)}, bf16[4,256,128]{2,1,0:T(8,128)(2,1)S(1)}, u32[]{:S(2)}) copy-start(bf16[4,256,128]{2,1,0:T(8,128)(2,1)S(1)} %all-to-all-done.q_ref) | copy-start | bytes 786436
  62.9 9.6 %all-to-all-start.2 = ((bf16[8,128,128]{2,1,0:T(8,128)(2,1)}), bf16[8,128,128]{2,1,0:T(8,128)(2,1)S(1)}, u32[]{:S(2)}, u32[]{:S(2)}) async-start(bf16[8,128,128]{2,1,0:T(8,128)(2,1)} %bitcast.27), calls=%async_computation.2 | async-start | bytes 524288 | tf_op jit(solution)/shard_map/all_to_all | solution.py:399
  67.8 4.6 %collective-permute-start.5 = (f32[8,128]{1,0:T(8,128)S(1)}, f32[8,128]{1,0:T(8,128)S(1)}, u32[]{:S(2)}, u32[]{:S(2)}) collective-permute-start(f32[8,128]{1,0:T(8,128)S(1)} %get-tuple-element.21), channel_id=1, source_target_pairs={{0,16},{2,18},{4,20},{6,22},{8,24},{10,26},{12,28},{14,30},{16,0},... | collective-permute-start | bytes 12296 | tf_op jit(solution)/shard_map/ppermute | solution.py:388
  72.5 17.2 %copy-start.6 = (bf16[8,128,128]{2,1,0:T(8,128)(2,1)}, bf16[8,128,128]{2,1,0:T(8,128)(2,1)S(1)}, u32[]{:S(2)}) copy-start(bf16[8,128,128]{2,1,0:T(8,128)(2,1)S(1)} %all-to-all-done.2.heads_ref) | copy-start | bytes 786436
  72.5 10.9 %collective-permute-start.6 = (bf16[8,128,128]{2,1,0:T(8,128)(2,1)S(1)}, bf16[8,128,128]{2,1,0:T(8,128)(2,1)S(1)}, u32[]{:S(2)}, u32[]{:S(2)}) collective-permute-start(bf16[8,128,128]{2,1,0:T(8,128)(2,1)S(1)} %all-to-all-done.2.heads_ref), channel_id=1, source_target_pairs={{0,16},{2,18},{4,20},{6,22},{8,24},{10,26},{12,28},{14,30},{16,0},... | collective-permute-start | bytes 786440 | tf_op jit(solution)/shard_map/ppermute | solution.py:402
  89.7 18.0 %all-to-all-start.5 = ((bf16[8,32,2048]{2,1,0:T(8,128)(2,1)}), bf16[8,32,2048]{2,1,0:T(8,128)(2,1)S(1)}, u32[]{:S(2)}, u32[]{:S(2)}) async-start(bf16[8,32,2048]{2,1,0:T(8,128)(2,1)} %bitcast.26), calls=%async_computation.5 | async-start | bytes 2097152 | tf_op jit(solution)/shard_map/all_to_all | solution.py:409
  107.7 17.9 %all-to-all-start.3 = ((bf16[8,32,2048]{2,1,0:T(8,128)(2,1)}), bf16[8,32,2048]{2,1,0:T(8,128)(2,1)S(1)}, u32[]{:S(2)}, u32[]{:S(2)}) async-start(bf16[8,32,2048]{2,1,0:T(8,128)(2,1)} %bitcast.21), calls=%async_computation.3 | async-start | bytes 2097152 | tf_op jit(solution)/shard_map/all_to_all | solution.py:409
  125.6 17.7 %all-to-all-start.6 = ((bf16[8,32,2048]{2,1,0:T(8,128)(2,1)}), bf16[8,32,2048]{2,1,0:T(8,128)(2,1)S(1)}, u32[]{:S(2)}, u32[]{:S(2)}) async-start(bf16[8,32,2048]{2,1,0:T(8,128)(2,1)} %bitcast.25), calls=%async_computation.6 | async-start | bytes 2097152 | tf_op jit(solution)/shard_map/all_to_all | solution.py:409
  143.4 24.6 %all-to-all-start.4 = ((bf16[8,32,2048]{2,1,0:T(8,128)(2,1)}), bf16[8,32,2048]{2,1,0:T(8,128)(2,1)S(1)}, u32[]{:S(2)}, u32[]{:S(2)}) async-start(bf16[8,32,2048]{2,1,0:T(8,128)(2,1)} %bitcast.24), calls=%async_computation.4 | async-start | bytes 2097152 | tf_op jit(solution)/shard_map/all_to_all | solution.py:409
  151.0 26.1 %collective-permute-start.8 = (bf16[128,2048]{1,0:T(8,128)(2,1)}, bf16[128,2048]{1,0:T(8,128)(2,1)S(1)}, u32[]{:S(2)}, u32[]{:S(2)}) collective-permute-start(bf16[128,2048]{1,0:T(8,128)(2,1)} %partial_sum.1), channel_id=1, source_target_pairs={{0,16},{2,18},{4,20},{6,22},{8,24},{10,26},{12,28},{14,30},{16,0},... | collective-permute-start | bytes 1572872 | tf_op jit(solution)/shard_map/ppermute | solution.py:420
  (8 other events, 48.1 us)

commit v2 on v1

v2 whole, which is shorter than its diff:
```python
import functools

import jax
import jax.numpy as jnp
from jax import lax
from jax.experimental import pallas as pl
from jax.experimental.pallas import tpu as pltpu
from jax.sharding import PartitionSpec as P


HD = 64
REACH = 3
EPS = 1e-06
BF = jnp.bfloat16
F32 = jnp.float32
VM = pl.BlockSpec(memory_space=pltpu.VMEM)
SM = pl.BlockSpec(memory_space=pltpu.SMEM)
ANY = pl.BlockSpec(memory_space=pl.ANY)


def params(mebibytes):
    return pltpu.CompilerParams(vmem_limit_bytes=mebibytes * 1024 * 1024)


def cost(flops, bytes_accessed):
    return pl.CostEstimate(flops=flops, bytes_accessed=bytes_accessed, transcendentals=0)


def pack_kernel(q_ref, k_ref, v_ref, id_ref, o_ref):
    length, width = k_ref.shape
    part = length // 2
    scaled = (q_ref[...].astype(F32) * (HD**-0.5)).astype(BF)
    o_ref[0, :length, :width] = k_ref[...]
    o_ref[0, :length, width:] = v_ref[...]
    o_ref[0, length : length + 16, :] = id_ref[...]
    o_ref[0, length + 16 :, :width] = scaled[:part]
    o_ref[0, length + 16 :, width:] = scaled[part:]


def pack(query_rows, key_rows, value_rows, id_rows, heads):
    length = query_rows.shape[0]
    width = query_rows.shape[1] // heads
    rows = length + 16 + length // 2
    columns = pl.BlockSpec((length, width), lambda h: (0, h))
    return pl.pallas_call(
        pack_kernel,
        grid=(heads,),
        in_specs=[columns] * 3 + [pl.BlockSpec(id_rows.shape, lambda h: (0, 0))],
        out_specs=pl.BlockSpec((1, rows, 2 * width), lambda h: (h, 0, 0)),
        out_shape=jax.ShapeDtypeStruct((heads, rows, 2 * width), BF),
        compiler_params=params(8),
        name="pack",
    )(query_rows, key_rows, value_rows, id_rows)


def attention_kernel(
    lam_ref, prev_ref, own_ref, next_ref, o_ref, k_ref, v_ref, line_ref, id_ref
):
    b = pl.program_id(0)
    length, width = o_ref.shape[1:]
    before, group, after = prev_ref.shape[0], own_ref.shape[0], next_ref.shape[0]
    span = before + 1 + after
    blocks = before + group + after

    @pl.when(b == 0)
    def _():
        id_ref[...] = jnp.zeros_like(id_ref)
        for first, ref in ((0, prev_ref), (before, own_ref), (before + group, next_ref)):
            for i in range(ref.shape[0]):
                rows = slice((first + i) * length, (first + i + 1) * length)
                k_ref[rows, :] = ref[i, :length, :width]
                v_ref[rows, :width] = ref[i, :length, width:]
                named = ref[i, length : length + 16, :].astype(F32)[:1]
                id_ref[first + i : first + i + 1, :] = named
                line_ref[0:1, rows] = named
        v_ref[:, width:] = jnp.ones((v_ref.shape[0], width), BF)
        k_ref[blocks * length :, :] = jnp.zeros((length, width), BF)
        v_ref[blocks * length :, :width] = jnp.zeros((length, width), BF)
        line_ref[0:1, blocks * length :] = jnp.zeros((1, length), F32)

    query_ids = id_ref[pl.ds(b + before, 1), :]
    low = jnp.min(query_ids, axis=1, keepdims=True)
    high = jnp.max(query_ids, axis=1, keepdims=True)
    ids = id_ref[...]
    smallest = jnp.min(ids, axis=1, keepdims=True)
    largest = jnp.max(ids, axis=1, keepdims=True)
    place = lax.broadcasted_iota(jnp.int32, smallest.shape, 0) - b
    apart = (largest < low) | (smallest > high)
    left = jnp.sum(jnp.where(apart & (place >= 0) & (place < before), 1.0, 0.0))
    right = jnp.sum(jnp.where(apart & (place > before) & (place < span), 1.0, 0.0))
    left = left.astype(jnp.int32)
    pairs = (span + 1 - right.astype(jnp.int32) - left) // 2
    start = pl.multiple_of((b + left) * length, length)
    query_column = jnp.transpose(jnp.broadcast_to(query_ids, (128, length)))
    lam = lam_ref[0]

    def attend(keys):
        named = line_ref[0:1, pl.ds(start, keys)]
        for chunk in range(length // 128):
            mine = query_column[chunk * 128 : (chunk + 1) * 128, :]
            q = own_ref[
                b,
                length + 16 + (chunk * 128) % (length // 2) : length
                + 16
                + (chunk * 128) % (length // 2)
                + 128,
                (chunk * 128 // (length // 2)) * width : (chunk * 128 // (length // 2) + 1) * width,
            ]
            zero = jnp.zeros((128, HD), BF)
            sides = (
                jnp.concatenate([q[:, :HD], zero], axis=1),
                jnp.concatenate([zero, q[:, HD:]], axis=1),
            )
            maps = []
            for side in sides:
                scores = lax.dot_general(
                    side,
                    k_ref[pl.ds(start, keys), :],
                    (((1,), (1,)), ((), ())),
                    preferred_element_type=F32,
                )
                pieces = []
                best = None
                for part in range(keys // 128):
                    columns = slice(part * 128, (part + 1) * 128)
                    piece = jnp.where(mine == named[:, columns], scores[:, columns], -1e30)
                    best = piece if best is None else jnp.maximum(best, piece)
                    pieces.append(piece)
                top = jnp.max(best, axis=1, keepdims=True)
                lifted = jnp.concatenate(
                    [jnp.exp(piece - top).astype(BF) for piece in pieces], axis=1
                )
                total = jnp.dot(
                    lifted, v_ref[pl.ds(start, keys), :], preferred_element_type=F32
                )
                maps.append(total[:, :width] / total[:, width:])
            out = maps[0] - lam * maps[1]
            scale = lax.rsqrt(jnp.mean(out * out, axis=1, keepdims=True) + EPS)
            o_ref[b, chunk * 128 : (chunk + 1) * 128, :] = (out * scale).astype(BF)

    for count in range(1, (span + 1) // 2 + 1):

        @pl.when(pairs == count)
        def _():
            attend(count * 2 * length)


def attention(lam, prev, own, following, length, width):
    group = own.shape[0]
    before, after = prev.shape[0], following.shape[0]
    blocks = before + group + after
    return pl.pallas_call(
        attention_kernel,
        grid=(group,),
        in_specs=[SM] + [VM] * 3,
        out_specs=VM,
        out_shape=jax.ShapeDtypeStruct((group, length, width), BF),
        scratch_shapes=[
            pltpu.VMEM(((blocks + 1) * length, width), BF),
            pltpu.VMEM(((blocks + 1) * length, 2 * width), BF),
            pltpu.VMEM((8, (blocks + 1) * length), F32),
            pltpu.VMEM((-(-(blocks + 1) // 8) * 8, length), F32),
        ],
        compiler_params=params(16),
        cost_estimate=cost(8 * 10**9, 4 * 10**6),
        name="attention",
    )(lam, prev, own, following)


def project_kernel(
    heads_ref, residual_ref, gain_ref, meta_ref, weight_ref, rows_ref, mixed_ref, left_ref, *, tile
):
    tokens, width = mixed_ref.shape
    members = heads_ref.shape[0]
    value_dim = heads_ref.shape[2]
    for source in range(members):
        head = (source % 2) * (members // 2) + source // 2
        left_ref[:, head * value_dim : (head + 1) * value_dim] = heads_ref[source]
    squares = jnp.zeros((tokens, 128), F32)
    for n in range(width // tile):
        columns = slice(n * tile, (n + 1) * tile)
        projected = jnp.dot(left_ref[...], weight_ref[:, columns], preferred_element_type=F32)
        mixed = (residual_ref[:, columns].astype(F32) + projected).astype(BF)
        mixed_ref[:, columns] = mixed
        wide = mixed.astype(F32)
        wide = wide * wide
        for part in range(tile // 128):
            squares = squares + wide[:, part * 128 : (part + 1) * 128]
    scale = lax.rsqrt(jnp.sum(squares, axis=1, keepdims=True) / width + EPS)
    slots = rows_ref.shape[0]
    place = lax.broadcasted_iota(jnp.int32, (slots, tokens), 0).astype(F32)
    pick = (place == meta_ref[0:1, :]) | (place == meta_ref[1:2, :])
    pick = jnp.where(pick, 1.0, 0.0).astype(BF)
    for n in range(width // tile):
        columns = slice(n * tile, (n + 1) * tile)
        normed = mixed_ref[:, columns].astype(F32) * scale * gain_ref[:, columns]
        rows_ref[:, columns] = jnp.dot(
            pick, normed.astype(BF), preferred_element_type=F32
        ).astype(BF)


def project(heads, residual, gain, meta, out_weight, slots, keep, tile=512):
    _, tokens, _ = heads.shape
    depth, width = out_weight.shape
    rows = jax.ShapeDtypeStruct((slots, width), BF)
    mixed = jax.ShapeDtypeStruct((tokens, width), BF)
    left = pltpu.VMEM((tokens, depth), BF)
    return pl.pallas_call(
        functools.partial(project_kernel, tile=tile),
        in_specs=[VM] * 5,
        out_specs=[VM, VM] if keep else VM,
        out_shape=[rows, mixed] if keep else rows,
        scratch_shapes=[left] if keep else [pltpu.VMEM((tokens, width), BF), left],
        compiler_params=params(16),
        cost_estimate=cost(3 * 10**9, 8 * 10**6),
    )(heads, residual, gain, meta, out_weight)


def expert_kernel(
    x_ref, g0, u0, d0, g1, u1, d1, y_ref, gb, ub, db, hidden_ref, half_ref, sems, *, tile
):
    steps = g0.shape[1] // tile
    width = y_ref.shape[1]
    arrivals = []
    for step in range(steps):
        at = pl.ds(step * tile, tile)
        arrivals.append(
            (
                pltpu.make_async_copy(g1.at[:, at], gb.at[:, at], sems.at[step]),
                pltpu.make_async_copy(u1.at[:, at], ub.at[:, at], sems.at[steps + step]),
            )
        )
    last = [
        pltpu.make_async_copy(
            d1.at[pl.ds(n * tile, tile)], db.at[pl.ds(n * tile, tile)], sems.at[2 * steps + n]
        )
        for n in range(steps)
    ]
    for pair in arrivals:
        for copy in pair:
            copy.start()
    for copy in last:
        copy.start()
    for h, (g, u, d) in enumerate(((g0, u0, d0), (gb, ub, db))):
        for step in range(steps):
            at = slice(step * tile, (step + 1) * tile)
            if h:
                for copy in arrivals[step]:
                    copy.wait()
            gate = jnp.dot(x_ref[...], g[:, at], preferred_element_type=F32)
            upward = jnp.dot(x_ref[...], u[:, at], preferred_element_type=F32)
            hidden_ref[:, at] = (gate / (1.0 + jnp.exp(-gate)) * upward).astype(BF)
        if h:
            for copy in last:
                copy.wait()
        for n in range(width // tile):
            at = slice(n * tile, (n + 1) * tile)
            part = jnp.dot(hidden_ref[...], d[:, at], preferred_element_type=F32).astype(BF)
            if h:
                y_ref[:, at] = (half_ref[:, at].astype(F32) + part.astype(F32)).astype(BF)
            else:
                half_ref[:, at] = part


def experts_of(x, own, other, tile=256):
    rows, width = x.shape
    depth = own[0].shape[1]
    return pl.pallas_call(
        functools.partial(expert_kernel, tile=tile),
        in_specs=[VM] * 4 + [ANY] * 3,
        out_specs=VM,
        out_shape=jax.ShapeDtypeStruct((rows, width), BF),
        scratch_shapes=[
            pltpu.VMEM((width, depth), BF),
            pltpu.VMEM((width, depth), BF),
            pltpu.VMEM((depth, width), BF),
            pltpu.VMEM((rows, depth), BF),
            pltpu.VMEM((rows, width), BF),
            pltpu.SemaphoreType.DMA((3 * (depth // tile),)),
        ],
        compiler_params=params(34),
        cost_estimate=cost(9 * 10**9, 26 * 10**6),
    )(x, *own, *other)


def picked(meta_ref, rows_ref, write, tile=512):
    slots, width = rows_ref.shape
    tokens = meta_ref.shape[1]
    columns = jnp.transpose(meta_ref[...])
    place = lax.broadcasted_iota(jnp.int32, (tokens, slots), 1).astype(F32)
    picks = jnp.concatenate(
        [jnp.where(place == columns[:, k : k + 1], 1.0, 0.0) for k in range(2)], axis=0
    ).astype(BF)
    for n in range(width // tile):
        at = slice(n * tile, (n + 1) * tile)
        rows = jnp.dot(picks, rows_ref[:, at], preferred_element_type=F32)
        write(at, rows[:tokens] * columns[:, 2:3] + rows[tokens:] * columns[:, 3:4])


def partial_kernel(meta_ref, rows_ref, o_ref):
    def write(at, total):
        o_ref[:, at] = total.astype(BF)

    picked(meta_ref, rows_ref, write)


def final_kernel(meta_ref, rows_ref, mixed_ref, far_ref, o_ref):
    def write(at, total):
        total = total + far_ref[:, at].astype(F32)
        o_ref[:, at] = (mixed_ref[:, at].astype(F32) + total).astype(BF)

    picked(meta_ref, rows_ref, write)


def partial_sum(meta, rows):
    return pl.pallas_call(
        partial_kernel,
        in_specs=[VM] * 2,
        out_specs=VM,
        out_shape=jax.ShapeDtypeStruct((meta.shape[1], rows.shape[1]), BF),
        compiler_params=params(12),
        cost_estimate=cost(10**9, 2 * 10**6),
        name="partial_sum",
    )(meta, rows)


def final_sum(meta, rows, mixed, far):
    return pl.pallas_call(
        final_kernel,
        in_specs=[VM] * 4,
        out_specs=VM,
        out_shape=jax.ShapeDtypeStruct(mixed.shape, BF),
        compiler_params=params(12),
        cost_estimate=cost(10**9, 3 * 10**6),
        name="final_sum",
    )(meta, rows, mixed, far)


def ranks_of(routes, experts):
    tokens = routes.shape[0]
    table = (routes[:, :, None] == jnp.arange(experts, dtype=jnp.int32)).astype(F32)
    named = jnp.sum(table, axis=1)
    order = jnp.arange(tokens)
    below = (order[:, None] > order[None, :]).astype(BF)
    earlier = jnp.dot(below, named.astype(BF), preferred_element_type=F32)
    return jnp.sum(earlier[:, None, :] * table, axis=2)


def meta_of(routes, ranks, route_weights, first, count, capacity):
    local = routes - first
    inside = (local >= 0) & (local < count)
    target = jnp.where(inside, local.astype(F32) * capacity + ranks, -1.0)
    rows = jnp.concatenate([target.T, route_weights.T], axis=0)
    return jnp.concatenate([rows, jnp.zeros((8 - rows.shape[0], rows.shape[1]), F32)], axis=0)


def on_device(
    residual,
    query_rows,
    key_rows,
    value_rows,
    mix_lambda,
    documents,
    out_weight,
    norm_gain,
    gate_weight,
    up_weight,
    down_weight,
    routes,
    route_weights,
):
    length = query_rows.shape[0]
    heads = mix_lambda.shape[0]
    width = residual.shape[1]
    count = lax.axis_size("sp")
    twins = lax.axis_size("tp")
    here = lax.axis_index("sp")
    half = count // 2
    capacity = 2 * length // count
    planes = [[g * heads + j for j in range(heads)] for g in range(count // heads)]
    halves = [[h * half + j for j in range(half)] for h in range(2)]
    mirror = [(i, (i + half) % count) for i in range(count)]
    swap = [(i, twins - 1 - i) for i in range(twins)]

    value_dim = value_rows.shape[1] // heads
    id_rows = jnp.broadcast_to((documents + 1).astype(BF)[None, :], (16, length))
    packed = pack(query_rows, key_rows, value_rows, id_rows, heads)
    packed = lax.all_to_all(packed, "sp", 0, 0, tiled=True, axis_index_groups=planes)
    pairs = packed[:, : length + 16]
    prev = lax.ppermute(
        pairs[heads - REACH :], "sp", [(i, i + heads) for i in range(count - heads)]
    )
    following = lax.ppermute(pairs[:REACH], "sp", [(i + heads, i) for i in range(count - heads)])

    ranks = ranks_of(routes, count)
    my_half = here // half
    meta_own = meta_of(routes, ranks, route_weights, my_half * half, half, capacity)
    meta_far = meta_of(routes, ranks, route_weights, (1 - my_half) * half, half, capacity)
    meta_far = lax.ppermute(meta_far, "sp", mirror)
    prev, following, residual_late = lax.optimization_barrier((prev, following, residual))
    residual_far = lax.ppermute(residual_late, "sp", mirror)

    own = (gate_weight[0], up_weight[0], down_weight[0])
    other = tuple(lax.ppermute(weight, "tp", swap) for weight in own)

    lam = lax.dynamic_slice(mix_lambda, (here % heads,), (1,))
    outs = attention(lam, prev, packed, following, length, value_dim)
    outs = outs.reshape(heads * twins, length // twins, value_dim)
    both = [[g * heads * twins + j for j in range(heads * twins)] for g in range(count // heads)]
    token_heads = lax.all_to_all(
        outs, ("sp", "tp"), 0, 0, tiled=True, axis_index_groups=both
    )
    heads_far = lax.ppermute(token_heads, "sp", mirror)

    gain = norm_gain.reshape(1, width)
    slots = half * capacity

    def exchange(rows):
        rows = rows.reshape(half, capacity, width)
        rows = lax.all_to_all(rows, "sp", 0, 0, tiled=True, axis_index_groups=halves)
        return rows.reshape(slots, width)

    rows_own, mixed = project(token_heads, residual, gain, meta_own, out_weight, slots, True)
    rows_own = exchange(rows_own)
    rows_far = project(heads_far, residual_far, gain, meta_far, out_weight, slots, False)
    rows_far = exchange(rows_far)
    answer_own = experts_of(rows_own, own, other)
    answer_far = experts_of(rows_far, own, other)
    back_far = exchange(answer_far)
    part_far = partial_sum(meta_far, back_far)
    part = lax.ppermute(part_far, "sp", mirror)
    back_own = exchange(answer_own)
    return final_sum(meta_own, back_own, mixed, part)


def solution(mesh):
    placed = (
        P(("sp", "tp"), None),
        P("sp", "tp"),
        P("sp", "tp"),
        P("sp", "tp"),
        P("tp"),
        P("sp"),
        P(),
        P(),
        P("sp", None, "tp"),
        P("sp", None, "tp"),
        P("sp", "tp", None),
        P(("sp", "tp"), None),
        P(("sp", "tp"), None),
    )
    return jax.shard_map(
        on_device, mesh=mesh, in_specs=placed, out_specs=P(("sp", "tp"), None), check_vma=False
    )
```

time: 184 us -> 187 us (1.016)
  Pallas kernels: 58.3 us -> 37 us
  local copies, waits for them, and re-layouts: 2.92 us -> 23.7 us
  waiting for transfers between devices: 70.8 us -> 77.9 us
    unnamed x32 -> x34, local copies, waits for them, and re-layouts: 1.54 us -> 22.2 us
    pallas_call x6, Pallas kernels: 52.7 us -> 35 us  [the longest x2 20.8 us: experts_of(): pl.pallas_call(functools.partial(expert_kernel, tile=tile), in_specs=[VM]...]
    ppermute x1, waiting for transfers between devices: 4.61 us -> 20.1 us  [on_device(): meta_far = lax.ppermute(meta_far, 'sp', mirror)]
    ppermute x1, waiting for transfers between devices: 14.7 us -> 3.21 us  [on_device(): lax.ppermute(pairs[:REACH], 'sp', [(i + heads, i) for i in range(count -...]
    all_to_all x4, waiting for transfers between devices: 19.5 us -> 26.4 us  [exchange(): lax.all_to_all(rows, 'sp', 0, 0, tiled=True, axis_index_groups=halves)]
    ppermute x1, waiting for transfers between devices: 9.18 us -> 2.75 us  [on_device(): part = lax.ppermute(part_far, 'sp', mirror)]
    all_to_all x2 -> x1, starting transfers between devices: 8.15 us -> 4.22 us  [on_device(): lax.all_to_all(packed, 'sp', 0, 0, tiled=True, axis_index_groups=planes)]
    ppermute x1, starting transfers between devices: 0.01 us -> 3.38 us  [on_device(): heads_far = lax.ppermute(token_heads, 'sp', mirror)]
  transfers between devices with their start and end apart: 16 -> 15, of which waited for: 9 -> 8; matrix products, arithmetic and copies ran while one was open for 1% -> 1% of each run, Pallas kernels for 29% -> 18%
where the time goes in v2:
time: 187 us; the launch traced here: 185 us
  waiting for transfers between devices  77.9 us (42%)
  starting transfers between devices  44.9 us (24%)
  Pallas kernels  37 us (20%)
  local copies, waits for them, and re-layouts  23.7 us (13%)
    all_to_all x4, waiting for transfers between devices, exchange(): lax.all_to_all(rows, 'sp', 0, 0, tiled=True, axis_index_groups=halves)  26.4 us
    unnamed x34, local copies, waits for them, and re-layouts  22.2 us
    all_to_all x4, starting transfers between devices, exchange(): lax.all_to_all(rows, 'sp', 0, 0, tiled=True, axis_index_groups=halves)  21.4 us
    pallas_call x2, Pallas kernels, experts_of(): pl.pallas_call(functools.partial(expert_kernel, tile=tile), in_specs=[VM]...  20.8 us
    ppermute x1, waiting for transfers between devices, on_device(): meta_far = lax.ppermute(meta_far, 'sp', mirror)  20.1 us
    ppermute x1, waiting for transfers between devices, on_device(): heads_far = lax.ppermute(token_heads, 'sp', mirror)  10.5 us
    all_to_all x1, waiting for transfers between devices, on_device(): lax.all_to_all(packed, 'sp', 0, 0, tiled=True, axis_index_groups=planes)  8.82 us
    pallas_call x1, Pallas kernels, attention(): pl.pallas_call(attention_kernel, grid=(group,), in_specs=[SM] + [VM] * 3,...  7.86 us
  transfers between devices with their start and end apart: 15, of which 8 were waited for; matrix products, arithmetic and copies ran while one was open for 1% of the time, Pallas kernels for 18%

profile of v2, /device:TPU:12, one launch (start us, length us, event | category | flops | bytes accessed | tf_op | source)
XLA Modules:
  0.0 184.6 jit_solution(1712881060302107600)
XLA Ops:
  5.2 4.2 %all-to-all-start = ((bf16[4,400,256]{2,1,0:T(8,128)(2,1)}), bf16[4,400,256]{2,1,0:T(8,128)(2,1)S(1)}, u32[]{:S(2)}, u32[]{:S(2)}) async-start(bf16[4,400,256]{2,1,0:T(8,128)(2,1)} %pack.1), calls=%async_computation | async-start | bytes 1638400 | tf_op jit(solution)/shard_map/all_to_all | solution.py:388
  11.3 8.8 %all-to-all-done.own_ref = bf16[4,400,256]{2,1,0:T(8,128)(2,1)S(1)} async-done(((bf16[4,400,256]{2,1,0:T(8,128)(2,1)}), bf16[4,400,256]{2,1,0:T(8,128)(2,1)S(1)}, u32[]{:S(2)}, u32[]{:S(2)}) %all-to-all-start) | async-done | bytes 819232 | tf_op jit(solution)/shard_map/all_to_all | solution.py:388
  20.1 3.5 %collective-permute-start = (bf16[3,272,256]{2,1,0:T(8,128)(2,1)S(1)}, bf16[3,272,256]{2,1,0:T(8,128)(2,1)S(1)}, u32[]{:S(2)}, u32[]{:S(2)}) collective-permute-start(bf16[3,272,256]{2,1,0:T(8,128)(2,1)S(1)} %get-tuple-element.16), channel_id=1, source_target_pairs={{0,8},{2,10},{4,12},{6,14},{8,16},{10,18},{12,20},{14,22},{16,24},... | collective-permute-start | bytes 1253384 | tf_op jit(solution)/shard_map/ppermute | solution.py:390
  23.6 2.4 %collective-permute-start.1 = (bf16[3,272,256]{2,1,0:T(8,128)(2,1)S(1)}, bf16[3,272,256]{2,1,0:T(8,128)(2,1)S(1)}, u32[]{:S(2)}, u32[]{:S(2)}) collective-permute-start(bf16[3,272,256]{2,1,0:T(8,128)(2,1)S(1)} %get-tuple-element.15), channel_id=1, source_target_pairs={{8,0},{10,2},{12,4},{14,6},{16,8},{18,10},{20,12},{22,14},{24,16},... | collective-permute-start | bytes 1253384 | tf_op jit(solution)/shard_map/ppermute | solution.py:393
  26.3 6.1 %collective-permute-done.prev_ref = bf16[3,272,256]{2,1,0:T(8,128)(2,1)S(1)} collective-permute-done((bf16[3,272,256]{2,1,0:T(8,128)(2,1)S(1)}, bf16[3,272,256]{2,1,0:T(8,128)(2,1)S(1)}, u32[]{:S(2)}, u32[]{:S(2)}) %collective-permute-start) | collective-permute-done | bytes 417824 | tf_op jit(solution)/shard_map/ppermute | solution.py:390
  32.4 3.2 %collective-permute-done.1.next_ref = bf16[3,272,256]{2,1,0:T(8,128)(2,1)S(1)} collective-permute-done((bf16[3,272,256]{2,1,0:T(8,128)(2,1)S(1)}, bf16[3,272,256]{2,1,0:T(8,128)(2,1)S(1)}, u32[]{:S(2)}, u32[]{:S(2)}) %collective-permute-start.1) | collective-permute-done | bytes 417824 | tf_op jit(solution)/shard_map/ppermute | solution.py:393
  35.6 7.9 %attention.1 = bf16[4,256,128]{2,1,0:T(8,128)(2,1)} custom-call(f32[1]{0:T(128)} %dynamic_slice.3.lam_ref, bf16[3,272,256]{2,1,0:T(8,128)(2,1)S(1)} %collective-permute-done.prev_ref, bf16[4,400,256]{2,1,0:T(8,128)(2,1)S(1)} %all-to-all-done.own_ref, bf16[3,272,256]{2,1,0:T(8,128)(2,1)S(1)} %collective-permute-done.1.next_ref), custom_call_target="tpu_custom_call" | custom-call | flops 8000000000 | bytes 4000000 | tf_op jit(solution)/shard_map/attention/pallas_call | solution.py:152
  43.4 4.2 %all-to-all-start.1 = ((bf16[8,128,128]{2,1,0:T(8,128)(2,1)}), bf16[8,128,128]{2,1,0:T(8,128)(2,1)S(1)}, u32[]{:S(2)}, u32[]{:S(2)}) async-start(bf16[8,128,128]{2,1,0:T(8,128)(2,1)} %bitcast.2), calls=%async_computation.1 | async-start | bytes 524288 | tf_op jit(solution)/shard_map/all_to_all | solution.py:410
  47.9 2.8 %collective-permute-start.5 = (f32[8,128]{1,0:T(8,128)S(1)}, f32[8,128]{1,0:T(8,128)S(1)}, u32[]{:S(2)}, u32[]{:S(2)}) collective-permute-start(f32[8,128]{1,0:T(8,128)S(1)} %get-tuple-element.19), channel_id=1, source_target_pairs={{0,16},{2,18},{4,20},{6,22},{8,24},{10,26},{12,28},{14,30},{16,0},... | collective-permute-start | bytes 12296 | tf_op jit(solution)/shard_map/ppermute | solution.py:399
  50.7 20.1 %collective-permute-done.5.meta_ref = f32[8,128]{1,0:T(8,128)S(1)} collective-permute-done((f32[8,128]{1,0:T(8,128)S(1)}, f32[8,128]{1,0:T(8,128)S(1)}, u32[]{:S(2)}, u32[]{:S(2)}) %collective-permute-start.5) | collective-permute-done | bytes 4128 | tf_op jit(solution)/shard_map/ppermute | solution.py:399
  70.8 3.4 %collective-permute-start.6 = (bf16[8,128,128]{2,1,0:T(8,128)(2,1)S(1)}, bf16[8,128,128]{2,1,0:T(8,128)(2,1)S(1)}, u32[]{:S(2)}, u32[]{:S(2)}) collective-permute-start(bf16[8,128,128]{2,1,0:T(8,128)(2,1)S(1)} %all-to-all-done.1.heads_ref), channel_id=1, source_target_pairs={{0,16},{2,18},{4,20},{6,22},{8,24},{10,26},{12,28},{14,30},{16,0},... | collective-permute-start | bytes 786440 | tf_op jit(solution)/shard_map/ppermute | solution.py:413
  74.2 10.5 %collective-permute-done.6.heads_ref = bf16[8,128,128]{2,1,0:T(8,128)(2,1)S(1)} collective-permute-done((bf16[8,128,128]{2,1,0:T(8,128)(2,1)S(1)}, bf16[8,128,128]{2,1,0:T(8,128)(2,1)S(1)}, u32[]{:S(2)}, u32[]{:S(2)}) %collective-permute-start.6) | collective-permute-done | bytes 262176 | tf_op jit(solution)/shard_map/ppermute | solution.py:413
  86.9 2.3 %shard_map.129 = bf16[256,2048]{1,0:T(8,128)(2,1)} custom-call(bf16[8,128,128]{2,1,0:T(8,128)(2,1)S(1)} %collective-permute-done.6.heads_ref, bf16[128,2048]{1,0:T(8,128)(2,1)S(1)} %collective-permute-done.7.residual_ref, f32[1,2048]{1,0:T(1,128)S(1)} %bitcast.32, f32[8,128]{1,0:T(8,128)S(1)} %collective-permute-done.5.meta_ref, bf16[1024,2048]{1,0:T(8,128)(2,1)S(1)} %copy-done.3), custom_call_target="tpu_custom_call" | custom-call | flops 3000000000 | bytes 8000000 | tf_op jit(solution)/shard_map/pallas_call | solution.py:208
  89.2 6.1 %all-to-all-start.4 = ((bf16[8,32,2048]{2,1,0:T(8,128)(2,1)}), bf16[8,32,2048]{2,1,0:T(8,128)(2,1)S(1)}, u32[]{:S(2)}, u32[]{:S(2)}) async-start(bf16[8,32,2048]{2,1,0:T(8,128)(2,1)} %bitcast.12), calls=%async_computation.4 | async-start | bytes 2097152 | tf_op jit(solution)/shard_map/all_to_all | solution.py:420
  97.5 2.3 %shard_map.127 = (bf16[256,2048]{1,0:T(8,128)(2,1)}, bf16[128,2048]{1,0:T(8,128)(2,1)S(1)}) custom-call(bf16[8,128,128]{2,1,0:T(8,128)(2,1)S(1)} %all-to-all-done.1.heads_ref, bf16[128,2048]{1,0:T(8,128)(2,1)S(1)} %copy-done.11, f32[1,2048]{1,0:T(1,128)S(1)} %bitcast.33, f32[8,128]{1,0:T(8,128)S(1)} %get-tuple-element.20.meta_ref, ...), custom_call_target="tpu_custom_call" | custom-call | flops 3000000000 | bytes 8000000 | tf_op jit(solution)/shard_map/pallas_call | solution.py:208
  100.6 8.0 %all-to-all-done.4 = bf16[8,32,2048]{2,1,0:T(8,128)(2,1)S(1)} async-done(((bf16[8,32,2048]{2,1,0:T(8,128)(2,1)}), bf16[8,32,2048]{2,1,0:T(8,128)(2,1)S(1)}, u32[]{:S(2)}, u32[]{:S(2)}) %all-to-all-start.4) | async-done | bytes 1048608 | tf_op jit(solution)/shard_map/all_to_all | solution.py:420
  108.6 5.1 %all-to-all-start.2 = ((bf16[8,32,2048]{2,1,0:T(8,128)(2,1)}), bf16[8,32,2048]{2,1,0:T(8,128)(2,1)S(1)}, u32[]{:S(2)}, u32[]{:S(2)}) async-start(bf16[8,32,2048]{2,1,0:T(8,128)(2,1)} %bitcast.4), calls=%async_computation.2 | async-start | bytes 2097152 | tf_op jit(solution)/shard_map/all_to_all | solution.py:420
  120.3 10.4 %shard_map.130 = bf16[256,2048]{1,0:T(8,128)(2,1)} custom-call(bf16[256,2048]{1,0:T(8,128)(2,1)S(1)} %bitcast.19, bf16[2048,1024]{1,0:T(8,128)(2,1)S(1)} %bitcast.24, bf16[2048,1024]{1,0:T(8,128)(2,1)S(1)} %bitcast.27, bf16[1024,2048]{1,0:T(8,128)(2,1)S(1)} %bitcast.30, bf16[2048,1024]{1,0:T(8,128)(2,1)} %collective-permute-done.2.g1, ...), custom_call_target="tpu_custom_call" | custom-call | flops 8999999488 | bytes 26000000 | tf_op jit(solution)/shard_map/pallas_call | solution.py:268
  130.7 5.1 %all-to-all-start.5 = ((bf16[8,32,2048]{2,1,0:T(8,128)(2,1)}), bf16[8,32,2048]{2,1,0:T(8,128)(2,1)S(1)}, u32[]{:S(2)}, u32[]{:S(2)}) async-start(bf16[8,32,2048]{2,1,0:T(8,128)(2,1)} %bitcast.14), calls=%async_computation.5 | async-start | bytes 2097152 | tf_op jit(solution)/shard_map/all_to_all | solution.py:420
  142.4 10.4 %shard_map.128 = bf16[256,2048]{1,0:T(8,128)(2,1)} custom-call(bf16[256,2048]{1,0:T(8,128)(2,1)S(1)} %bitcast.20, bf16[2048,1024]{1,0:T(8,128)(2,1)S(1)} %bitcast.25, bf16[2048,1024]{1,0:T(8,128)(2,1)S(1)} %bitcast.28, bf16[1024,2048]{1,0:T(8,128)(2,1)S(1)} %bitcast.31, bf16[2048,1024]{1,0:T(8,128)(2,1)} %collective-permute-done.2.g1, ...), custom_call_target="tpu_custom_call" | custom-call | flops 8999999488 | bytes 26000000 | tf_op jit(solution)/shard_map/pallas_call | solution.py:268
  152.8 5.1 %all-to-all-start.3 = ((bf16[8,32,2048]{2,1,0:T(8,128)(2,1)}), bf16[8,32,2048]{2,1,0:T(8,128)(2,1)S(1)}, u32[]{:S(2)}, u32[]{:S(2)}) async-start(bf16[8,32,2048]{2,1,0:T(8,128)(2,1)} %bitcast.9), calls=%async_computation.3 | async-start | bytes 2097152 | tf_op jit(solution)/shard_map/all_to_all | solution.py:420
  158.5 2.4 %collective-permute-start.8 = (bf16[128,2048]{1,0:T(8,128)(2,1)S(1)}, bf16[128,2048]{1,0:T(8,128)(2,1)S(1)}, u32[]{:S(2)}, u32[]{:S(2)}) collective-permute-start(bf16[128,2048]{1,0:T(8,128)(2,1)S(1)} %partial_sum.1), channel_id=1, source_target_pairs={{0,16},{2,18},{4,20},{6,22},{8,24},{10,26},{12,28},{14,30},{16,0},... | collective-permute-start | bytes 1572872 | tf_op jit(solution)/shard_map/ppermute | solution.py:431
  160.9 18.4 %all-to-all-done.3 = bf16[8,32,2048]{2,1,0:T(8,128)(2,1)S(1)} async-done(((bf16[8,32,2048]{2,1,0:T(8,128)(2,1)}), bf16[8,32,2048]{2,1,0:T(8,128)(2,1)S(1)}, u32[]{:S(2)}, u32[]{:S(2)}) %all-to-all-start.3) | async-done | bytes 1048608 | tf_op jit(solution)/shard_map/all_to_all | solution.py:420
  179.3 2.8 %collective-permute-done.8.far_ref = bf16[128,2048]{1,0:T(8,128)(2,1)S(1)} collective-permute-done((bf16[128,2048]{1,0:T(8,128)(2,1)S(1)}, bf16[128,2048]{1,0:T(8,128)(2,1)S(1)}, u32[]{:S(2)}, u32[]{:S(2)}) %collective-permute-start.8) | collective-permute-done | bytes 524320 | tf_op jit(solution)/shard_map/ppermute | solution.py:431
  (59 shorter events, 28.9 us)
Async XLA Ops:
  0.0 26.0 %copy-start.15 = (s32[128,2]{0,1:T(2,128)S(1)}, s32[128,2]{0,1:T(2,128)}, u32[]{:S(2)}) copy-start(s32[128,2]{0,1:T(2,128)} %param.24) | copy-start | bytes 3076
  5.2 14.9 %all-to-all-start = ((bf16[4,400,256]{2,1,0:T(8,128)(2,1)}), bf16[4,400,256]{2,1,0:T(8,128)(2,1)S(1)}, u32[]{:S(2)}, u32[]{:S(2)}) async-start(bf16[4,400,256]{2,1,0:T(8,128)(2,1)} %pack.1), calls=%async_computation | async-start | bytes 1638400 | tf_op jit(solution)/shard_map/all_to_all | solution.py:388
  9.4 104.3 %collective-permute-start.2 = (bf16[2048,1024]{1,0:T(8,128)(2,1)}, bf16[2048,1024]{1,0:T(8,128)(2,1)}, u32[]{:S(2)}, u32[]{:S(2)}) collective-permute-start(bf16[2048,1024]{1,0:T(8,128)(2,1)} %bitcast.23), channel_id=1, source_target_pairs={{0,1},{1,0},{2,3},{3,2},{4,5},{5,4},{6,7},{7,6},{8,9},{9,8},{10,11... | collective-permute-start | bytes 12582920 | tf_op jit(solution)/shard_map/ppermute | solution.py:404
  9.4 104.3 %collective-permute-start.3 = (bf16[2048,1024]{1,0:T(8,128)(2,1)}, bf16[2048,1024]{1,0:T(8,128)(2,1)}, u32[]{:S(2)}, u32[]{:S(2)}) collective-permute-start(bf16[2048,1024]{1,0:T(8,128)(2,1)} %bitcast.26), channel_id=1, source_target_pairs={{0,1},{1,0},{2,3},{3,2},{4,5},{5,4},{6,7},{7,6},{8,9},{9,8},{10,11... | collective-permute-start | bytes 12582920 | tf_op jit(solution)/shard_map/ppermute | solution.py:404
  9.9 103.8 %collective-permute-start.4 = (bf16[1024,2048]{1,0:T(8,128)(2,1)}, bf16[1024,2048]{1,0:T(8,128)(2,1)}, u32[]{:S(2)}, u32[]{:S(2)}) collective-permute-start(bf16[1024,2048]{1,0:T(8,128)(2,1)} %bitcast.29), channel_id=1, source_target_pairs={{0,1},{1,0},{2,3},{3,2},{4,5},{5,4},{6,7},{7,6},{8,9},{9,8},{10,11... | collective-permute-start | bytes 12582920 | tf_op jit(solution)/shard_map/ppermute | solution.py:404
  20.1 12.2 %collective-permute-start = (bf16[3,272,256]{2,1,0:T(8,128)(2,1)S(1)}, bf16[3,272,256]{2,1,0:T(8,128)(2,1)S(1)}, u32[]{:S(2)}, u32[]{:S(2)}) collective-permute-start(bf16[3,272,256]{2,1,0:T(8,128)(2,1)S(1)} %get-tuple-element.16), channel_id=1, source_target_pairs={{0,8},{2,10},{4,12},{6,14},{8,16},{10,18},{12,20},{14,22},{16,24},... | collective-permute-start | bytes 1253384 | tf_op jit(solution)/shard_map/ppermute | solution.py:390
  23.6 11.9 %collective-permute-start.1 = (bf16[3,272,256]{2,1,0:T(8,128)(2,1)S(1)}, bf16[3,272,256]{2,1,0:T(8,128)(2,1)S(1)}, u32[]{:S(2)}, u32[]{:S(2)}) collective-permute-start(bf16[3,272,256]{2,1,0:T(8,128)(2,1)S(1)} %get-tuple-element.15), channel_id=1, source_target_pairs={{8,0},{10,2},{12,4},{14,6},{16,8},{18,10},{20,12},{22,14},{24,16},... | collective-permute-start | bytes 1253384 | tf_op jit(solution)/shard_map/ppermute | solution.py:393
  26.2 21.4 %copy-start.11 = (bf16[128,2048]{1,0:T(8,128)(2,1)S(1)}, bf16[128,2048]{1,0:T(8,128)(2,1)}, u32[]{:S(2)}) copy-start(bf16[128,2048]{1,0:T(8,128)(2,1)} %residual_ref.1) | copy-start | bytes 1572868
  26.2 21.6 %copy-start.16 = (f32[128,2]{0,1:T(2,128)S(1)}, f32[128,2]{0,1:T(2,128)}, u32[]{:S(2)}) copy-start(f32[128,2]{0,1:T(2,128)} %param.25) | copy-start | bytes 3076
  26.2 58.4 %copy-start.12 = (f32[2048]{0:T(1024)S(1)}, f32[2048]{0:T(1024)}, u32[]{:S(2)}) copy-start(f32[2048]{0:T(1024)} %param.20) | copy-start | bytes 24580
  43.4 27.4 %all-to-all-start.1 = ((bf16[8,128,128]{2,1,0:T(8,128)(2,1)}), bf16[8,128,128]{2,1,0:T(8,128)(2,1)S(1)}, u32[]{:S(2)}, u32[]{:S(2)}) async-start(bf16[8,128,128]{2,1,0:T(8,128)(2,1)} %bitcast.2), calls=%async_computation.1 | async-start | bytes 524288 | tf_op jit(solution)/shard_map/all_to_all | solution.py:410
  47.6 37.1 %collective-permute-start.7 = (bf16[128,2048]{1,0:T(8,128)(2,1)S(1)}, bf16[128,2048]{1,0:T(8,128)(2,1)S(1)}, u32[]{:S(2)}, u32[]{:S(2)}) collective-permute-start(bf16[128,2048]{1,0:T(8,128)(2,1)S(1)} %copy-done.11), channel_id=1, source_target_pairs={{0,16},{2,18},{4,20},{6,22},{8,24},{10,26},{12,28},{14,30},{16,0},... | collective-permute-start | bytes 1572872 | tf_op jit(solution)/shard_map/ppermute | solution.py:401
  47.9 22.9 %collective-permute-start.5 = (f32[8,128]{1,0:T(8,128)S(1)}, f32[8,128]{1,0:T(8,128)S(1)}, u32[]{:S(2)}, u32[]{:S(2)}) collective-permute-start(f32[8,128]{1,0:T(8,128)S(1)} %get-tuple-element.19), channel_id=1, source_target_pairs={{0,16},{2,18},{4,20},{6,22},{8,24},{10,26},{12,28},{14,30},{16,0},... | collective-permute-start | bytes 12296 | tf_op jit(solution)/shard_map/ppermute | solution.py:399
  70.8 13.9 %collective-permute-start.6 = (bf16[8,128,128]{2,1,0:T(8,128)(2,1)S(1)}, bf16[8,128,128]{2,1,0:T(8,128)(2,1)S(1)}, u32[]{:S(2)}, u32[]{:S(2)}) collective-permute-start(bf16[8,128,128]{2,1,0:T(8,128)(2,1)S(1)} %all-to-all-done.1.heads_ref), channel_id=1, source_target_pairs={{0,16},{2,18},{4,20},{6,22},{8,24},{10,26},{12,28},{14,30},{16,0},... | collective-permute-start | bytes 786440 | tf_op jit(solution)/shard_map/ppermute | solution.py:413
  84.7 2.2 %copy-start.3 = (bf16[1024,2048]{1,0:T(8,128)(2,1)S(1)}, bf16[1024,2048]{1,0:T(8,128)(2,1)}, u32[]{:S(2)}) copy-start(bf16[1024,2048]{1,0:T(8,128)(2,1)} %weight_ref.3) | copy-start | bytes 12582916
  89.2 19.4 %all-to-all-start.4 = ((bf16[8,32,2048]{2,1,0:T(8,128)(2,1)}), bf16[8,32,2048]{2,1,0:T(8,128)(2,1)S(1)}, u32[]{:S(2)}, u32[]{:S(2)}) async-start(bf16[8,32,2048]{2,1,0:T(8,128)(2,1)} %bitcast.12), calls=%async_computation.4 | async-start | bytes 2097152 | tf_op jit(solution)/shard_map/all_to_all | solution.py:420
  108.6 22.1 %all-to-all-start.2 = ((bf16[8,32,2048]{2,1,0:T(8,128)(2,1)}), bf16[8,32,2048]{2,1,0:T(8,128)(2,1)S(1)}, u32[]{:S(2)}, u32[]{:S(2)}) async-start(bf16[8,32,2048]{2,1,0:T(8,128)(2,1)} %bitcast.4), calls=%async_computation.2 | async-start | bytes 2097152 | tf_op jit(solution)/shard_map/all_to_all | solution.py:420
  113.7 2.2 %copy-start.5 = (bf16[1,2048,1024]{2,1,0:T(8,128)(2,1)S(1)}, bf16[1,2048,1024]{2,1,0:T(8,128)(2,1)}, u32[]{:S(2)}) copy-start(bf16[1,2048,1024]{2,1,0:T(8,128)(2,1)} %param.21) | copy-start | bytes 12582916
  115.9 2.2 %copy-start.7 = (bf16[1,2048,1024]{2,1,0:T(8,128)(2,1)S(1)}, bf16[1,2048,1024]{2,1,0:T(8,128)(2,1)}, u32[]{:S(2)}) copy-start(bf16[1,2048,1024]{2,1,0:T(8,128)(2,1)} %param.22) | copy-start | bytes 12582916
  118.1 2.2 %copy-start.9 = (bf16[1,1024,2048]{2,1,0:T(8,128)(2,1)S(1)}, bf16[1,1024,2048]{2,1,0:T(8,128)(2,1)}, u32[]{:S(2)}) copy-start(bf16[1,1024,2048]{2,1,0:T(8,128)(2,1)} %param.23) | copy-start | bytes 12582916
  130.7 22.1 %all-to-all-start.5 = ((bf16[8,32,2048]{2,1,0:T(8,128)(2,1)}), bf16[8,32,2048]{2,1,0:T(8,128)(2,1)S(1)}, u32[]{:S(2)}, u32[]{:S(2)}) async-start(bf16[8,32,2048]{2,1,0:T(8,128)(2,1)} %bitcast.14), calls=%async_computation.5 | async-start | bytes 2097152 | tf_op jit(solution)/shard_map/all_to_all | solution.py:420
  135.9 2.2 %copy-start.6 = (bf16[1,2048,1024]{2,1,0:T(8,128)(2,1)S(1)}, bf16[1,2048,1024]{2,1,0:T(8,128)(2,1)}, u32[]{:S(2)}) copy-start(bf16[1,2048,1024]{2,1,0:T(8,128)(2,1)} %param.21) | copy-start | bytes 12582916
  152.8 26.5 %all-to-all-start.3 = ((bf16[8,32,2048]{2,1,0:T(8,128)(2,1)}), bf16[8,32,2048]{2,1,0:T(8,128)(2,1)S(1)}, u32[]{:S(2)}, u32[]{:S(2)}) async-start(bf16[8,32,2048]{2,1,0:T(8,128)(2,1)} %bitcast.9), calls=%async_computation.3 | async-start | bytes 2097152 | tf_op jit(solution)/shard_map/all_to_all | solution.py:420
  158.5 23.6 %collective-permute-start.8 = (bf16[128,2048]{1,0:T(8,128)(2,1)S(1)}, bf16[128,2048]{1,0:T(8,128)(2,1)S(1)}, u32[]{:S(2)}, u32[]{:S(2)}) collective-permute-start(bf16[128,2048]{1,0:T(8,128)(2,1)S(1)} %partial_sum.1), channel_id=1, source_target_pairs={{0,16},{2,18},{4,20},{6,22},{8,24},{10,26},{12,28},{14,30},{16,0},... | collective-permute-start | bytes 1572872 | tf_op jit(solution)/shard_map/ppermute | solution.py:431
  (8 other events, 11.2 us)

commit v3 on v2

--- a/solution.py
+++ b/solution.py
@@ -20,6 +20,10 @@
 
 def params(mebibytes):
     return pltpu.CompilerParams(vmem_limit_bytes=mebibytes * 1024 * 1024)
+
+
+def in_hbm(value):
+    return pltpu.with_memory_space_constraint(value, pltpu.HBM)
 
 
 def cost(flops, bytes_accessed):
@@ -50,11 +54,19 @@
         out_shape=jax.ShapeDtypeStruct((heads, rows, 2 * width), BF),
         compiler_params=params(8),
         name="pack",
-    )(query_rows, key_rows, value_rows, id_rows)
+    )(*(in_hbm(rows) for rows in (query_rows, key_rows, value_rows)), id_rows)
 
 
 def attention_kernel(
-    lam_ref, prev_ref, own_ref, next_ref, o_ref, k_ref, v_ref, line_ref, id_ref
+    lam_ref,
+    prev_ref,
+    own_ref,
+    next_ref,
+    o_ref,
+    k_ref,
+    v_ref,
+    line_ref,
+    id_ref,
 ):
     b = pl.program_id(0)
     length, width = o_ref.shape[1:]
@@ -168,9 +180,27 @@
 
 
 def project_kernel(
-    heads_ref, residual_ref, gain_ref, meta_ref, weight_ref, rows_ref, mixed_ref, left_ref, *, tile
+    heads_ref,
+    residual_ref,
+    gain_ref,
+    meta_ref,
+    weight_ref,
+    rows_ref,
+    mixed_ref,
+    left_ref,
+    held_ref,
+    sems,
+    *,
+    tile,
 ):
     tokens, width = mixed_ref.shape
+    arrivals = []
+    for n in range(width // tile):
+        at = pl.ds(n * tile, tile)
+        arrivals.append(
+            pltpu.make_async_copy(weight_ref.at[:, at], held_ref.at[:, at], sems.at[n])
+        )
+        arrivals[n].start()
     members = heads_ref.shape[0]
     value_dim = heads_ref.shape[2]
     for source in range(members):
@@ -179,7 +209,8 @@
     squares = jnp.zeros((tokens, 128), F32)
     for n in range(width // tile):
         columns = slice(n * tile, (n + 1) * tile)
-        projected = jnp.dot(left_ref[...], weight_ref[:, columns], preferred_element_type=F32)
+        arrivals[n].wait()
+        projected = jnp.dot(left_ref[...], held_ref[:, columns], preferred_element_type=F32)
         mixed = (residual_ref[:, columns].astype(F32) + projected).astype(BF)
         mixed_ref[:, columns] = mixed
         wide = mixed.astype(F32)
@@ -204,83 +235,89 @@
     depth, width = out_weight.shape
     rows = jax.ShapeDtypeStruct((slots, width), BF)
     mixed = jax.ShapeDtypeStruct((tokens, width), BF)
-    left = pltpu.VMEM((tokens, depth), BF)
+    scratch = [
+        pltpu.VMEM((tokens, depth), BF),
+        pltpu.VMEM((depth, width), BF),
+        pltpu.SemaphoreType.DMA((width // tile,)),
+    ]
     return pl.pallas_call(
         functools.partial(project_kernel, tile=tile),
-        in_specs=[VM] * 5,
+        in_specs=[VM] * 4 + [ANY],
         out_specs=[VM, VM] if keep else VM,
         out_shape=[rows, mixed] if keep else rows,
-        scratch_shapes=[left] if keep else [pltpu.VMEM((tokens, width), BF), left],
+        scratch_shapes=scratch if keep else [pltpu.VMEM((tokens, width), BF), *scratch],
         compiler_params=params(16),
         cost_estimate=cost(3 * 10**9, 8 * 10**6),
-    )(heads, residual, gain, meta, out_weight)
-
-
-def expert_kernel(
-    x_ref, g0, u0, d0, g1, u1, d1, y_ref, gb, ub, db, hidden_ref, half_ref, sems, *, tile
-):
-    steps = g0.shape[1] // tile
-    width = y_ref.shape[1]
-    arrivals = []
-    for step in range(steps):
-        at = pl.ds(step * tile, tile)
-        arrivals.append(
-            (
-                pltpu.make_async_copy(g1.at[:, at], gb.at[:, at], sems.at[step]),
-                pltpu.make_async_copy(u1.at[:, at], ub.at[:, at], sems.at[steps + step]),
-            )
-        )
-    last = [
-        pltpu.make_async_copy(
-            d1.at[pl.ds(n * tile, tile)], db.at[pl.ds(n * tile, tile)], sems.at[2 * steps + n]
-        )
-        for n in range(steps)
-    ]
-    for pair in arrivals:
-        for copy in pair:
-            copy.start()
-    for copy in last:
-        copy.start()
-    for h, (g, u, d) in enumerate(((g0, u0, d0), (gb, ub, db))):
-        for step in range(steps):
+    )(heads, residual, gain, meta, in_hbm(out_weight))
+
+
+def expert_rows(x_ref, g, u, d, y_ref, hidden_ref, half_ref, tile, arrive):
+    halves, width, depth = g.shape
+    for h in range(halves):
+        for step in range(depth // tile):
             at = slice(step * tile, (step + 1) * tile)
-            if h:
-                for copy in arrivals[step]:
-                    copy.wait()
-            gate = jnp.dot(x_ref[...], g[:, at], preferred_element_type=F32)
-            upward = jnp.dot(x_ref[...], u[:, at], preferred_element_type=F32)
+            arrive(h, step)
+            gate = jnp.dot(x_ref[...], g[h, :, at], preferred_element_type=F32)
+            upward = jnp.dot(x_ref[...], u[h, :, at], preferred_element_type=F32)
             hidden_ref[:, at] = (gate / (1.0 + jnp.exp(-gate)) * upward).astype(BF)
-        if h:
-            for copy in last:
-                copy.wait()
+        arrive(h, depth // tile)
         for n in range(width // tile):
             at = slice(n * tile, (n + 1) * tile)
-            part = jnp.dot(hidden_ref[...], d[:, at], preferred_element_type=F32).astype(BF)
+            part = jnp.dot(hidden_ref[...], d[h, :, at], preferred_element_type=F32).astype(BF)
             if h:
                 y_ref[:, at] = (half_ref[:, at].astype(F32) + part.astype(F32)).astype(BF)
             else:
                 half_ref[:, at] = part
 
 
+def expert_kernel(
+    x_ref, g0, u0, d0, g1, u1, d1, y_ref, gs, us, ds, hidden_ref, half_ref, sems, *, tile
+):
+    steps = g0.shape[1] // tile
+    arrivals = []
+    for h, (g, u, d) in enumerate(((g0, u0, d0), (g1, u1, d1))):
+        waves = []
+        for step in range(steps):
+            at = pl.ds(step * tile, tile)
+            waves.append(
+                (
+                    pltpu.make_async_copy(g.at[:, at], gs.at[h, :, at], sems.at[h, 2 * step]),
+                    pltpu.make_async_copy(u.at[:, at], us.at[h, :, at], sems.at[h, 2 * step + 1]),
+                )
+            )
+        waves.append((pltpu.make_async_copy(d, ds.at[h], sems.at[h, 2 * steps]),))
+        arrivals.append(waves)
+    for waves in arrivals:
+        for wave in waves:
+            for copy in wave:
+                copy.start()
+
+    def arrive(h, step):
+        for copy in arrivals[h][step]:
+            copy.wait()
+
+    expert_rows(x_ref, gs, us, ds, y_ref, hidden_ref, half_ref, tile, arrive)
+
+
 def experts_of(x, own, other, tile=256):
     rows, width = x.shape
     depth = own[0].shape[1]
     return pl.pallas_call(
         functools.partial(expert_kernel, tile=tile),
-        in_specs=[VM] * 4 + [ANY] * 3,
+        in_specs=[VM] + [ANY] * 6,
         out_specs=VM,
         out_shape=jax.ShapeDtypeStruct((rows, width), BF),
         scratch_shapes=[
-            pltpu.VMEM((width, depth), BF),
-            pltpu.VMEM((width, depth), BF),
-            pltpu.VMEM((depth, width), BF),
+            pltpu.VMEM((2, width, depth), BF),
+            pltpu.VMEM((2, width, depth), BF),
+            pltpu.VMEM((2, depth, width), BF),
             pltpu.VMEM((rows, depth), BF),
             pltpu.VMEM((rows, width), BF),
-            pltpu.SemaphoreType.DMA((3 * (depth // tile),)),
+            pltpu.SemaphoreType.DMA((2, 2 * (depth // tile) + 1)),
         ],
-        compiler_params=params(34),
+        compiler_params=params(40),
         cost_estimate=cost(9 * 10**9, 26 * 10**6),
-    )(x, *own, *other)
+    )(x, *(in_hbm(weight) for weight in (*own, *other)))
 
 
 def picked(meta_ref, rows_ref, write, tile=512):
@@ -379,7 +416,7 @@
     capacity = 2 * length // count
     planes = [[g * heads + j for j in range(heads)] for g in range(count // heads)]
     halves = [[h * half + j for j in range(half)] for h in range(2)]
-    mirror = [(i, (i + half) % count) for i in range(count)]
+    mirror = [(i, i ^ (count - count // 4)) for i in range(count)]
     swap = [(i, twins - 1 - i) for i in range(twins)]
 
     value_dim = value_rows.shape[1] // heads

time: 187 us -> 176 us (0.941)
  the two profiles are of different devices: /device:TPU:12 before, /device:TPU:0 now
where the time goes in v3:
time: 176 us; the launch traced here: 175 us
  waiting for transfers between devices  75.9 us (43%)
  starting transfers between devices  52.1 us (30%)
  Pallas kernels  44.5 us (25%)
    all_to_all x4, starting transfers between devices, exchange(): lax.all_to_all(rows, 'sp', 0, 0, tiled=True, axis_index_groups=halves)  29 us
    pallas_call x2, Pallas kernels, experts_of(): pl.pallas_call(functools.partial(expert_kernel, tile=tile), in_specs=[VM]...  23.1 us
    all_to_all x4, waiting for transfers between devices, exchange(): lax.all_to_all(rows, 'sp', 0, 0, tiled=True, axis_index_groups=halves)  23 us
    ppermute x1, waiting for transfers between devices, on_device(): part = lax.ppermute(part_far, 'sp', mirror)  12.3 us
    ppermute x1, waiting for transfers between devices, on_device(): meta_far = lax.ppermute(meta_far, 'sp', mirror)  12.2 us
    all_to_all x1, waiting for transfers between devices, on_device(): lax.all_to_all(packed, 'sp', 0, 0, tiled=True, axis_index_groups=planes)  9.34 us
    ppermute x1, waiting for transfers between devices, on_device(): heads_far = lax.ppermute(token_heads, 'sp', mirror)  8.4 us
    pallas_call x2, Pallas kernels, project(): pl.pallas_call(functools.partial(project_kernel, tile=tile), in_specs=[VM...  8.21 us
  transfers between devices with their start and end apart: 15, of which 10 were waited for; matrix products, arithmetic and copies ran while one was open for 1% of the time, Pallas kernels for 23%

profile of v3, /device:TPU:0, one launch (start us, length us, event | category | flops | bytes accessed | tf_op | source)
XLA Modules:
  0.0 175.1 jit_solution(14106608616114252017)
XLA Ops:
  0.7 3.3 %pack.1 = bf16[4,400,256]{2,1,0:T(8,128)(2,1)} custom-call(bf16[256,512]{1,0:T(8,128)(2,1)} %q_ref.1, bf16[256,512]{1,0:T(8,128)(2,1)} %k_ref.1, bf16[256,512]{1,0:T(8,128)(2,1)} %v_ref.1, bf16[16,256]{1,0:T(8,128)(2,1)S(1)} %broadcast_in_dim.7.id_ref), custom_call_target="tpu_custom_call" | custom-call | tf_op jit(solution)/shard_map/pack/pallas_call | solution.py:49
  4.0 5.2 %all-to-all-start = ((bf16[4,400,256]{2,1,0:T(8,128)(2,1)}), bf16[4,400,256]{2,1,0:T(8,128)(2,1)S(1)}, u32[]{:S(2)}, u32[]{:S(2)}) async-start(bf16[4,400,256]{2,1,0:T(8,128)(2,1)} %pack.1), calls=%async_computation | async-start | bytes 1638400 | tf_op jit(solution)/shard_map/all_to_all | solution.py:425
  11.0 9.3 %all-to-all-done.own_ref = bf16[4,400,256]{2,1,0:T(8,128)(2,1)S(1)} async-done(((bf16[4,400,256]{2,1,0:T(8,128)(2,1)}), bf16[4,400,256]{2,1,0:T(8,128)(2,1)S(1)}, u32[]{:S(2)}, u32[]{:S(2)}) %all-to-all-start) | async-done | bytes 819232 | tf_op jit(solution)/shard_map/all_to_all | solution.py:425
  20.4 3.5 %collective-permute-start = (bf16[3,272,256]{2,1,0:T(8,128)(2,1)S(1)}, bf16[3,272,256]{2,1,0:T(8,128)(2,1)S(1)}, u32[]{:S(2)}, u32[]{:S(2)}) collective-permute-start(bf16[3,272,256]{2,1,0:T(8,128)(2,1)S(1)} %get-tuple-element.16), channel_id=1, source_target_pairs={{0,8},{2,10},{4,12},{6,14},{8,16},{10,18},{12,20},{14,22},{16,24},... | collective-permute-start | bytes 1253384 | tf_op jit(solution)/shard_map/ppermute | solution.py:427
  25.5 6.6 %collective-permute-done.prev_ref = bf16[3,272,256]{2,1,0:T(8,128)(2,1)S(1)} collective-permute-done((bf16[3,272,256]{2,1,0:T(8,128)(2,1)S(1)}, bf16[3,272,256]{2,1,0:T(8,128)(2,1)S(1)}, u32[]{:S(2)}, u32[]{:S(2)}) %collective-permute-start) | collective-permute-done | bytes 417824 | tf_op jit(solution)/shard_map/ppermute | solution.py:427
  32.1 4.1 %collective-permute-done.1.next_ref = bf16[3,272,256]{2,1,0:T(8,128)(2,1)S(1)} collective-permute-done((bf16[3,272,256]{2,1,0:T(8,128)(2,1)S(1)}, bf16[3,272,256]{2,1,0:T(8,128)(2,1)S(1)}, u32[]{:S(2)}, u32[]{:S(2)}) %collective-permute-start.1) | collective-permute-done | bytes 417824 | tf_op jit(solution)/shard_map/ppermute | solution.py:430
  36.2 7.9 %attention.1 = bf16[4,256,128]{2,1,0:T(8,128)(2,1)} custom-call(f32[1]{0:T(128)} %dynamic_slice.3.lam_ref, bf16[3,272,256]{2,1,0:T(8,128)(2,1)S(1)} %collective-permute-done.prev_ref, bf16[4,400,256]{2,1,0:T(8,128)(2,1)S(1)} %all-to-all-done.own_ref, bf16[3,272,256]{2,1,0:T(8,128)(2,1)S(1)} %collective-permute-done.1.next_ref), custom_call_target="tpu_custom_call" | custom-call | flops 8000000000 | bytes 4000000 | tf_op jit(solution)/shard_map/attention/pallas_call | solution.py:164
  44.1 3.4 %all-to-all-start.1 = ((bf16[8,128,128]{2,1,0:T(8,128)(2,1)}), bf16[8,128,128]{2,1,0:T(8,128)(2,1)S(1)}, u32[]{:S(2)}, u32[]{:S(2)}) async-start(bf16[8,128,128]{2,1,0:T(8,128)(2,1)} %bitcast.2), calls=%async_computation.1 | async-start | bytes 524288 | tf_op jit(solution)/shard_map/all_to_all | solution.py:447
  48.9 2.7 %collective-permute-start.5 = (f32[8,128]{1,0:T(8,128)S(1)}, f32[8,128]{1,0:T(8,128)S(1)}, u32[]{:S(2)}, u32[]{:S(2)}) collective-permute-start(f32[8,128]{1,0:T(8,128)S(1)} %get-tuple-element.19), channel_id=1, source_target_pairs={{0,24},{2,26},{4,28},{6,30},{8,16},{10,18},{12,20},{14,22},{16,8},... | collective-permute-start | bytes 12296 | tf_op jit(solution)/shard_map/ppermute | solution.py:436
  51.6 12.2 %collective-permute-done.5.meta_ref = f32[8,128]{1,0:T(8,128)S(1)} collective-permute-done((f32[8,128]{1,0:T(8,128)S(1)}, f32[8,128]{1,0:T(8,128)S(1)}, u32[]{:S(2)}, u32[]{:S(2)}) %collective-permute-start.5) | collective-permute-done | bytes 4128 | tf_op jit(solution)/shard_map/ppermute | solution.py:436
  64.8 8.4 %collective-permute-done.6.heads_ref = bf16[8,128,128]{2,1,0:T(8,128)(2,1)S(1)} collective-permute-done((bf16[8,128,128]{2,1,0:T(8,128)(2,1)S(1)}, bf16[8,128,128]{2,1,0:T(8,128)(2,1)S(1)}, u32[]{:S(2)}, u32[]{:S(2)}) %collective-permute-start.6) | collective-permute-done | bytes 262176 | tf_op jit(solution)/shard_map/ppermute | solution.py:450
  73.3 4.1 %shard_map.129 = bf16[256,2048]{1,0:T(8,128)(2,1)} custom-call(bf16[8,128,128]{2,1,0:T(8,128)(2,1)S(1)} %collective-permute-done.6.heads_ref, bf16[128,2048]{1,0:T(8,128)(2,1)S(1)} %collective-permute-done.7.residual_ref, f32[1,2048]{1,0:T(1,128)S(1)} %bitcast.23, f32[8,128]{1,0:T(8,128)S(1)} %collective-permute-done.5.meta_ref, bf16[1024,2048]{1,0:T(8,128)(2,1)} %weight_ref.3), custom_call_target="tpu_custom_call" | custom-call | flops 3000000000 | bytes 8000000 | tf_op jit(solution)/shard_map/pallas_call | solution.py:243
  77.4 17.9 %all-to-all-start.4 = ((bf16[8,32,2048]{2,1,0:T(8,128)(2,1)}), bf16[8,32,2048]{2,1,0:T(8,128)(2,1)S(1)}, u32[]{:S(2)}, u32[]{:S(2)}) async-start(bf16[8,32,2048]{2,1,0:T(8,128)(2,1)} %bitcast.12), calls=%async_computation.4 | async-start | bytes 2097152 | tf_op jit(solution)/shard_map/all_to_all | solution.py:457
  95.3 4.1 %shard_map.127 = (bf16[256,2048]{1,0:T(8,128)(2,1)}, bf16[128,2048]{1,0:T(8,128)(2,1)S(1)}) custom-call(bf16[8,128,128]{2,1,0:T(8,128)(2,1)S(1)} %all-to-all-done.1.heads_ref, bf16[128,2048]{1,0:T(8,128)(2,1)S(1)} %copy-done, f32[1,2048]{1,0:T(1,128)S(1)} %bitcast.24, f32[8,128]{1,0:T(8,128)S(1)} %get-tuple-element.20.meta_ref, bf16[1024,2048]{1,0:T(8,128)(2,1)} %weight_ref.3), custom_call_target="tpu_custom_call" | custom-call | flops 3000000000 | bytes 8000000 | tf_op jit(solution)/shard_map/pallas_call | solution.py:243
  99.4 9.2 %all-to-all-done.4 = bf16[8,32,2048]{2,1,0:T(8,128)(2,1)S(1)} async-done(((bf16[8,32,2048]{2,1,0:T(8,128)(2,1)}), bf16[8,32,2048]{2,1,0:T(8,128)(2,1)S(1)}, u32[]{:S(2)}, u32[]{:S(2)}) %all-to-all-start.4) | async-done | bytes 1048608 | tf_op jit(solution)/shard_map/all_to_all | solution.py:457
  108.6 3.7 %all-to-all-start.2 = ((bf16[8,32,2048]{2,1,0:T(8,128)(2,1)}), bf16[8,32,2048]{2,1,0:T(8,128)(2,1)S(1)}, u32[]{:S(2)}, u32[]{:S(2)}) async-start(bf16[8,32,2048]{2,1,0:T(8,128)(2,1)} %bitcast.4), calls=%async_computation.2 | async-start | bytes 2097152 | tf_op jit(solution)/shard_map/all_to_all | solution.py:457
  112.4 11.6 %shard_map.130 = bf16[256,2048]{1,0:T(8,128)(2,1)} custom-call(bf16[256,2048]{1,0:T(8,128)(2,1)S(1)} %bitcast.19, bf16[2048,1024]{1,0:T(8,128)(2,1)} %bitcast.27, bf16[2048,1024]{1,0:T(8,128)(2,1)} %bitcast.30, bf16[1024,2048]{1,0:T(8,128)(2,1)} %bitcast.33, bf16[2048,1024]{1,0:T(8,128)(2,1)} %collective-permute-done.2.g1, ...), custom_call_target="tpu_custom_call" | custom-call | flops 8999999488 | bytes 26000000 | tf_op jit(solution)/shard_map/pallas_call | solution.py:305
  126.1 3.8 %all-to-all-start.5 = ((bf16[8,32,2048]{2,1,0:T(8,128)(2,1)}), bf16[8,32,2048]{2,1,0:T(8,128)(2,1)S(1)}, u32[]{:S(2)}, u32[]{:S(2)}) async-start(bf16[8,32,2048]{2,1,0:T(8,128)(2,1)} %bitcast.14), calls=%async_computation.5 | async-start | bytes 2097152 | tf_op jit(solution)/shard_map/all_to_all | solution.py:457
  129.9 11.5 %shard_map.128 = bf16[256,2048]{1,0:T(8,128)(2,1)} custom-call(bf16[256,2048]{1,0:T(8,128)(2,1)S(1)} %bitcast.20, bf16[2048,1024]{1,0:T(8,128)(2,1)} %bitcast.28, bf16[2048,1024]{1,0:T(8,128)(2,1)} %bitcast.31, bf16[1024,2048]{1,0:T(8,128)(2,1)} %bitcast.34, bf16[2048,1024]{1,0:T(8,128)(2,1)} %collective-permute-done.2.g1, ...), custom_call_target="tpu_custom_call" | custom-call | flops 8999999488 | bytes 26000000 | tf_op jit(solution)/shard_map/pallas_call | solution.py:305
  141.5 2.2 %all-to-all-done.5 = bf16[8,32,2048]{2,1,0:T(8,128)(2,1)S(1)} async-done(((bf16[8,32,2048]{2,1,0:T(8,128)(2,1)}), bf16[8,32,2048]{2,1,0:T(8,128)(2,1)S(1)}, u32[]{:S(2)}, u32[]{:S(2)}) %all-to-all-start.5) | async-done | bytes 1048608 | tf_op jit(solution)/shard_map/all_to_all | solution.py:457
  143.7 3.6 %all-to-all-start.3 = ((bf16[8,32,2048]{2,1,0:T(8,128)(2,1)}), bf16[8,32,2048]{2,1,0:T(8,128)(2,1)S(1)}, u32[]{:S(2)}, u32[]{:S(2)}) async-start(bf16[8,32,2048]{2,1,0:T(8,128)(2,1)} %bitcast.9), calls=%async_computation.3 | async-start | bytes 2097152 | tf_op jit(solution)/shard_map/all_to_all | solution.py:457
  147.9 4.1 %collective-permute-start.8 = (bf16[128,2048]{1,0:T(8,128)(2,1)S(1)}, bf16[128,2048]{1,0:T(8,128)(2,1)S(1)}, u32[]{:S(2)}, u32[]{:S(2)}) collective-permute-start(bf16[128,2048]{1,0:T(8,128)(2,1)S(1)} %partial_sum.1), channel_id=1, source_target_pairs={{0,24},{2,26},{4,28},{6,30},{8,16},{10,18},{12,20},{14,22},{16,8},... | collective-permute-start | bytes 1572872 | tf_op jit(solution)/shard_map/ppermute | solution.py:468
  152.0 9.3 %all-to-all-done.3 = bf16[8,32,2048]{2,1,0:T(8,128)(2,1)S(1)} async-done(((bf16[8,32,2048]{2,1,0:T(8,128)(2,1)}), bf16[8,32,2048]{2,1,0:T(8,128)(2,1)S(1)}, u32[]{:S(2)}, u32[]{:S(2)}) %all-to-all-start.3) | async-done | bytes 1048608 | tf_op jit(solution)/shard_map/all_to_all | solution.py:457
  161.3 12.3 %collective-permute-done.8.far_ref = bf16[128,2048]{1,0:T(8,128)(2,1)S(1)} collective-permute-done((bf16[128,2048]{1,0:T(8,128)(2,1)S(1)}, bf16[128,2048]{1,0:T(8,128)(2,1)S(1)}, u32[]{:S(2)}, u32[]{:S(2)}) %collective-permute-start.8) | collective-permute-done | bytes 524320 | tf_op jit(solution)/shard_map/ppermute | solution.py:468
  (33 shorter events, 10.8 us)
Async XLA Ops:
  0.0 25.3 %copy-start.2 = (s32[128,2]{0,1:T(2,128)S(1)}, s32[128,2]{0,1:T(2,128)}, u32[]{:S(2)}) copy-start(s32[128,2]{0,1:T(2,128)} %param.24) | copy-start | bytes 3076
  4.0 16.4 %all-to-all-start = ((bf16[4,400,256]{2,1,0:T(8,128)(2,1)}), bf16[4,400,256]{2,1,0:T(8,128)(2,1)S(1)}, u32[]{:S(2)}, u32[]{:S(2)}) async-start(bf16[4,400,256]{2,1,0:T(8,128)(2,1)} %pack.1), calls=%async_computation | async-start | bytes 1638400 | tf_op jit(solution)/shard_map/all_to_all | solution.py:425
  9.2 103.2 %collective-permute-start.2 = (bf16[2048,1024]{1,0:T(8,128)(2,1)}, bf16[2048,1024]{1,0:T(8,128)(2,1)}, u32[]{:S(2)}, u32[]{:S(2)}) collective-permute-start(bf16[2048,1024]{1,0:T(8,128)(2,1)} %bitcast.26), channel_id=1, source_target_pairs={{0,1},{1,0},{2,3},{3,2},{4,5},{5,4},{6,7},{7,6},{8,9},{9,8},{10,11... | collective-permute-start | bytes 12582920 | tf_op jit(solution)/shard_map/ppermute | solution.py:441
  9.2 103.2 %collective-permute-start.3 = (bf16[2048,1024]{1,0:T(8,128)(2,1)}, bf16[2048,1024]{1,0:T(8,128)(2,1)}, u32[]{:S(2)}, u32[]{:S(2)}) collective-permute-start(bf16[2048,1024]{1,0:T(8,128)(2,1)} %bitcast.29), channel_id=1, source_target_pairs={{0,1},{1,0},{2,3},{3,2},{4,5},{5,4},{6,7},{7,6},{8,9},{9,8},{10,11... | collective-permute-start | bytes 12582920 | tf_op jit(solution)/shard_map/ppermute | solution.py:441
  9.7 102.7 %collective-permute-start.4 = (bf16[1024,2048]{1,0:T(8,128)(2,1)}, bf16[1024,2048]{1,0:T(8,128)(2,1)}, u32[]{:S(2)}, u32[]{:S(2)}) collective-permute-start(bf16[1024,2048]{1,0:T(8,128)(2,1)} %bitcast.32), channel_id=1, source_target_pairs={{0,1},{1,0},{2,3},{3,2},{4,5},{5,4},{6,7},{7,6},{8,9},{9,8},{10,11... | collective-permute-start | bytes 12582920 | tf_op jit(solution)/shard_map/ppermute | solution.py:441
  20.4 11.6 %collective-permute-start = (bf16[3,272,256]{2,1,0:T(8,128)(2,1)S(1)}, bf16[3,272,256]{2,1,0:T(8,128)(2,1)S(1)}, u32[]{:S(2)}, u32[]{:S(2)}) collective-permute-start(bf16[3,272,256]{2,1,0:T(8,128)(2,1)S(1)} %get-tuple-element.16), channel_id=1, source_target_pairs={{0,8},{2,10},{4,12},{6,14},{8,16},{10,18},{12,20},{14,22},{16,24},... | collective-permute-start | bytes 1253384 | tf_op jit(solution)/shard_map/ppermute | solution.py:427
  24.0 12.2 %collective-permute-start.1 = (bf16[3,272,256]{2,1,0:T(8,128)(2,1)S(1)}, bf16[3,272,256]{2,1,0:T(8,128)(2,1)S(1)}, u32[]{:S(2)}, u32[]{:S(2)}) collective-permute-start(bf16[3,272,256]{2,1,0:T(8,128)(2,1)S(1)} %get-tuple-element.15), channel_id=1, source_target_pairs={{8,0},{10,2},{12,4},{14,6},{16,8},{18,10},{20,12},{22,14},{24,16},... | collective-permute-start | bytes 1253384 | tf_op jit(solution)/shard_map/ppermute | solution.py:430
  25.5 22.0 %copy-start = (bf16[128,2048]{1,0:T(8,128)(2,1)S(1)}, bf16[128,2048]{1,0:T(8,128)(2,1)}, u32[]{:S(2)}) copy-start(bf16[128,2048]{1,0:T(8,128)(2,1)} %residual_ref.1) | copy-start | bytes 1572868
  25.5 23.3 %copy-start.3 = (f32[128,2]{0,1:T(2,128)S(1)}, f32[128,2]{0,1:T(2,128)}, u32[]{:S(2)}) copy-start(f32[128,2]{0,1:T(2,128)} %param.25) | copy-start | bytes 3076
  25.5 47.8 %copy-start.1 = (f32[2048]{0:T(1024)S(1)}, f32[2048]{0:T(1024)}, u32[]{:S(2)}) copy-start(f32[2048]{0:T(1024)} %param.20) | copy-start | bytes 24580
  44.1 19.6 %all-to-all-start.1 = ((bf16[8,128,128]{2,1,0:T(8,128)(2,1)}), bf16[8,128,128]{2,1,0:T(8,128)(2,1)S(1)}, u32[]{:S(2)}, u32[]{:S(2)}) async-start(bf16[8,128,128]{2,1,0:T(8,128)(2,1)} %bitcast.2), calls=%async_computation.1 | async-start | bytes 524288 | tf_op jit(solution)/shard_map/all_to_all | solution.py:447
  47.5 25.8 %collective-permute-start.7 = (bf16[128,2048]{1,0:T(8,128)(2,1)S(1)}, bf16[128,2048]{1,0:T(8,128)(2,1)S(1)}, u32[]{:S(2)}, u32[]{:S(2)}) collective-permute-start(bf16[128,2048]{1,0:T(8,128)(2,1)S(1)} %copy-done), channel_id=1, source_target_pairs={{0,24},{2,26},{4,28},{6,30},{8,16},{10,18},{12,20},{14,22},{16,8},... | collective-permute-start | bytes 1572872 | tf_op jit(solution)/shard_map/ppermute | solution.py:438
  48.9 14.9 %collective-permute-start.5 = (f32[8,128]{1,0:T(8,128)S(1)}, f32[8,128]{1,0:T(8,128)S(1)}, u32[]{:S(2)}, u32[]{:S(2)}) collective-permute-start(f32[8,128]{1,0:T(8,128)S(1)} %get-tuple-element.19), channel_id=1, source_target_pairs={{0,24},{2,26},{4,28},{6,30},{8,16},{10,18},{12,20},{14,22},{16,8},... | collective-permute-start | bytes 12296 | tf_op jit(solution)/shard_map/ppermute | solution.py:436
  63.7 9.5 %collective-permute-start.6 = (bf16[8,128,128]{2,1,0:T(8,128)(2,1)S(1)}, bf16[8,128,128]{2,1,0:T(8,128)(2,1)S(1)}, u32[]{:S(2)}, u32[]{:S(2)}) collective-permute-start(bf16[8,128,128]{2,1,0:T(8,128)(2,1)S(1)} %all-to-all-done.1.heads_ref), channel_id=1, source_target_pairs={{0,24},{2,26},{4,28},{6,30},{8,16},{10,18},{12,20},{14,22},{16,8},... | collective-permute-start | bytes 786440 | tf_op jit(solution)/shard_map/ppermute | solution.py:450
  77.4 31.2 %all-to-all-start.4 = ((bf16[8,32,2048]{2,1,0:T(8,128)(2,1)}), bf16[8,32,2048]{2,1,0:T(8,128)(2,1)S(1)}, u32[]{:S(2)}, u32[]{:S(2)}) async-start(bf16[8,32,2048]{2,1,0:T(8,128)(2,1)} %bitcast.12), calls=%async_computation.4 | async-start | bytes 2097152 | tf_op jit(solution)/shard_map/all_to_all | solution.py:457
  108.6 17.5 %all-to-all-start.2 = ((bf16[8,32,2048]{2,1,0:T(8,128)(2,1)}), bf16[8,32,2048]{2,1,0:T(8,128)(2,1)S(1)}, u32[]{:S(2)}, u32[]{:S(2)}) async-start(bf16[8,32,2048]{2,1,0:T(8,128)(2,1)} %bitcast.4), calls=%async_computation.2 | async-start | bytes 2097152 | tf_op jit(solution)/shard_map/all_to_all | solution.py:457
  126.1 17.6 %all-to-all-start.5 = ((bf16[8,32,2048]{2,1,0:T(8,128)(2,1)}), bf16[8,32,2048]{2,1,0:T(8,128)(2,1)S(1)}, u32[]{:S(2)}, u32[]{:S(2)}) async-start(bf16[8,32,2048]{2,1,0:T(8,128)(2,1)} %bitcast.14), calls=%async_computation.5 | async-start | bytes 2097152 | tf_op jit(solution)/shard_map/all_to_all | solution.py:457
  143.7 17.6 %all-to-all-start.3 = ((bf16[8,32,2048]{2,1,0:T(8,128)(2,1)}), bf16[8,32,2048]{2,1,0:T(8,128)(2,1)S(1)}, u32[]{:S(2)}, u32[]{:S(2)}) async-start(bf16[8,32,2048]{2,1,0:T(8,128)(2,1)} %bitcast.9), calls=%async_computation.3 | async-start | bytes 2097152 | tf_op jit(solution)/shard_map/all_to_all | solution.py:457
  147.9 25.8 %collective-permute-start.8 = (bf16[128,2048]{1,0:T(8,128)(2,1)S(1)}, bf16[128,2048]{1,0:T(8,128)(2,1)S(1)}, u32[]{:S(2)}, u32[]{:S(2)}) collective-permute-start(bf16[128,2048]{1,0:T(8,128)(2,1)S(1)} %partial_sum.1), channel_id=1, source_target_pairs={{0,24},{2,26},{4,28},{6,30},{8,16},{10,18},{12,20},{14,22},{16,8},... | collective-permute-start | bytes 1572872 | tf_op jit(solution)/shard_map/ppermute | solution.py:468

commit v4 on v3

--- a/solution.py
+++ b/solution.py
@@ -30,35 +30,33 @@
     return pl.CostEstimate(flops=flops, bytes_accessed=bytes_accessed, transcendentals=0)
 
 
-def pack_kernel(q_ref, k_ref, v_ref, id_ref, o_ref):
-    length, width = k_ref.shape
-    part = length // 2
-    scaled = (q_ref[...].astype(F32) * (HD**-0.5)).astype(BF)
-    o_ref[0, :length, :width] = k_ref[...]
-    o_ref[0, :length, width:] = v_ref[...]
-    o_ref[0, length : length + 16, :] = id_ref[...]
-    o_ref[0, length + 16 :, :width] = scaled[:part]
-    o_ref[0, length + 16 :, width:] = scaled[part:]
-
-
-def pack(query_rows, key_rows, value_rows, id_rows, heads):
-    length = query_rows.shape[0]
-    width = query_rows.shape[1] // heads
-    rows = length + 16 + length // 2
-    columns = pl.BlockSpec((length, width), lambda h: (0, h))
+def pack_kernel(k_ref, v_ref, id_ref, o_ref):
+    heads, _, width = o_ref.shape
+    length = k_ref.shape[0]
+    part = width // 2
+    for h in range(heads):
+        columns = slice(h * part, (h + 1) * part)
+        o_ref[h, :length, :part] = k_ref[:, columns]
+        o_ref[h, :length, part:] = v_ref[:, columns]
+        o_ref[h, length:, :] = id_ref[...]
+
+
+def pack(key_rows, value_rows, id_rows, heads):
+    length = key_rows.shape[0]
+    width = key_rows.shape[1] // heads
     return pl.pallas_call(
         pack_kernel,
-        grid=(heads,),
-        in_specs=[columns] * 3 + [pl.BlockSpec(id_rows.shape, lambda h: (0, 0))],
-        out_specs=pl.BlockSpec((1, rows, 2 * width), lambda h: (h, 0, 0)),
-        out_shape=jax.ShapeDtypeStruct((heads, rows, 2 * width), BF),
+        in_specs=[VM] * 3,
+        out_specs=VM,
+        out_shape=jax.ShapeDtypeStruct((heads, length + 16, 2 * width), BF),
         compiler_params=params(8),
         name="pack",
-    )(*(in_hbm(rows) for rows in (query_rows, key_rows, value_rows)), id_rows)
+    )(in_hbm(key_rows), in_hbm(value_rows), id_rows)
 
 
 def attention_kernel(
     lam_ref,
+    q_ref,
     prev_ref,
     own_ref,
     next_ref,
@@ -67,6 +65,7 @@
     v_ref,
     line_ref,
     id_ref,
+    bound_ref,
 ):
     b = pl.program_id(0)
     length, width = o_ref.shape[1:]
@@ -90,18 +89,22 @@
         v_ref[blocks * length :, :width] = jnp.zeros((length, width), BF)
         line_ref[0:1, blocks * length :] = jnp.zeros((1, length), F32)
 
+        ids = id_ref[...]
+        smallest = jnp.min(ids, axis=1, keepdims=True)
+        largest = jnp.max(ids, axis=1, keepdims=True)
+        place = lax.broadcasted_iota(jnp.int32, smallest.shape, 0)
+        for i in range(group):
+            low = smallest[before + i : before + i + 1]
+            high = largest[before + i : before + i + 1]
+            apart = (largest < low) | (smallest > high)
+            early = apart & (place >= i) & (place < i + before)
+            late = apart & (place > i + before) & (place < i + span)
+            bound_ref[0, i] = jnp.sum(jnp.where(early, 1.0, 0.0)).astype(jnp.int32)
+            bound_ref[1, i] = jnp.sum(jnp.where(late, 1.0, 0.0)).astype(jnp.int32)
+
     query_ids = id_ref[pl.ds(b + before, 1), :]
-    low = jnp.min(query_ids, axis=1, keepdims=True)
-    high = jnp.max(query_ids, axis=1, keepdims=True)
-    ids = id_ref[...]
-    smallest = jnp.min(ids, axis=1, keepdims=True)
-    largest = jnp.max(ids, axis=1, keepdims=True)
-    place = lax.broadcasted_iota(jnp.int32, smallest.shape, 0) - b
-    apart = (largest < low) | (smallest > high)
-    left = jnp.sum(jnp.where(apart & (place >= 0) & (place < before), 1.0, 0.0))
-    right = jnp.sum(jnp.where(apart & (place > before) & (place < span), 1.0, 0.0))
-    left = left.astype(jnp.int32)
-    pairs = (span + 1 - right.astype(jnp.int32) - left) // 2
+    left = bound_ref[0, b]
+    pairs = (span + 1 - bound_ref[1, b] - left) // 2
     start = pl.multiple_of((b + left) * length, length)
     query_column = jnp.transpose(jnp.broadcast_to(query_ids, (128, length)))
     lam = lam_ref[0]
@@ -110,14 +113,8 @@
         named = line_ref[0:1, pl.ds(start, keys)]
         for chunk in range(length // 128):
             mine = query_column[chunk * 128 : (chunk + 1) * 128, :]
-            q = own_ref[
-                b,
-                length + 16 + (chunk * 128) % (length // 2) : length
-                + 16
-                + (chunk * 128) % (length // 2)
-                + 128,
-                (chunk * 128 // (length // 2)) * width : (chunk * 128 // (length // 2) + 1) * width,
-            ]
+            q = q_ref[b, chunk * 128 : (chunk + 1) * 128, :]
+            q = (q.astype(F32) * (HD**-0.5)).astype(BF)
             zero = jnp.zeros((128, HD), BF)
             sides = (
                 jnp.concatenate([q[:, :HD], zero], axis=1),
@@ -157,14 +154,14 @@
             attend(count * 2 * length)
 
 
-def attention(lam, prev, own, following, length, width):
-    group = own.shape[0]
+def attention(lam, queries, prev, own, following):
+    group, length, width = queries.shape
     before, after = prev.shape[0], following.shape[0]
     blocks = before + group + after
     return pl.pallas_call(
         attention_kernel,
         grid=(group,),
-        in_specs=[SM] + [VM] * 3,
+        in_specs=[SM] + [VM] * 4,
         out_specs=VM,
         out_shape=jax.ShapeDtypeStruct((group, length, width), BF),
         scratch_shapes=[
@@ -172,11 +169,12 @@
             pltpu.VMEM(((blocks + 1) * length, 2 * width), BF),
             pltpu.VMEM((8, (blocks + 1) * length), F32),
             pltpu.VMEM((-(-(blocks + 1) // 8) * 8, length), F32),
+            pltpu.SMEM((2, group), jnp.int32),
         ],
         compiler_params=params(16),
         cost_estimate=cost(8 * 10**9, 4 * 10**6),
         name="attention",
-    )(lam, prev, own, following)
+    )(lam, queries, prev, own, following)
 
 
 def project_kernel(
@@ -234,7 +232,7 @@
     _, tokens, _ = heads.shape
     depth, width = out_weight.shape
     rows = jax.ShapeDtypeStruct((slots, width), BF)
-    mixed = jax.ShapeDtypeStruct((tokens, width), BF)
+    mixed = pltpu.HBM((tokens, width), BF)
     scratch = [
         pltpu.VMEM((tokens, depth), BF),
         pltpu.VMEM((depth, width), BF),
@@ -421,9 +419,10 @@
 
     value_dim = value_rows.shape[1] // heads
     id_rows = jnp.broadcast_to((documents + 1).astype(BF)[None, :], (16, length))
-    packed = pack(query_rows, key_rows, value_rows, id_rows, heads)
-    packed = lax.all_to_all(packed, "sp", 0, 0, tiled=True, axis_index_groups=planes)
-    pairs = packed[:, : length + 16]
+    pairs = pack(key_rows, value_rows, id_rows, heads)
+    pairs = lax.all_to_all(pairs, "sp", 0, 0, tiled=True, axis_index_groups=planes)
+    queries = jnp.moveaxis(query_rows.reshape(length, heads, value_dim), 1, 0)
+    queries = lax.all_to_all(queries, "sp", 0, 0, tiled=True, axis_index_groups=planes)
     prev = lax.ppermute(
         pairs[heads - REACH :], "sp", [(i, i + heads) for i in range(count - heads)]
     )
@@ -441,7 +440,7 @@
     other = tuple(lax.ppermute(weight, "tp", swap) for weight in own)
 
     lam = lax.dynamic_slice(mix_lambda, (here % heads,), (1,))
-    outs = attention(lam, prev, packed, following, length, value_dim)
+    outs = attention(lam, queries, prev, pairs, following)
     outs = outs.reshape(heads * twins, length // twins, value_dim)
     both = [[g * heads * twins + j for j in range(heads * twins)] for g in range(count // heads)]
     token_heads = lax.all_to_all(

time: 176 us -> 175 us (level)
  waiting for transfers between devices: 75.9 us -> 71.9 us
  starting transfers between devices: 52.1 us -> 55.8 us
  Pallas kernels: 44.5 us -> 42.5 us
    all_to_all x1 -> x2, waiting for transfers between devices: 9.34 us -> 5.93 us  [the longest x1 5.92 us: on_device(): lax.all_to_all(pairs, 'sp', 0, 0, tiled=True, axis_index_groups=planes)]
    all_to_all x1 -> x2, starting transfers between devices: 5.19 us -> 8.6 us  [the longest x1 5.19 us: on_device(): lax.all_to_all(pairs, 'sp', 0, 0, tiled=True, axis_index_groups=planes)]
    pallas_call x2, Pallas kernels: 11.2 us -> 9.29 us  [the longest x1 7.3 us: attention(): pl.pallas_call(attention_kernel, grid=(group,), in_specs=[SM] + [VM] * 4,...]
  transfers between devices with their start and end apart: 15 -> 16, of which waited for: 10 -> 10; matrix products, arithmetic and copies ran while one was open for 1% -> 2% of each run, Pallas kernels for 23% -> 22%
where the time goes in v4:
time: 175 us; the launch traced here: 174 us
  waiting for transfers between devices  71.9 us (41%)
  starting transfers between devices  55.8 us (32%)
  Pallas kernels  42.5 us (24%)
  local copies, waits for them, and re-layouts  2.7 us (2%)
    all_to_all x4, starting transfers between devices, exchange(): lax.all_to_all(rows, 'sp', 0, 0, tiled=True, axis_index_groups=halves)  28.8 us
    all_to_all x4, waiting for transfers between devices, exchange(): lax.all_to_all(rows, 'sp', 0, 0, tiled=True, axis_index_groups=halves)  23.1 us
    pallas_call x2, Pallas kernels, experts_of(): pl.pallas_call(functools.partial(expert_kernel, tile=tile), in_specs=[VM]...  23 us
    ppermute x1, waiting for transfers between devices, on_device(): part = lax.ppermute(part_far, 'sp', mirror)  12.4 us
    ppermute x1, waiting for transfers between devices, on_device(): meta_far = lax.ppermute(meta_far, 'sp', mirror)  12.3 us
    ppermute x1, waiting for transfers between devices, on_device(): heads_far = lax.ppermute(token_heads, 'sp', mirror)  8.5 us
    pallas_call x2, Pallas kernels, project(): pl.pallas_call(functools.partial(project_kernel, tile=tile), in_specs=[VM...  8.18 us
    pallas_call x1, Pallas kernels, attention(): pl.pallas_call(attention_kernel, grid=(group,), in_specs=[SM] + [VM] * 4,...  7.3 us
  transfers between devices with their start and end apart: 16, of which 10 were waited for; matrix products, arithmetic and copies ran while one was open for 2% of the time, Pallas kernels for 22%

profile of v4, /device:TPU:0, one launch (start us, length us, event | category | flops | bytes accessed | tf_op | source)
XLA Modules:
  0.0 174.1 jit_solution(5714550583953843097)
XLA Ops:
  2.7 5.2 %all-to-all-start.1 = ((bf16[4,272,256]{2,1,0:T(8,128)(2,1)}), bf16[4,272,256]{2,1,0:T(8,128)(2,1)S(1)}, u32[]{:S(2)}, u32[]{:S(2)}) async-start(bf16[4,272,256]{2,1,0:T(8,128)(2,1)} %pack.1), calls=%async_computation.1 | async-start | bytes 1114112 | tf_op jit(solution)/shard_map/all_to_all | solution.py:423
  10.3 5.9 %all-to-all-done.1.own_ref = bf16[4,272,256]{2,1,0:T(8,128)(2,1)S(1)} async-done(((bf16[4,272,256]{2,1,0:T(8,128)(2,1)}), bf16[4,272,256]{2,1,0:T(8,128)(2,1)S(1)}, u32[]{:S(2)}, u32[]{:S(2)}) %all-to-all-start.1) | async-done | bytes 557088 | tf_op jit(solution)/shard_map/all_to_all | solution.py:423
  16.3 3.4 %all-to-all-start = ((bf16[4,256,128]{2,1,0:T(8,128)(2,1)}), bf16[4,256,128]{2,1,0:T(8,128)(2,1)S(1)}, u32[]{:S(2)}, u32[]{:S(2)}) async-start(bf16[4,256,128]{2,1,0:T(8,128)(2,1)} %bitcast.3), calls=%async_computation | async-start | bytes 524288 | tf_op jit(solution)/shard_map/all_to_all | solution.py:425
  19.7 3.5 %collective-permute-start = (bf16[3,272,256]{2,1,0:T(8,128)(2,1)S(1)}, bf16[3,272,256]{2,1,0:T(8,128)(2,1)S(1)}, u32[]{:S(2)}, u32[]{:S(2)}) collective-permute-start(bf16[3,272,256]{2,1,0:T(8,128)(2,1)S(1)} %get-tuple-element.16), channel_id=1, source_target_pairs={{0,8},{2,10},{4,12},{6,14},{8,16},{10,18},{12,20},{14,22},{16,24},... | collective-permute-start | bytes 1253384 | tf_op jit(solution)/shard_map/ppermute | solution.py:426
  25.4 5.7 %collective-permute-done.prev_ref = bf16[3,272,256]{2,1,0:T(8,128)(2,1)S(1)} collective-permute-done((bf16[3,272,256]{2,1,0:T(8,128)(2,1)S(1)}, bf16[3,272,256]{2,1,0:T(8,128)(2,1)S(1)}, u32[]{:S(2)}, u32[]{:S(2)}) %collective-permute-start) | collective-permute-done | bytes 417824 | tf_op jit(solution)/shard_map/ppermute | solution.py:426
  31.0 4.1 %collective-permute-done.1.next_ref = bf16[3,272,256]{2,1,0:T(8,128)(2,1)S(1)} collective-permute-done((bf16[3,272,256]{2,1,0:T(8,128)(2,1)S(1)}, bf16[3,272,256]{2,1,0:T(8,128)(2,1)S(1)}, u32[]{:S(2)}, u32[]{:S(2)}) %collective-permute-start.1) | collective-permute-done | bytes 417824 | tf_op jit(solution)/shard_map/ppermute | solution.py:429
  35.2 7.3 %attention.1 = bf16[4,256,128]{2,1,0:T(8,128)(2,1)} custom-call(f32[1]{0:T(128)} %dynamic_slice.3.lam_ref, bf16[4,256,128]{2,1,0:T(8,128)(2,1)S(1)} %all-to-all-done.q_ref, bf16[3,272,256]{2,1,0:T(8,128)(2,1)S(1)} %collective-permute-done.prev_ref, bf16[4,272,256]{2,1,0:T(8,128)(2,1)S(1)} %all-to-all-done.1.own_ref, ...), custom_call_target="tpu_custom_call" | custom-call | flops 8000000000 | bytes 4000000 | tf_op jit(solution)/shard_map/attention/pallas_call | solution.py:161
  42.5 3.9 %all-to-all-start.2 = ((bf16[8,128,128]{2,1,0:T(8,128)(2,1)}), bf16[8,128,128]{2,1,0:T(8,128)(2,1)S(1)}, u32[]{:S(2)}, u32[]{:S(2)}) async-start(bf16[8,128,128]{2,1,0:T(8,128)(2,1)} %bitcast.4), calls=%async_computation.2 | async-start | bytes 524288 | tf_op jit(solution)/shard_map/all_to_all | solution.py:446
  47.7 2.7 %collective-permute-start.5 = (f32[8,128]{1,0:T(8,128)S(1)}, f32[8,128]{1,0:T(8,128)S(1)}, u32[]{:S(2)}, u32[]{:S(2)}) collective-permute-start(f32[8,128]{1,0:T(8,128)S(1)} %get-tuple-element.19), channel_id=1, source_target_pairs={{0,24},{2,26},{4,28},{6,30},{8,16},{10,18},{12,20},{14,22},{16,8},... | collective-permute-start | bytes 12296 | tf_op jit(solution)/shard_map/ppermute | solution.py:435
  50.4 12.3 %collective-permute-done.5.meta_ref = f32[8,128]{1,0:T(8,128)S(1)} collective-permute-done((f32[8,128]{1,0:T(8,128)S(1)}, f32[8,128]{1,0:T(8,128)S(1)}, u32[]{:S(2)}, u32[]{:S(2)}) %collective-permute-start.5) | collective-permute-done | bytes 4128 | tf_op jit(solution)/shard_map/ppermute | solution.py:435
  63.8 8.5 %collective-permute-done.6.heads_ref = bf16[8,128,128]{2,1,0:T(8,128)(2,1)S(1)} collective-permute-done((bf16[8,128,128]{2,1,0:T(8,128)(2,1)S(1)}, bf16[8,128,128]{2,1,0:T(8,128)(2,1)S(1)}, u32[]{:S(2)}, u32[]{:S(2)}) %collective-permute-start.6) | collective-permute-done | bytes 262176 | tf_op jit(solution)/shard_map/ppermute | solution.py:449
  72.3 4.1 %shard_map.129 = bf16[256,2048]{1,0:T(8,128)(2,1)} custom-call(bf16[8,128,128]{2,1,0:T(8,128)(2,1)S(1)} %collective-permute-done.6.heads_ref, bf16[128,2048]{1,0:T(8,128)(2,1)S(1)} %collective-permute-done.7.residual_ref, f32[1,2048]{1,0:T(1,128)S(1)} %bitcast.25, f32[8,128]{1,0:T(8,128)S(1)} %collective-permute-done.5.meta_ref, bf16[1024,2048]{1,0:T(8,128)(2,1)} %weight_ref.3), custom_call_target="tpu_custom_call" | custom-call | flops 3000000000 | bytes 8000000 | tf_op jit(solution)/shard_map/pallas_call | solution.py:241
  76.5 17.8 %all-to-all-start.5 = ((bf16[8,32,2048]{2,1,0:T(8,128)(2,1)}), bf16[8,32,2048]{2,1,0:T(8,128)(2,1)S(1)}, u32[]{:S(2)}, u32[]{:S(2)}) async-start(bf16[8,32,2048]{2,1,0:T(8,128)(2,1)} %bitcast.14), calls=%async_computation.5 | async-start | bytes 2097152 | tf_op jit(solution)/shard_map/all_to_all | solution.py:456
  94.2 4.1 %shard_map.127 = (bf16[256,2048]{1,0:T(8,128)(2,1)}, bf16[128,2048]{1,0:T(8,128)(2,1)}) custom-call(bf16[8,128,128]{2,1,0:T(8,128)(2,1)S(1)} %all-to-all-done.2.heads_ref, bf16[128,2048]{1,0:T(8,128)(2,1)S(1)} %copy-done, f32[1,2048]{1,0:T(1,128)S(1)} %bitcast.26, f32[8,128]{1,0:T(8,128)S(1)} %get-tuple-element.20.meta_ref, bf16[1024,2048]{1,0:T(8,128)(2,1)} %weight_ref.3), custom_call_target="tpu_custom_call" | custom-call | flops 3000000000 | bytes 8000000 | tf_op jit(solution)/shard_map/pallas_call | solution.py:241
  98.3 9.2 %all-to-all-done.5 = bf16[8,32,2048]{2,1,0:T(8,128)(2,1)S(1)} async-done(((bf16[8,32,2048]{2,1,0:T(8,128)(2,1)}), bf16[8,32,2048]{2,1,0:T(8,128)(2,1)S(1)}, u32[]{:S(2)}, u32[]{:S(2)}) %all-to-all-start.5) | async-done | bytes 1048608 | tf_op jit(solution)/shard_map/all_to_all | solution.py:456
  107.5 3.7 %all-to-all-start.3 = ((bf16[8,32,2048]{2,1,0:T(8,128)(2,1)}), bf16[8,32,2048]{2,1,0:T(8,128)(2,1)S(1)}, u32[]{:S(2)}, u32[]{:S(2)}) async-start(bf16[8,32,2048]{2,1,0:T(8,128)(2,1)} %bitcast.6), calls=%async_computation.3 | async-start | bytes 2097152 | tf_op jit(solution)/shard_map/all_to_all | solution.py:456
  111.3 11.5 %shard_map.130 = bf16[256,2048]{1,0:T(8,128)(2,1)} custom-call(bf16[256,2048]{1,0:T(8,128)(2,1)S(1)} %bitcast.21, bf16[2048,1024]{1,0:T(8,128)(2,1)} %bitcast.30, bf16[2048,1024]{1,0:T(8,128)(2,1)} %bitcast.33, bf16[1024,2048]{1,0:T(8,128)(2,1)} %bitcast.36, bf16[2048,1024]{1,0:T(8,128)(2,1)} %collective-permute-done.2.g1, ...), custom_call_target="tpu_custom_call" | custom-call | flops 8999999488 | bytes 26000000 | tf_op jit(solution)/shard_map/pallas_call | solution.py:303
  125.1 3.8 %all-to-all-start.6 = ((bf16[8,32,2048]{2,1,0:T(8,128)(2,1)}), bf16[8,32,2048]{2,1,0:T(8,128)(2,1)S(1)}, u32[]{:S(2)}, u32[]{:S(2)}) async-start(bf16[8,32,2048]{2,1,0:T(8,128)(2,1)} %bitcast.16), calls=%async_computation.6 | async-start | bytes 2097152 | tf_op jit(solution)/shard_map/all_to_all | solution.py:456
  128.9 11.5 %shard_map.128 = bf16[256,2048]{1,0:T(8,128)(2,1)} custom-call(bf16[256,2048]{1,0:T(8,128)(2,1)S(1)} %bitcast.22, bf16[2048,1024]{1,0:T(8,128)(2,1)} %bitcast.31, bf16[2048,1024]{1,0:T(8,128)(2,1)} %bitcast.34, bf16[1024,2048]{1,0:T(8,128)(2,1)} %bitcast.37, bf16[2048,1024]{1,0:T(8,128)(2,1)} %collective-permute-done.2.g1, ...), custom_call_target="tpu_custom_call" | custom-call | flops 8999999488 | bytes 26000000 | tf_op jit(solution)/shard_map/pallas_call | solution.py:303
  140.3 2.3 %all-to-all-done.6 = bf16[8,32,2048]{2,1,0:T(8,128)(2,1)S(1)} async-done(((bf16[8,32,2048]{2,1,0:T(8,128)(2,1)}), bf16[8,32,2048]{2,1,0:T(8,128)(2,1)S(1)}, u32[]{:S(2)}, u32[]{:S(2)}) %all-to-all-start.6) | async-done | bytes 1048608 | tf_op jit(solution)/shard_map/all_to_all | solution.py:456
  142.7 3.6 %all-to-all-start.4 = ((bf16[8,32,2048]{2,1,0:T(8,128)(2,1)}), bf16[8,32,2048]{2,1,0:T(8,128)(2,1)S(1)}, u32[]{:S(2)}, u32[]{:S(2)}) async-start(bf16[8,32,2048]{2,1,0:T(8,128)(2,1)} %bitcast.11), calls=%async_computation.4 | async-start | bytes 2097152 | tf_op jit(solution)/shard_map/all_to_all | solution.py:456
  146.8 4.2 %collective-permute-start.8 = (bf16[128,2048]{1,0:T(8,128)(2,1)S(1)}, bf16[128,2048]{1,0:T(8,128)(2,1)S(1)}, u32[]{:S(2)}, u32[]{:S(2)}) collective-permute-start(bf16[128,2048]{1,0:T(8,128)(2,1)S(1)} %partial_sum.1), channel_id=1, source_target_pairs={{0,24},{2,26},{4,28},{6,30},{8,16},{10,18},{12,20},{14,22},{16,8},... | collective-permute-start | bytes 1572872 | tf_op jit(solution)/shard_map/ppermute | solution.py:467
  150.9 9.3 %all-to-all-done.4 = bf16[8,32,2048]{2,1,0:T(8,128)(2,1)S(1)} async-done(((bf16[8,32,2048]{2,1,0:T(8,128)(2,1)}), bf16[8,32,2048]{2,1,0:T(8,128)(2,1)S(1)}, u32[]{:S(2)}, u32[]{:S(2)}) %all-to-all-start.4) | async-done | bytes 1048608 | tf_op jit(solution)/shard_map/all_to_all | solution.py:456
  160.3 12.4 %collective-permute-done.8.far_ref = bf16[128,2048]{1,0:T(8,128)(2,1)S(1)} collective-permute-done((bf16[128,2048]{1,0:T(8,128)(2,1)S(1)}, bf16[128,2048]{1,0:T(8,128)(2,1)S(1)}, u32[]{:S(2)}, u32[]{:S(2)}) %collective-permute-start.8) | collective-permute-done | bytes 524320 | tf_op jit(solution)/shard_map/ppermute | solution.py:467
  (41 shorter events, 14.1 us)
Async XLA Ops:
  0.0 24.6 %copy-start.3 = (s32[128,2]{0,1:T(2,128)S(1)}, s32[128,2]{0,1:T(2,128)}, u32[]{:S(2)}) copy-start(s32[128,2]{0,1:T(2,128)} %param.24) | copy-start | bytes 3076
  0.0 24.7 %copy-start.5 = (f32[4]{0:T(128)S(1)}, f32[4]{0:T(128)}, u32[]{:S(2)}) copy-start(f32[4]{0:T(128)} %param.17) | copy-start | bytes 52
  2.7 13.6 %all-to-all-start.1 = ((bf16[4,272,256]{2,1,0:T(8,128)(2,1)}), bf16[4,272,256]{2,1,0:T(8,128)(2,1)S(1)}, u32[]{:S(2)}, u32[]{:S(2)}) async-start(bf16[4,272,256]{2,1,0:T(8,128)(2,1)} %pack.1), calls=%async_computation.1 | async-start | bytes 1114112 | tf_op jit(solution)/shard_map/all_to_all | solution.py:423
  7.9 103.4 %collective-permute-start.2 = (bf16[2048,1024]{1,0:T(8,128)(2,1)}, bf16[2048,1024]{1,0:T(8,128)(2,1)}, u32[]{:S(2)}, u32[]{:S(2)}) collective-permute-start(bf16[2048,1024]{1,0:T(8,128)(2,1)} %bitcast.29), channel_id=1, source_target_pairs={{0,1},{1,0},{2,3},{3,2},{4,5},{5,4},{6,7},{7,6},{8,9},{9,8},{10,11... | collective-permute-start | bytes 12582920 | tf_op jit(solution)/shard_map/ppermute | solution.py:440
  7.9 103.4 %collective-permute-start.3 = (bf16[2048,1024]{1,0:T(8,128)(2,1)}, bf16[2048,1024]{1,0:T(8,128)(2,1)}, u32[]{:S(2)}, u32[]{:S(2)}) collective-permute-start(bf16[2048,1024]{1,0:T(8,128)(2,1)} %bitcast.32), channel_id=1, source_target_pairs={{0,1},{1,0},{2,3},{3,2},{4,5},{5,4},{6,7},{7,6},{8,9},{9,8},{10,11... | collective-permute-start | bytes 12582920 | tf_op jit(solution)/shard_map/ppermute | solution.py:440
  8.4 102.9 %collective-permute-start.4 = (bf16[1024,2048]{1,0:T(8,128)(2,1)}, bf16[1024,2048]{1,0:T(8,128)(2,1)}, u32[]{:S(2)}, u32[]{:S(2)}) collective-permute-start(bf16[1024,2048]{1,0:T(8,128)(2,1)} %bitcast.35), channel_id=1, source_target_pairs={{0,1},{1,0},{2,3},{3,2},{4,5},{5,4},{6,7},{7,6},{8,9},{9,8},{10,11... | collective-permute-start | bytes 12582920 | tf_op jit(solution)/shard_map/ppermute | solution.py:440
  16.3 18.9 %all-to-all-start = ((bf16[4,256,128]{2,1,0:T(8,128)(2,1)}), bf16[4,256,128]{2,1,0:T(8,128)(2,1)S(1)}, u32[]{:S(2)}, u32[]{:S(2)}) async-start(bf16[4,256,128]{2,1,0:T(8,128)(2,1)} %bitcast.3), calls=%async_computation | async-start | bytes 524288 | tf_op jit(solution)/shard_map/all_to_all | solution.py:425
  19.7 11.3 %collective-permute-start = (bf16[3,272,256]{2,1,0:T(8,128)(2,1)S(1)}, bf16[3,272,256]{2,1,0:T(8,128)(2,1)S(1)}, u32[]{:S(2)}, u32[]{:S(2)}) collective-permute-start(bf16[3,272,256]{2,1,0:T(8,128)(2,1)S(1)} %get-tuple-element.16), channel_id=1, source_target_pairs={{0,8},{2,10},{4,12},{6,14},{8,16},{10,18},{12,20},{14,22},{16,24},... | collective-permute-start | bytes 1253384 | tf_op jit(solution)/shard_map/ppermute | solution.py:426
  23.3 11.9 %collective-permute-start.1 = (bf16[3,272,256]{2,1,0:T(8,128)(2,1)S(1)}, bf16[3,272,256]{2,1,0:T(8,128)(2,1)S(1)}, u32[]{:S(2)}, u32[]{:S(2)}) collective-permute-start(bf16[3,272,256]{2,1,0:T(8,128)(2,1)S(1)} %get-tuple-element.15), channel_id=1, source_target_pairs={{8,0},{10,2},{12,4},{14,6},{16,8},{18,10},{20,12},{22,14},{24,16},... | collective-permute-start | bytes 1253384 | tf_op jit(solution)/shard_map/ppermute | solution.py:429
  25.4 21.0 %copy-start = (bf16[128,2048]{1,0:T(8,128)(2,1)S(1)}, bf16[128,2048]{1,0:T(8,128)(2,1)}, u32[]{:S(2)}) copy-start(bf16[128,2048]{1,0:T(8,128)(2,1)} %residual_ref.1) | copy-start | bytes 1572868
  25.4 22.3 %copy-start.4 = (f32[128,2]{0,1:T(2,128)S(1)}, f32[128,2]{0,1:T(2,128)}, u32[]{:S(2)}) copy-start(f32[128,2]{0,1:T(2,128)} %param.25) | copy-start | bytes 3076
  25.4 47.0 %copy-start.1 = (f32[2048]{0:T(1024)S(1)}, f32[2048]{0:T(1024)}, u32[]{:S(2)}) copy-start(f32[2048]{0:T(1024)} %param.20) | copy-start | bytes 24580
  42.5 20.2 %all-to-all-start.2 = ((bf16[8,128,128]{2,1,0:T(8,128)(2,1)}), bf16[8,128,128]{2,1,0:T(8,128)(2,1)S(1)}, u32[]{:S(2)}, u32[]{:S(2)}) async-start(bf16[8,128,128]{2,1,0:T(8,128)(2,1)} %bitcast.4), calls=%async_computation.2 | async-start | bytes 524288 | tf_op jit(solution)/shard_map/all_to_all | solution.py:446
  46.4 26.0 %collective-permute-start.7 = (bf16[128,2048]{1,0:T(8,128)(2,1)S(1)}, bf16[128,2048]{1,0:T(8,128)(2,1)S(1)}, u32[]{:S(2)}, u32[]{:S(2)}) collective-permute-start(bf16[128,2048]{1,0:T(8,128)(2,1)S(1)} %copy-done), channel_id=1, source_target_pairs={{0,24},{2,26},{4,28},{6,30},{8,16},{10,18},{12,20},{14,22},{16,8},... | collective-permute-start | bytes 1572872 | tf_op jit(solution)/shard_map/ppermute | solution.py:437
  47.7 15.0 %collective-permute-start.5 = (f32[8,128]{1,0:T(8,128)S(1)}, f32[8,128]{1,0:T(8,128)S(1)}, u32[]{:S(2)}, u32[]{:S(2)}) collective-permute-start(f32[8,128]{1,0:T(8,128)S(1)} %get-tuple-element.19), channel_id=1, source_target_pairs={{0,24},{2,26},{4,28},{6,30},{8,16},{10,18},{12,20},{14,22},{16,8},... | collective-permute-start | bytes 12296 | tf_op jit(solution)/shard_map/ppermute | solution.py:435
  62.7 9.6 %collective-permute-start.6 = (bf16[8,128,128]{2,1,0:T(8,128)(2,1)S(1)}, bf16[8,128,128]{2,1,0:T(8,128)(2,1)S(1)}, u32[]{:S(2)}, u32[]{:S(2)}) collective-permute-start(bf16[8,128,128]{2,1,0:T(8,128)(2,1)S(1)} %all-to-all-done.2.heads_ref), channel_id=1, source_target_pairs={{0,24},{2,26},{4,28},{6,30},{8,16},{10,18},{12,20},{14,22},{16,8},... | collective-permute-start | bytes 786440 | tf_op jit(solution)/shard_map/ppermute | solution.py:449
  76.5 31.1 %all-to-all-start.5 = ((bf16[8,32,2048]{2,1,0:T(8,128)(2,1)}), bf16[8,32,2048]{2,1,0:T(8,128)(2,1)S(1)}, u32[]{:S(2)}, u32[]{:S(2)}) async-start(bf16[8,32,2048]{2,1,0:T(8,128)(2,1)} %bitcast.14), calls=%async_computation.5 | async-start | bytes 2097152 | tf_op jit(solution)/shard_map/all_to_all | solution.py:456
  107.5 17.5 %all-to-all-start.3 = ((bf16[8,32,2048]{2,1,0:T(8,128)(2,1)}), bf16[8,32,2048]{2,1,0:T(8,128)(2,1)S(1)}, u32[]{:S(2)}, u32[]{:S(2)}) async-start(bf16[8,32,2048]{2,1,0:T(8,128)(2,1)} %bitcast.6), calls=%async_computation.3 | async-start | bytes 2097152 | tf_op jit(solution)/shard_map/all_to_all | solution.py:456
  125.1 17.6 %all-to-all-start.6 = ((bf16[8,32,2048]{2,1,0:T(8,128)(2,1)}), bf16[8,32,2048]{2,1,0:T(8,128)(2,1)S(1)}, u32[]{:S(2)}, u32[]{:S(2)}) async-start(bf16[8,32,2048]{2,1,0:T(8,128)(2,1)} %bitcast.16), calls=%async_computation.6 | async-start | bytes 2097152 | tf_op jit(solution)/shard_map/all_to_all | solution.py:456
  140.3 32.3 %copy-start.2 = (bf16[128,2048]{1,0:T(8,128)(2,1)S(1)}, bf16[128,2048]{1,0:T(8,128)(2,1)}, u32[]{:S(2)}) copy-start(bf16[128,2048]{1,0:T(8,128)(2,1)} %get-tuple-element.13.mixed_ref) | copy-start | bytes 1572868
  142.7 17.6 %all-to-all-start.4 = ((bf16[8,32,2048]{2,1,0:T(8,128)(2,1)}), bf16[8,32,2048]{2,1,0:T(8,128)(2,1)S(1)}, u32[]{:S(2)}, u32[]{:S(2)}) async-start(bf16[8,32,2048]{2,1,0:T(8,128)(2,1)} %bitcast.11), calls=%async_computation.4 | async-start | bytes 2097152 | tf_op jit(solution)/shard_map/all_to_all | solution.py:456
  146.8 25.8 %collective-permute-start.8 = (bf16[128,2048]{1,0:T(8,128)(2,1)S(1)}, bf16[128,2048]{1,0:T(8,128)(2,1)S(1)}, u32[]{:S(2)}, u32[]{:S(2)}) collective-permute-start(bf16[128,2048]{1,0:T(8,128)(2,1)S(1)} %partial_sum.1), channel_id=1, source_target_pairs={{0,24},{2,26},{4,28},{6,30},{8,16},{10,18},{12,20},{14,22},{16,8},... | collective-permute-start | bytes 1572872 | tf_op jit(solution)/shard_map/ppermute | solution.py:467

commit v5 on v4

--- a/solution.py
+++ b/solution.py
@@ -31,17 +31,18 @@
 
 
 def pack_kernel(k_ref, v_ref, id_ref, o_ref):
-    heads, _, width = o_ref.shape
+    heads, rows, width = o_ref.shape
     length = k_ref.shape[0]
     part = width // 2
+    ids = jnp.broadcast_to((id_ref[...] + 1).astype(F32)[None, :], (rows - length, width)).astype(BF)
     for h in range(heads):
         columns = slice(h * part, (h + 1) * part)
         o_ref[h, :length, :part] = k_ref[:, columns]
         o_ref[h, :length, part:] = v_ref[:, columns]
-        o_ref[h, length:, :] = id_ref[...]
-
-
-def pack(key_rows, value_rows, id_rows, heads):
+        o_ref[h, length:, :] = ids
+
+
+def pack(key_rows, value_rows, documents, heads):
     length = key_rows.shape[0]
     width = key_rows.shape[1] // heads
     return pl.pallas_call(
@@ -51,7 +52,7 @@
         out_shape=jax.ShapeDtypeStruct((heads, length + 16, 2 * width), BF),
         compiler_params=params(8),
         name="pack",
-    )(in_hbm(key_rows), in_hbm(value_rows), id_rows)
+    )(in_hbm(key_rows), in_hbm(value_rows), in_hbm(documents))
 
 
 def attention_kernel(
@@ -418,8 +419,7 @@
     swap = [(i, twins - 1 - i) for i in range(twins)]
 
     value_dim = value_rows.shape[1] // heads
-    id_rows = jnp.broadcast_to((documents + 1).astype(BF)[None, :], (16, length))
-    pairs = pack(key_rows, value_rows, id_rows, heads)
+    pairs = pack(key_rows, value_rows, documents, heads)
     pairs = lax.all_to_all(pairs, "sp", 0, 0, tiled=True, axis_index_groups=planes)
     queries = jnp.moveaxis(query_rows.reshape(length, heads, value_dim), 1, 0)
     queries = lax.all_to_all(queries, "sp", 0, 0, tiled=True, axis_index_groups=planes)
@@ -433,7 +433,7 @@
     meta_own = meta_of(routes, ranks, route_weights, my_half * half, half, capacity)
     meta_far = meta_of(routes, ranks, route_weights, (1 - my_half) * half, half, capacity)
     meta_far = lax.ppermute(meta_far, "sp", mirror)
-    prev, following, residual_late = lax.optimization_barrier((prev, following, residual))
+    prev, residual_late = lax.optimization_barrier((prev, residual))
     residual_far = lax.ppermute(residual_late, "sp", mirror)
 
     own = (gate_weight[0], up_weight[0], down_weight[0])

time: 175 us -> 174 us (level)
  transfers between devices with their start and end apart: 16 -> 16, of which waited for: 10 -> 10; matrix products, arithmetic and copies ran while one was open for 2% -> 2% of each run, Pallas kernels for 22% -> 23%
where the time goes in v5:
time: 174 us; the launch traced here: 173 us
  waiting for transfers between devices  71.9 us (41%)
  starting transfers between devices  55.8 us (32%)
  Pallas kernels  42.5 us (24%)
  local copies, waits for them, and re-layouts  2.69 us (2%)
    all_to_all x4, starting transfers between devices, exchange(): lax.all_to_all(rows, 'sp', 0, 0, tiled=True, axis_index_groups=halves)  28.8 us
    all_to_all x4, waiting for transfers between devices, exchange(): lax.all_to_all(rows, 'sp', 0, 0, tiled=True, axis_index_groups=halves)  23.1 us
    pallas_call x2, Pallas kernels, experts_of(): pl.pallas_call(functools.partial(expert_kernel, tile=tile), in_specs=[VM]...  23 us
    ppermute x1, waiting for transfers between devices, on_device(): part = lax.ppermute(part_far, 'sp', mirror)  12.4 us
    ppermute x1, waiting for transfers between devices, on_device(): meta_far = lax.ppermute(meta_far, 'sp', mirror)  12.3 us
    ppermute x1, waiting for transfers between devices, on_device(): heads_far = lax.ppermute(token_heads, 'sp', mirror)  8.5 us
    pallas_call x2, Pallas kernels, project(): pl.pallas_call(functools.partial(project_kernel, tile=tile), in_specs=[VM...  8.19 us
    pallas_call x1, Pallas kernels, attention(): pl.pallas_call(attention_kernel, grid=(group,), in_specs=[SM] + [VM] * 4,...  7.3 us
  transfers between devices with their start and end apart: 16, of which 10 were waited for; matrix products, arithmetic and copies ran while one was open for 2% of the time, Pallas kernels for 23%

profile of v5, /device:TPU:0, one launch (start us, length us, event | category | flops | bytes accessed | tf_op | source)
XLA Modules:
  0.0 173.4 jit_solution(10785747857040097377)
XLA Ops:
  2.0 5.2 %all-to-all-start.1 = ((bf16[4,272,256]{2,1,0:T(8,128)(2,1)}), bf16[4,272,256]{2,1,0:T(8,128)(2,1)S(1)}, u32[]{:S(2)}, u32[]{:S(2)}) async-start(bf16[4,272,256]{2,1,0:T(8,128)(2,1)} %pack.1), calls=%async_computation.1 | async-start | bytes 1114112 | tf_op jit(solution)/shard_map/all_to_all | solution.py:423
  9.7 5.9 %all-to-all-done.1.own_ref = bf16[4,272,256]{2,1,0:T(8,128)(2,1)S(1)} async-done(((bf16[4,272,256]{2,1,0:T(8,128)(2,1)}), bf16[4,272,256]{2,1,0:T(8,128)(2,1)S(1)}, u32[]{:S(2)}, u32[]{:S(2)}) %all-to-all-start.1) | async-done | bytes 557088 | tf_op jit(solution)/shard_map/all_to_all | solution.py:423
  15.6 3.4 %all-to-all-start = ((bf16[4,256,128]{2,1,0:T(8,128)(2,1)}), bf16[4,256,128]{2,1,0:T(8,128)(2,1)S(1)}, u32[]{:S(2)}, u32[]{:S(2)}) async-start(bf16[4,256,128]{2,1,0:T(8,128)(2,1)} %bitcast.3), calls=%async_computation | async-start | bytes 524288 | tf_op jit(solution)/shard_map/all_to_all | solution.py:425
  19.1 3.5 %collective-permute-start = (bf16[3,272,256]{2,1,0:T(8,128)(2,1)S(1)}, bf16[3,272,256]{2,1,0:T(8,128)(2,1)S(1)}, u32[]{:S(2)}, u32[]{:S(2)}) collective-permute-start(bf16[3,272,256]{2,1,0:T(8,128)(2,1)S(1)} %get-tuple-element.14), channel_id=1, source_target_pairs={{0,8},{2,10},{4,12},{6,14},{8,16},{10,18},{12,20},{14,22},{16,24},... | collective-permute-start | bytes 1253384 | tf_op jit(solution)/shard_map/ppermute | solution.py:426
  24.7 5.7 %collective-permute-done.prev_ref = bf16[3,272,256]{2,1,0:T(8,128)(2,1)S(1)} collective-permute-done((bf16[3,272,256]{2,1,0:T(8,128)(2,1)S(1)}, bf16[3,272,256]{2,1,0:T(8,128)(2,1)S(1)}, u32[]{:S(2)}, u32[]{:S(2)}) %collective-permute-start) | collective-permute-done | bytes 417824 | tf_op jit(solution)/shard_map/ppermute | solution.py:426
  30.4 4.1 %collective-permute-done.1.next_ref = bf16[3,272,256]{2,1,0:T(8,128)(2,1)S(1)} collective-permute-done((bf16[3,272,256]{2,1,0:T(8,128)(2,1)S(1)}, bf16[3,272,256]{2,1,0:T(8,128)(2,1)S(1)}, u32[]{:S(2)}, u32[]{:S(2)}) %collective-permute-start.1) | collective-permute-done | bytes 417824 | tf_op jit(solution)/shard_map/ppermute | solution.py:429
  34.5 7.3 %attention.1 = bf16[4,256,128]{2,1,0:T(8,128)(2,1)} custom-call(f32[1]{0:T(128)} %dynamic_slice.3.lam_ref, bf16[4,256,128]{2,1,0:T(8,128)(2,1)S(1)} %all-to-all-done.q_ref, bf16[3,272,256]{2,1,0:T(8,128)(2,1)S(1)} %collective-permute-done.prev_ref, bf16[4,272,256]{2,1,0:T(8,128)(2,1)S(1)} %all-to-all-done.1.own_ref, ...), custom_call_target="tpu_custom_call" | custom-call | flops 8000000000 | bytes 4000000 | tf_op jit(solution)/shard_map/attention/pallas_call | solution.py:162
  41.8 3.9 %all-to-all-start.2 = ((bf16[8,128,128]{2,1,0:T(8,128)(2,1)}), bf16[8,128,128]{2,1,0:T(8,128)(2,1)S(1)}, u32[]{:S(2)}, u32[]{:S(2)}) async-start(bf16[8,128,128]{2,1,0:T(8,128)(2,1)} %bitcast.4), calls=%async_computation.2 | async-start | bytes 524288 | tf_op jit(solution)/shard_map/all_to_all | solution.py:446
  47.0 2.7 %collective-permute-start.5 = (f32[8,128]{1,0:T(8,128)S(1)}, f32[8,128]{1,0:T(8,128)S(1)}, u32[]{:S(2)}, u32[]{:S(2)}) collective-permute-start(f32[8,128]{1,0:T(8,128)S(1)} %get-tuple-element.17), channel_id=1, source_target_pairs={{0,24},{2,26},{4,28},{6,30},{8,16},{10,18},{12,20},{14,22},{16,8},... | collective-permute-start | bytes 12296 | tf_op jit(solution)/shard_map/ppermute | solution.py:435
  49.7 12.3 %collective-permute-done.5.meta_ref = f32[8,128]{1,0:T(8,128)S(1)} collective-permute-done((f32[8,128]{1,0:T(8,128)S(1)}, f32[8,128]{1,0:T(8,128)S(1)}, u32[]{:S(2)}, u32[]{:S(2)}) %collective-permute-start.5) | collective-permute-done | bytes 4128 | tf_op jit(solution)/shard_map/ppermute | solution.py:435
  63.1 8.5 %collective-permute-done.6.heads_ref = bf16[8,128,128]{2,1,0:T(8,128)(2,1)S(1)} collective-permute-done((bf16[8,128,128]{2,1,0:T(8,128)(2,1)S(1)}, bf16[8,128,128]{2,1,0:T(8,128)(2,1)S(1)}, u32[]{:S(2)}, u32[]{:S(2)}) %collective-permute-start.6) | collective-permute-done | bytes 262176 | tf_op jit(solution)/shard_map/ppermute | solution.py:449
  71.6 4.1 %shard_map.129 = bf16[256,2048]{1,0:T(8,128)(2,1)} custom-call(bf16[8,128,128]{2,1,0:T(8,128)(2,1)S(1)} %collective-permute-done.6.heads_ref, bf16[128,2048]{1,0:T(8,128)(2,1)S(1)} %collective-permute-done.7.residual_ref, f32[1,2048]{1,0:T(1,128)S(1)} %bitcast.25, f32[8,128]{1,0:T(8,128)S(1)} %collective-permute-done.5.meta_ref, bf16[1024,2048]{1,0:T(8,128)(2,1)} %weight_ref.3), custom_call_target="tpu_custom_call" | custom-call | flops 3000000000 | bytes 8000000 | tf_op jit(solution)/shard_map/pallas_call | solution.py:242
  75.8 17.8 %all-to-all-start.5 = ((bf16[8,32,2048]{2,1,0:T(8,128)(2,1)}), bf16[8,32,2048]{2,1,0:T(8,128)(2,1)S(1)}, u32[]{:S(2)}, u32[]{:S(2)}) async-start(bf16[8,32,2048]{2,1,0:T(8,128)(2,1)} %bitcast.14), calls=%async_computation.5 | async-start | bytes 2097152 | tf_op jit(solution)/shard_map/all_to_all | solution.py:456
  93.5 4.1 %shard_map.127 = (bf16[256,2048]{1,0:T(8,128)(2,1)}, bf16[128,2048]{1,0:T(8,128)(2,1)}) custom-call(bf16[8,128,128]{2,1,0:T(8,128)(2,1)S(1)} %all-to-all-done.2.heads_ref, bf16[128,2048]{1,0:T(8,128)(2,1)S(1)} %copy-done, f32[1,2048]{1,0:T(1,128)S(1)} %bitcast.26, f32[8,128]{1,0:T(8,128)S(1)} %get-tuple-element.18.meta_ref, bf16[1024,2048]{1,0:T(8,128)(2,1)} %weight_ref.3), custom_call_target="tpu_custom_call" | custom-call | flops 3000000000 | bytes 8000000 | tf_op jit(solution)/shard_map/pallas_call | solution.py:242
  97.6 9.2 %all-to-all-done.5 = bf16[8,32,2048]{2,1,0:T(8,128)(2,1)S(1)} async-done(((bf16[8,32,2048]{2,1,0:T(8,128)(2,1)}), bf16[8,32,2048]{2,1,0:T(8,128)(2,1)S(1)}, u32[]{:S(2)}, u32[]{:S(2)}) %all-to-all-start.5) | async-done | bytes 1048608 | tf_op jit(solution)/shard_map/all_to_all | solution.py:456
  106.8 3.7 %all-to-all-start.3 = ((bf16[8,32,2048]{2,1,0:T(8,128)(2,1)}), bf16[8,32,2048]{2,1,0:T(8,128)(2,1)S(1)}, u32[]{:S(2)}, u32[]{:S(2)}) async-start(bf16[8,32,2048]{2,1,0:T(8,128)(2,1)} %bitcast.6), calls=%async_computation.3 | async-start | bytes 2097152 | tf_op jit(solution)/shard_map/all_to_all | solution.py:456
  110.6 11.5 %shard_map.130 = bf16[256,2048]{1,0:T(8,128)(2,1)} custom-call(bf16[256,2048]{1,0:T(8,128)(2,1)S(1)} %bitcast.21, bf16[2048,1024]{1,0:T(8,128)(2,1)} %bitcast.30, bf16[2048,1024]{1,0:T(8,128)(2,1)} %bitcast.33, bf16[1024,2048]{1,0:T(8,128)(2,1)} %bitcast.36, bf16[2048,1024]{1,0:T(8,128)(2,1)} %collective-permute-done.2.g1, ...), custom_call_target="tpu_custom_call" | custom-call | flops 8999999488 | bytes 26000000 | tf_op jit(solution)/shard_map/pallas_call | solution.py:304
  124.4 3.8 %all-to-all-start.6 = ((bf16[8,32,2048]{2,1,0:T(8,128)(2,1)}), bf16[8,32,2048]{2,1,0:T(8,128)(2,1)S(1)}, u32[]{:S(2)}, u32[]{:S(2)}) async-start(bf16[8,32,2048]{2,1,0:T(8,128)(2,1)} %bitcast.16), calls=%async_computation.6 | async-start | bytes 2097152 | tf_op jit(solution)/shard_map/all_to_all | solution.py:456
  128.2 11.5 %shard_map.128 = bf16[256,2048]{1,0:T(8,128)(2,1)} custom-call(bf16[256,2048]{1,0:T(8,128)(2,1)S(1)} %bitcast.22, bf16[2048,1024]{1,0:T(8,128)(2,1)} %bitcast.31, bf16[2048,1024]{1,0:T(8,128)(2,1)} %bitcast.34, bf16[1024,2048]{1,0:T(8,128)(2,1)} %bitcast.37, bf16[2048,1024]{1,0:T(8,128)(2,1)} %collective-permute-done.2.g1, ...), custom_call_target="tpu_custom_call" | custom-call | flops 8999999488 | bytes 26000000 | tf_op jit(solution)/shard_map/pallas_call | solution.py:304
  139.6 2.3 %all-to-all-done.6 = bf16[8,32,2048]{2,1,0:T(8,128)(2,1)S(1)} async-done(((bf16[8,32,2048]{2,1,0:T(8,128)(2,1)}), bf16[8,32,2048]{2,1,0:T(8,128)(2,1)S(1)}, u32[]{:S(2)}, u32[]{:S(2)}) %all-to-all-start.6) | async-done | bytes 1048608 | tf_op jit(solution)/shard_map/all_to_all | solution.py:456
  142.0 3.6 %all-to-all-start.4 = ((bf16[8,32,2048]{2,1,0:T(8,128)(2,1)}), bf16[8,32,2048]{2,1,0:T(8,128)(2,1)S(1)}, u32[]{:S(2)}, u32[]{:S(2)}) async-start(bf16[8,32,2048]{2,1,0:T(8,128)(2,1)} %bitcast.11), calls=%async_computation.4 | async-start | bytes 2097152 | tf_op jit(solution)/shard_map/all_to_all | solution.py:456
  146.1 4.2 %collective-permute-start.8 = (bf16[128,2048]{1,0:T(8,128)(2,1)S(1)}, bf16[128,2048]{1,0:T(8,128)(2,1)S(1)}, u32[]{:S(2)}, u32[]{:S(2)}) collective-permute-start(bf16[128,2048]{1,0:T(8,128)(2,1)S(1)} %partial_sum.1), channel_id=1, source_target_pairs={{0,24},{2,26},{4,28},{6,30},{8,16},{10,18},{12,20},{14,22},{16,8},... | collective-permute-start | bytes 1572872 | tf_op jit(solution)/shard_map/ppermute | solution.py:467
  150.2 9.3 %all-to-all-done.4 = bf16[8,32,2048]{2,1,0:T(8,128)(2,1)S(1)} async-done(((bf16[8,32,2048]{2,1,0:T(8,128)(2,1)}), bf16[8,32,2048]{2,1,0:T(8,128)(2,1)S(1)}, u32[]{:S(2)}, u32[]{:S(2)}) %all-to-all-start.4) | async-done | bytes 1048608 | tf_op jit(solution)/shard_map/all_to_all | solution.py:456
  159.6 12.4 %collective-permute-done.8.far_ref = bf16[128,2048]{1,0:T(8,128)(2,1)S(1)} collective-permute-done((bf16[128,2048]{1,0:T(8,128)(2,1)S(1)}, bf16[128,2048]{1,0:T(8,128)(2,1)S(1)}, u32[]{:S(2)}, u32[]{:S(2)}) %collective-permute-start.8) | collective-permute-done | bytes 524320 | tf_op jit(solution)/shard_map/ppermute | solution.py:467
  (39 shorter events, 13.4 us)
Async XLA Ops:
  0.0 23.9 %copy-start.3 = (s32[128,2]{0,1:T(2,128)S(1)}, s32[128,2]{0,1:T(2,128)}, u32[]{:S(2)}) copy-start(s32[128,2]{0,1:T(2,128)} %param.24) | copy-start | bytes 3076
  0.0 24.0 %copy-start.5 = (f32[4]{0:T(128)S(1)}, f32[4]{0:T(128)}, u32[]{:S(2)}) copy-start(f32[4]{0:T(128)} %param.17) | copy-start | bytes 52
  2.0 13.6 %all-to-all-start.1 = ((bf16[4,272,256]{2,1,0:T(8,128)(2,1)}), bf16[4,272,256]{2,1,0:T(8,128)(2,1)S(1)}, u32[]{:S(2)}, u32[]{:S(2)}) async-start(bf16[4,272,256]{2,1,0:T(8,128)(2,1)} %pack.1), calls=%async_computation.1 | async-start | bytes 1114112 | tf_op jit(solution)/shard_map/all_to_all | solution.py:423
  7.2 103.4 %collective-permute-start.2 = (bf16[2048,1024]{1,0:T(8,128)(2,1)}, bf16[2048,1024]{1,0:T(8,128)(2,1)}, u32[]{:S(2)}, u32[]{:S(2)}) collective-permute-start(bf16[2048,1024]{1,0:T(8,128)(2,1)} %bitcast.29), channel_id=1, source_target_pairs={{0,1},{1,0},{2,3},{3,2},{4,5},{5,4},{6,7},{7,6},{8,9},{9,8},{10,11... | collective-permute-start | bytes 12582920 | tf_op jit(solution)/shard_map/ppermute | solution.py:440
  7.2 103.4 %collective-permute-start.3 = (bf16[2048,1024]{1,0:T(8,128)(2,1)}, bf16[2048,1024]{1,0:T(8,128)(2,1)}, u32[]{:S(2)}, u32[]{:S(2)}) collective-permute-start(bf16[2048,1024]{1,0:T(8,128)(2,1)} %bitcast.32), channel_id=1, source_target_pairs={{0,1},{1,0},{2,3},{3,2},{4,5},{5,4},{6,7},{7,6},{8,9},{9,8},{10,11... | collective-permute-start | bytes 12582920 | tf_op jit(solution)/shard_map/ppermute | solution.py:440
  7.7 102.9 %collective-permute-start.4 = (bf16[1024,2048]{1,0:T(8,128)(2,1)}, bf16[1024,2048]{1,0:T(8,128)(2,1)}, u32[]{:S(2)}, u32[]{:S(2)}) collective-permute-start(bf16[1024,2048]{1,0:T(8,128)(2,1)} %bitcast.35), channel_id=1, source_target_pairs={{0,1},{1,0},{2,3},{3,2},{4,5},{5,4},{6,7},{7,6},{8,9},{9,8},{10,11... | collective-permute-start | bytes 12582920 | tf_op jit(solution)/shard_map/ppermute | solution.py:440
  15.6 14.8 %all-to-all-start = ((bf16[4,256,128]{2,1,0:T(8,128)(2,1)}), bf16[4,256,128]{2,1,0:T(8,128)(2,1)S(1)}, u32[]{:S(2)}, u32[]{:S(2)}) async-start(bf16[4,256,128]{2,1,0:T(8,128)(2,1)} %bitcast.3), calls=%async_computation | async-start | bytes 524288 | tf_op jit(solution)/shard_map/all_to_all | solution.py:425
  19.1 11.3 %collective-permute-start = (bf16[3,272,256]{2,1,0:T(8,128)(2,1)S(1)}, bf16[3,272,256]{2,1,0:T(8,128)(2,1)S(1)}, u32[]{:S(2)}, u32[]{:S(2)}) collective-permute-start(bf16[3,272,256]{2,1,0:T(8,128)(2,1)S(1)} %get-tuple-element.14), channel_id=1, source_target_pairs={{0,8},{2,10},{4,12},{6,14},{8,16},{10,18},{12,20},{14,22},{16,24},... | collective-permute-start | bytes 1253384 | tf_op jit(solution)/shard_map/ppermute | solution.py:426
  22.6 11.9 %collective-permute-start.1 = (bf16[3,272,256]{2,1,0:T(8,128)(2,1)S(1)}, bf16[3,272,256]{2,1,0:T(8,128)(2,1)S(1)}, u32[]{:S(2)}, u32[]{:S(2)}) collective-permute-start(bf16[3,272,256]{2,1,0:T(8,128)(2,1)S(1)} %get-tuple-element.13), channel_id=1, source_target_pairs={{8,0},{10,2},{12,4},{14,6},{16,8},{18,10},{20,12},{22,14},{24,16},... | collective-permute-start | bytes 1253384 | tf_op jit(solution)/shard_map/ppermute | solution.py:429
  24.7 21.0 %copy-start = (bf16[128,2048]{1,0:T(8,128)(2,1)S(1)}, bf16[128,2048]{1,0:T(8,128)(2,1)}, u32[]{:S(2)}) copy-start(bf16[128,2048]{1,0:T(8,128)(2,1)} %residual_ref.1) | copy-start | bytes 1572868
  24.7 22.3 %copy-start.4 = (f32[128,2]{0,1:T(2,128)S(1)}, f32[128,2]{0,1:T(2,128)}, u32[]{:S(2)}) copy-start(f32[128,2]{0,1:T(2,128)} %param.25) | copy-start | bytes 3076
  24.7 47.0 %copy-start.1 = (f32[2048]{0:T(1024)S(1)}, f32[2048]{0:T(1024)}, u32[]{:S(2)}) copy-start(f32[2048]{0:T(1024)} %param.20) | copy-start | bytes 24580
  41.8 20.2 %all-to-all-start.2 = ((bf16[8,128,128]{2,1,0:T(8,128)(2,1)}), bf16[8,128,128]{2,1,0:T(8,128)(2,1)S(1)}, u32[]{:S(2)}, u32[]{:S(2)}) async-start(bf16[8,128,128]{2,1,0:T(8,128)(2,1)} %bitcast.4), calls=%async_computation.2 | async-start | bytes 524288 | tf_op jit(solution)/shard_map/all_to_all | solution.py:446
  45.7 26.0 %collective-permute-start.7 = (bf16[128,2048]{1,0:T(8,128)(2,1)S(1)}, bf16[128,2048]{1,0:T(8,128)(2,1)S(1)}, u32[]{:S(2)}, u32[]{:S(2)}) collective-permute-start(bf16[128,2048]{1,0:T(8,128)(2,1)S(1)} %copy-done), channel_id=1, source_target_pairs={{0,24},{2,26},{4,28},{6,30},{8,16},{10,18},{12,20},{14,22},{16,8},... | collective-permute-start | bytes 1572872 | tf_op jit(solution)/shard_map/ppermute | solution.py:437
  47.0 15.0 %collective-permute-start.5 = (f32[8,128]{1,0:T(8,128)S(1)}, f32[8,128]{1,0:T(8,128)S(1)}, u32[]{:S(2)}, u32[]{:S(2)}) collective-permute-start(f32[8,128]{1,0:T(8,128)S(1)} %get-tuple-element.17), channel_id=1, source_target_pairs={{0,24},{2,26},{4,28},{6,30},{8,16},{10,18},{12,20},{14,22},{16,8},... | collective-permute-start | bytes 12296 | tf_op jit(solution)/shard_map/ppermute | solution.py:435
  62.0 9.6 %collective-permute-start.6 = (bf16[8,128,128]{2,1,0:T(8,128)(2,1)S(1)}, bf16[8,128,128]{2,1,0:T(8,128)(2,1)S(1)}, u32[]{:S(2)}, u32[]{:S(2)}) collective-permute-start(bf16[8,128,128]{2,1,0:T(8,128)(2,1)S(1)} %all-to-all-done.2.heads_ref), channel_id=1, source_target_pairs={{0,24},{2,26},{4,28},{6,30},{8,16},{10,18},{12,20},{14,22},{16,8},... | collective-permute-start | bytes 786440 | tf_op jit(solution)/shard_map/ppermute | solution.py:449
  75.8 31.1 %all-to-all-start.5 = ((bf16[8,32,2048]{2,1,0:T(8,128)(2,1)}), bf16[8,32,2048]{2,1,0:T(8,128)(2,1)S(1)}, u32[]{:S(2)}, u32[]{:S(2)}) async-start(bf16[8,32,2048]{2,1,0:T(8,128)(2,1)} %bitcast.14), calls=%async_computation.5 | async-start | bytes 2097152 | tf_op jit(solution)/shard_map/all_to_all | solution.py:456
  106.8 17.5 %all-to-all-start.3 = ((bf16[8,32,2048]{2,1,0:T(8,128)(2,1)}), bf16[8,32,2048]{2,1,0:T(8,128)(2,1)S(1)}, u32[]{:S(2)}, u32[]{:S(2)}) async-start(bf16[8,32,2048]{2,1,0:T(8,128)(2,1)} %bitcast.6), calls=%async_computation.3 | async-start | bytes 2097152 | tf_op jit(solution)/shard_map/all_to_all | solution.py:456
  124.4 17.6 %all-to-all-start.6 = ((bf16[8,32,2048]{2,1,0:T(8,128)(2,1)}), bf16[8,32,2048]{2,1,0:T(8,128)(2,1)S(1)}, u32[]{:S(2)}, u32[]{:S(2)}) async-start(bf16[8,32,2048]{2,1,0:T(8,128)(2,1)} %bitcast.16), calls=%async_computation.6 | async-start | bytes 2097152 | tf_op jit(solution)/shard_map/all_to_all | solution.py:456
  139.6 32.3 %copy-start.2 = (bf16[128,2048]{1,0:T(8,128)(2,1)S(1)}, bf16[128,2048]{1,0:T(8,128)(2,1)}, u32[]{:S(2)}) copy-start(bf16[128,2048]{1,0:T(8,128)(2,1)} %get-tuple-element.11.mixed_ref) | copy-start | bytes 1572868
  142.0 17.6 %all-to-all-start.4 = ((bf16[8,32,2048]{2,1,0:T(8,128)(2,1)}), bf16[8,32,2048]{2,1,0:T(8,128)(2,1)S(1)}, u32[]{:S(2)}, u32[]{:S(2)}) async-start(bf16[8,32,2048]{2,1,0:T(8,128)(2,1)} %bitcast.11), calls=%async_computation.4 | async-start | bytes 2097152 | tf_op jit(solution)/shard_map/all_to_all | solution.py:456
  146.1 25.8 %collective-permute-start.8 = (bf16[128,2048]{1,0:T(8,128)(2,1)S(1)}, bf16[128,2048]{1,0:T(8,128)(2,1)S(1)}, u32[]{:S(2)}, u32[]{:S(2)}) collective-permute-start(bf16[128,2048]{1,0:T(8,128)(2,1)S(1)} %partial_sum.1), channel_id=1, source_target_pairs={{0,24},{2,26},{4,28},{6,30},{8,16},{10,18},{12,20},{14,22},{16,8},... | collective-permute-start | bytes 1572872 | tf_op jit(solution)/shard_map/ppermute | solution.py:467

commit v6 on v5

--- a/solution.py
+++ b/solution.py
@@ -72,7 +72,6 @@
     length, width = o_ref.shape[1:]
     before, group, after = prev_ref.shape[0], own_ref.shape[0], next_ref.shape[0]
     span = before + 1 + after
-    blocks = before + group + after
 
     @pl.when(b == 0)
     def _():
@@ -86,9 +85,6 @@
                 id_ref[first + i : first + i + 1, :] = named
                 line_ref[0:1, rows] = named
         v_ref[:, width:] = jnp.ones((v_ref.shape[0], width), BF)
-        k_ref[blocks * length :, :] = jnp.zeros((length, width), BF)
-        v_ref[blocks * length :, :width] = jnp.zeros((length, width), BF)
-        line_ref[0:1, blocks * length :] = jnp.zeros((1, length), F32)
 
         ids = id_ref[...]
         smallest = jnp.min(ids, axis=1, keepdims=True)
@@ -105,7 +101,7 @@
 
     query_ids = id_ref[pl.ds(b + before, 1), :]
     left = bound_ref[0, b]
-    pairs = (span + 1 - bound_ref[1, b] - left) // 2
+    needed = span - bound_ref[1, b] - left
     start = pl.multiple_of((b + left) * length, length)
     query_column = jnp.transpose(jnp.broadcast_to(query_ids, (128, length)))
     lam = lam_ref[0]
@@ -148,11 +144,11 @@
             scale = lax.rsqrt(jnp.mean(out * out, axis=1, keepdims=True) + EPS)
             o_ref[b, chunk * 128 : (chunk + 1) * 128, :] = (out * scale).astype(BF)
 
-    for count in range(1, (span + 1) // 2 + 1):
-
-        @pl.when(pairs == count)
+    for count in range(1, span + 1):
+
+        @pl.when(needed == count)
         def _():
-            attend(count * 2 * length)
+            attend(count * length)
 
 
 def attention(lam, queries, prev, own, following):
@@ -166,10 +162,10 @@
         out_specs=VM,
         out_shape=jax.ShapeDtypeStruct((group, length, width), BF),
         scratch_shapes=[
-            pltpu.VMEM(((blocks + 1) * length, width), BF),
-            pltpu.VMEM(((blocks + 1) * length, 2 * width), BF),
-            pltpu.VMEM((8, (blocks + 1) * length), F32),
-            pltpu.VMEM((-(-(blocks + 1) // 8) * 8, length), F32),
+            pltpu.VMEM((blocks * length, width), BF),
+            pltpu.VMEM((blocks * length, 2 * width), BF),
+            pltpu.VMEM((8, blocks * length), F32),
+            pltpu.VMEM((-(-blocks // 8) * 8, length), F32),
             pltpu.SMEM((2, group), jnp.int32),
         ],
         compiler_params=params(16),
@@ -250,7 +246,7 @@
     )(heads, residual, gain, meta, in_hbm(out_weight))
 
 
-def expert_rows(x_ref, g, u, d, y_ref, hidden_ref, half_ref, tile, arrive):
+def expert_rows(x_ref, g, u, d, y_ref, hidden_ref, half_ref, tile, wide, arrive):
     halves, width, depth = g.shape
     for h in range(halves):
         for step in range(depth // tile):
@@ -260,8 +256,8 @@
             upward = jnp.dot(x_ref[...], u[h, :, at], preferred_element_type=F32)
             hidden_ref[:, at] = (gate / (1.0 + jnp.exp(-gate)) * upward).astype(BF)
         arrive(h, depth // tile)
-        for n in range(width // tile):
-            at = slice(n * tile, (n + 1) * tile)
+        for n in range(width // wide):
+            at = slice(n * wide, (n + 1) * wide)
             part = jnp.dot(hidden_ref[...], d[h, :, at], preferred_element_type=F32).astype(BF)
             if h:
                 y_ref[:, at] = (half_ref[:, at].astype(F32) + part.astype(F32)).astype(BF)
@@ -270,7 +266,7 @@
 
 
 def expert_kernel(
-    x_ref, g0, u0, d0, g1, u1, d1, y_ref, gs, us, ds, hidden_ref, half_ref, sems, *, tile
+    x_ref, g0, u0, d0, g1, u1, d1, y_ref, gs, us, ds, hidden_ref, half_ref, sems, *, tile, wide
 ):
     steps = g0.shape[1] // tile
     arrivals = []
@@ -295,14 +291,14 @@
         for copy in arrivals[h][step]:
             copy.wait()
 
-    expert_rows(x_ref, gs, us, ds, y_ref, hidden_ref, half_ref, tile, arrive)
-
-
-def experts_of(x, own, other, tile=256):
+    expert_rows(x_ref, gs, us, ds, y_ref, hidden_ref, half_ref, tile, wide, arrive)
+
+
+def experts_of(x, own, other, tile=512, wide=1024):
     rows, width = x.shape
     depth = own[0].shape[1]
     return pl.pallas_call(
-        functools.partial(expert_kernel, tile=tile),
+        functools.partial(expert_kernel, tile=tile, wide=wide),
         in_specs=[VM] + [ANY] * 6,
         out_specs=VM,
         out_shape=jax.ShapeDtypeStruct((rows, width), BF),
@@ -446,8 +442,6 @@
     token_heads = lax.all_to_all(
         outs, ("sp", "tp"), 0, 0, tiled=True, axis_index_groups=both
     )
-    heads_far = lax.ppermute(token_heads, "sp", mirror)
-
     gain = norm_gain.reshape(1, width)
     slots = half * capacity
 
@@ -457,6 +451,8 @@
         return rows.reshape(slots, width)
 
     rows_own, mixed = project(token_heads, residual, gain, meta_own, out_weight, slots, True)
+    heads_late, mixed = lax.optimization_barrier((token_heads, mixed))
+    heads_far = lax.ppermute(heads_late, "sp", mirror)
     rows_own = exchange(rows_own)
     rows_far = project(heads_far, residual_far, gain, meta_far, out_weight, slots, False)
     rows_far = exchange(rows_far)

time: 174 us -> 168 us (0.966)
  the two profiles are of different devices: /device:TPU:0 before, /device:TPU:12 now
where the time goes in v6:
time: 168 us; the launch traced here: 166 us
  waiting for transfers between devices  67.5 us (40%)
  Pallas kernels  40.1 us (24%)
  starting transfers between devices  38.3 us (23%)
  blocking collectives  17.1 us (10%)
  local copies, waits for them, and re-layouts  2.68 us (2%)
    ppermute x1, waiting for transfers between devices, on_device(): heads_far = lax.ppermute(heads_late, 'sp', mirror)  26.7 us
    pallas_call x2, Pallas kernels, experts_of(): pl.pallas_call(functools.partial(expert_kernel, tile=tile, wide=wide), in...  21.8 us
    all_to_all x1, blocking collectives, exchange(): lax.all_to_all(rows, 'sp', 0, 0, tiled=True, axis_index_groups=halves)  17.1 us
    all_to_all x3, starting transfers between devices, exchange(): lax.all_to_all(rows, 'sp', 0, 0, tiled=True, axis_index_groups=halves)  15.8 us
    all_to_all x3, waiting for transfers between devices, exchange(): lax.all_to_all(rows, 'sp', 0, 0, tiled=True, axis_index_groups=halves)  14.4 us
    ppermute x1, waiting for transfers between devices, on_device(): part = lax.ppermute(part_far, 'sp', mirror)  10.4 us
    ppermute x1, waiting for transfers between devices, on_device(): lax.ppermute(pairs[heads - REACH:], 'sp', [(i, i + heads) for i in range(...  7.31 us
    pallas_call x2, Pallas kernels, project(): pl.pallas_call(functools.partial(project_kernel, tile=tile), in_specs=[VM...  7.17 us
  transfers between devices with their start and end apart: 15, of which 7 were waited for; matrix products, arithmetic and copies ran while one was open for 2% of the time, Pallas kernels for 22%

profile of v6, /device:TPU:12, one launch (start us, length us, event | category | flops | bytes accessed | tf_op | source)
XLA Modules:
  0.0 166.0 jit_solution(2951156185865810304)
XLA Ops:
  0.0 2.0 %pack.1 = bf16[4,272,256]{2,1,0:T(8,128)(2,1)} custom-call(bf16[256,512]{1,0:T(8,128)(2,1)} %k_ref.1, bf16[256,512]{1,0:T(8,128)(2,1)} %v_ref.1, s32[256]{0:T(256)} %id_ref.1), custom_call_target="tpu_custom_call" | custom-call | tf_op jit(solution)/shard_map/pack/pallas_call | solution.py:48
  2.0 4.2 %all-to-all-start.1 = ((bf16[4,272,256]{2,1,0:T(8,128)(2,1)}), bf16[4,272,256]{2,1,0:T(8,128)(2,1)S(1)}, u32[]{:S(2)}, u32[]{:S(2)}) async-start(bf16[4,272,256]{2,1,0:T(8,128)(2,1)} %pack.1), calls=%async_computation.1 | async-start | bytes 1114112 | tf_op jit(solution)/shard_map/all_to_all | solution.py:419
  8.7 5.4 %all-to-all-done.1.own_ref = bf16[4,272,256]{2,1,0:T(8,128)(2,1)S(1)} async-done(((bf16[4,272,256]{2,1,0:T(8,128)(2,1)}), bf16[4,272,256]{2,1,0:T(8,128)(2,1)S(1)}, u32[]{:S(2)}, u32[]{:S(2)}) %all-to-all-start.1) | async-done | bytes 557088 | tf_op jit(solution)/shard_map/all_to_all | solution.py:419
  14.1 3.9 %all-to-all-start = ((bf16[4,256,128]{2,1,0:T(8,128)(2,1)}), bf16[4,256,128]{2,1,0:T(8,128)(2,1)S(1)}, u32[]{:S(2)}, u32[]{:S(2)}) async-start(bf16[4,256,128]{2,1,0:T(8,128)(2,1)} %bitcast.3), calls=%async_computation | async-start | bytes 524288 | tf_op jit(solution)/shard_map/all_to_all | solution.py:421
  18.0 2.3 %collective-permute-start.1 = (bf16[3,272,256]{2,1,0:T(8,128)(2,1)S(1)}, bf16[3,272,256]{2,1,0:T(8,128)(2,1)S(1)}, u32[]{:S(2)}, u32[]{:S(2)}) collective-permute-start(bf16[3,272,256]{2,1,0:T(8,128)(2,1)S(1)} %get-tuple-element.17), channel_id=1, source_target_pairs={{8,0},{10,2},{12,4},{14,6},{16,8},{18,10},{20,12},{22,14},{24,16},... | collective-permute-start | bytes 1253384 | tf_op jit(solution)/shard_map/ppermute | solution.py:425
  20.4 3.5 %collective-permute-start = (bf16[3,272,256]{2,1,0:T(8,128)(2,1)S(1)}, bf16[3,272,256]{2,1,0:T(8,128)(2,1)S(1)}, u32[]{:S(2)}, u32[]{:S(2)}) collective-permute-start(bf16[3,272,256]{2,1,0:T(8,128)(2,1)S(1)} %get-tuple-element.18), channel_id=1, source_target_pairs={{0,8},{2,10},{4,12},{6,14},{8,16},{10,18},{12,20},{14,22},{16,24},... | collective-permute-start | bytes 1253384 | tf_op jit(solution)/shard_map/ppermute | solution.py:422
  24.7 7.3 %collective-permute-done.prev_ref = bf16[3,272,256]{2,1,0:T(8,128)(2,1)S(1)} collective-permute-done((bf16[3,272,256]{2,1,0:T(8,128)(2,1)S(1)}, bf16[3,272,256]{2,1,0:T(8,128)(2,1)S(1)}, u32[]{:S(2)}, u32[]{:S(2)}) %collective-permute-start) | collective-permute-done | bytes 417824 | tf_op jit(solution)/shard_map/ppermute | solution.py:422
  32.0 7.2 %attention.1 = bf16[4,256,128]{2,1,0:T(8,128)(2,1)} custom-call(f32[1]{0:T(128)} %dynamic_slice.3.lam_ref, bf16[4,256,128]{2,1,0:T(8,128)(2,1)S(1)} %all-to-all-done.q_ref, bf16[3,272,256]{2,1,0:T(8,128)(2,1)S(1)} %collective-permute-done.prev_ref, bf16[4,272,256]{2,1,0:T(8,128)(2,1)S(1)} %all-to-all-done.1.own_ref, ...), custom_call_target="tpu_custom_call" | custom-call | flops 8000000000 | bytes 4000000 | tf_op jit(solution)/shard_map/attention/pallas_call | solution.py:158
  39.2 4.2 %all-to-all-start.2 = ((bf16[8,128,128]{2,1,0:T(8,128)(2,1)}), bf16[8,128,128]{2,1,0:T(8,128)(2,1)S(1)}, u32[]{:S(2)}, u32[]{:S(2)}) async-start(bf16[8,128,128]{2,1,0:T(8,128)(2,1)} %bitcast.4), calls=%async_computation.2 | async-start | bytes 524288 | tf_op jit(solution)/shard_map/all_to_all | solution.py:442
  43.6 1.6 collective-permute-start.5
  45.6 3.2 %all-to-all-done.2.heads_ref = bf16[8,128,128]{2,1,0:T(8,128)(2,1)S(1)} async-done(((bf16[8,128,128]{2,1,0:T(8,128)(2,1)}), bf16[8,128,128]{2,1,0:T(8,128)(2,1)S(1)}, u32[]{:S(2)}, u32[]{:S(2)}) %all-to-all-start.2) | async-done | bytes 262176 | tf_op jit(solution)/shard_map/all_to_all | solution.py:442
  48.8 4.1 %shard_map.127 = (bf16[256,2048]{1,0:T(8,128)(2,1)}, bf16[128,2048]{1,0:T(8,128)(2,1)}) custom-call(bf16[8,128,128]{2,1,0:T(8,128)(2,1)S(1)} %all-to-all-done.2.heads_ref, bf16[128,2048]{1,0:T(8,128)(2,1)S(1)} %copy-done, f32[1,2048]{1,0:T(1,128)S(1)} %bitcast.26, f32[8,128]{1,0:T(8,128)S(1)} %get-tuple-element.22.meta_ref, bf16[1024,2048]{1,0:T(8,128)(2,1)} %weight_ref.3), custom_call_target="tpu_custom_call" | custom-call | flops 3000000000 | bytes 8000000 | tf_op jit(solution)/shard_map/pallas_call | solution.py:238
  52.9 1.7 collective-permute-start.6
  54.6 26.7 %collective-permute-done.6.heads_ref = bf16[8,128,128]{2,1,0:T(8,128)(2,1)S(1)} collective-permute-done((bf16[8,128,128]{2,1,0:T(8,128)(2,1)S(1)}, bf16[8,128,128]{2,1,0:T(8,128)(2,1)S(1)}, u32[]{:S(2)}, u32[]{:S(2)}) %collective-permute-start.6) | collective-permute-done | bytes 262176 | tf_op jit(solution)/shard_map/ppermute | solution.py:455
  81.3 3.1 %shard_map.129 = bf16[256,2048]{1,0:T(8,128)(2,1)S(1)} custom-call(bf16[8,128,128]{2,1,0:T(8,128)(2,1)S(1)} %collective-permute-done.6.heads_ref, bf16[128,2048]{1,0:T(8,128)(2,1)S(1)} %collective-permute-done.7.residual_ref, f32[1,2048]{1,0:T(1,128)S(1)} %bitcast.27, f32[8,128]{1,0:T(8,128)S(1)} %collective-permute-done.5.meta_ref, ...), custom_call_target="tpu_custom_call" | custom-call | flops 3000000000 | bytes 8000000 | tf_op jit(solution)/shard_map/pallas_call | solution.py:238
  84.4 17.1 %all_to_all.35 = bf16[8,32,2048]{2,1,0:T(8,128)(2,1)S(1)} all-to-all(bf16[8,32,2048]{2,1,0:T(8,128)(2,1)S(1)} %bitcast.25), channel_id=1, replica_groups={{0,2,4,6,8,10,12,14},{16,18,20,22,24,26,28,30},{1,3,5,7,9,11,13,15},{17..., dimensions={0} | all-to-all | bytes 2097152 | tf_op jit(solution)/shard_map/all_to_all | solution.py:450
  101.5 5.5 %all-to-all-start.3 = ((bf16[8,32,2048]{2,1,0:T(8,128)(2,1)}), bf16[8,32,2048]{2,1,0:T(8,128)(2,1)S(1)}, u32[]{:S(2)}, u32[]{:S(2)}) async-start(bf16[8,32,2048]{2,1,0:T(8,128)(2,1)} %bitcast.6), calls=%async_computation.3 | async-start | bytes 2097152 | tf_op jit(solution)/shard_map/all_to_all | solution.py:450
  107.0 10.9 %shard_map.130 = bf16[256,2048]{1,0:T(8,128)(2,1)} custom-call(bf16[256,2048]{1,0:T(8,128)(2,1)S(1)} %bitcast.24, bf16[2048,1024]{1,0:T(8,128)(2,1)} %bitcast.31, bf16[2048,1024]{1,0:T(8,128)(2,1)} %bitcast.34, bf16[1024,2048]{1,0:T(8,128)(2,1)} %bitcast.37, bf16[2048,1024]{1,0:T(8,128)(2,1)} %collective-permute-done.2.g1, ...), custom_call_target="tpu_custom_call" | custom-call | flops 8999999488 | bytes 26000000 | tf_op jit(solution)/shard_map/pallas_call | solution.py:300
  117.9 5.1 %all-to-all-start.6 = ((bf16[8,32,2048]{2,1,0:T(8,128)(2,1)}), bf16[8,32,2048]{2,1,0:T(8,128)(2,1)S(1)}, u32[]{:S(2)}, u32[]{:S(2)}) async-start(bf16[8,32,2048]{2,1,0:T(8,128)(2,1)} %bitcast.16), calls=%async_computation.6 | async-start | bytes 2097152 | tf_op jit(solution)/shard_map/all_to_all | solution.py:450
  123.0 10.9 %shard_map.128 = bf16[256,2048]{1,0:T(8,128)(2,1)} custom-call(bf16[256,2048]{1,0:T(8,128)(2,1)S(1)} %bitcast.21, bf16[2048,1024]{1,0:T(8,128)(2,1)} %bitcast.32, bf16[2048,1024]{1,0:T(8,128)(2,1)} %bitcast.35, bf16[1024,2048]{1,0:T(8,128)(2,1)} %bitcast.38, bf16[2048,1024]{1,0:T(8,128)(2,1)} %collective-permute-done.2.g1, ...), custom_call_target="tpu_custom_call" | custom-call | flops 8999999488 | bytes 26000000 | tf_op jit(solution)/shard_map/pallas_call | solution.py:300
  135.2 5.2 %all-to-all-start.4 = ((bf16[8,32,2048]{2,1,0:T(8,128)(2,1)}), bf16[8,32,2048]{2,1,0:T(8,128)(2,1)S(1)}, u32[]{:S(2)}, u32[]{:S(2)}) async-start(bf16[8,32,2048]{2,1,0:T(8,128)(2,1)} %bitcast.11), calls=%async_computation.4 | async-start | bytes 2097152 | tf_op jit(solution)/shard_map/all_to_all | solution.py:450
  141.1 13.1 %all-to-all-done.4 = bf16[8,32,2048]{2,1,0:T(8,128)(2,1)S(1)} async-done(((bf16[8,32,2048]{2,1,0:T(8,128)(2,1)}), bf16[8,32,2048]{2,1,0:T(8,128)(2,1)S(1)}, u32[]{:S(2)}, u32[]{:S(2)}) %all-to-all-start.4) | async-done | bytes 1048608 | tf_op jit(solution)/shard_map/all_to_all | solution.py:450
  154.2 10.4 %collective-permute-done.8.far_ref = bf16[128,2048]{1,0:T(8,128)(2,1)S(1)} collective-permute-done((bf16[128,2048]{1,0:T(8,128)(2,1)S(1)}, bf16[128,2048]{1,0:T(8,128)(2,1)S(1)}, u32[]{:S(2)}, u32[]{:S(2)}) %collective-permute-start.8) | collective-permute-done | bytes 524320 | tf_op jit(solution)/shard_map/ppermute | solution.py:463
  164.6 1.4 final_sum.1
  (38 shorter events, 5.8 us)
Async XLA Ops:
  0.0 23.9 %copy-start.3 = (s32[128,2]{0,1:T(2,128)S(1)}, s32[128,2]{0,1:T(2,128)}, u32[]{:S(2)}) copy-start(s32[128,2]{0,1:T(2,128)} %param.24) | copy-start | bytes 3076
  0.0 24.1 %copy-start.5 = (f32[4]{0:T(128)S(1)}, f32[4]{0:T(128)}, u32[]{:S(2)}) copy-start(f32[4]{0:T(128)} %param.17) | copy-start | bytes 52
  2.0 12.0 %all-to-all-start.1 = ((bf16[4,272,256]{2,1,0:T(8,128)(2,1)}), bf16[4,272,256]{2,1,0:T(8,128)(2,1)S(1)}, u32[]{:S(2)}, u32[]{:S(2)}) async-start(bf16[4,272,256]{2,1,0:T(8,128)(2,1)} %pack.1), calls=%async_computation.1 | async-start | bytes 1114112 | tf_op jit(solution)/shard_map/all_to_all | solution.py:419
  6.2 100.7 %collective-permute-start.2 = (bf16[2048,1024]{1,0:T(8,128)(2,1)}, bf16[2048,1024]{1,0:T(8,128)(2,1)}, u32[]{:S(2)}, u32[]{:S(2)}) collective-permute-start(bf16[2048,1024]{1,0:T(8,128)(2,1)} %bitcast.30), channel_id=1, source_target_pairs={{0,1},{1,0},{2,3},{3,2},{4,5},{5,4},{6,7},{7,6},{8,9},{9,8},{10,11... | collective-permute-start | bytes 12582920 | tf_op jit(solution)/shard_map/ppermute | solution.py:436
  6.2 100.7 %collective-permute-start.3 = (bf16[2048,1024]{1,0:T(8,128)(2,1)}, bf16[2048,1024]{1,0:T(8,128)(2,1)}, u32[]{:S(2)}, u32[]{:S(2)}) collective-permute-start(bf16[2048,1024]{1,0:T(8,128)(2,1)} %bitcast.33), channel_id=1, source_target_pairs={{0,1},{1,0},{2,3},{3,2},{4,5},{5,4},{6,7},{7,6},{8,9},{9,8},{10,11... | collective-permute-start | bytes 12582920 | tf_op jit(solution)/shard_map/ppermute | solution.py:436
  6.7 100.2 %collective-permute-start.4 = (bf16[1024,2048]{1,0:T(8,128)(2,1)}, bf16[1024,2048]{1,0:T(8,128)(2,1)}, u32[]{:S(2)}, u32[]{:S(2)}) collective-permute-start(bf16[1024,2048]{1,0:T(8,128)(2,1)} %bitcast.36), channel_id=1, source_target_pairs={{0,1},{1,0},{2,3},{3,2},{4,5},{5,4},{6,7},{7,6},{8,9},{9,8},{10,11... | collective-permute-start | bytes 12582920 | tf_op jit(solution)/shard_map/ppermute | solution.py:436
  14.1 18.0 %all-to-all-start = ((bf16[4,256,128]{2,1,0:T(8,128)(2,1)}), bf16[4,256,128]{2,1,0:T(8,128)(2,1)S(1)}, u32[]{:S(2)}, u32[]{:S(2)}) async-start(bf16[4,256,128]{2,1,0:T(8,128)(2,1)} %bitcast.3), calls=%async_computation | async-start | bytes 524288 | tf_op jit(solution)/shard_map/all_to_all | solution.py:421
  18.0 14.0 %collective-permute-start.1 = (bf16[3,272,256]{2,1,0:T(8,128)(2,1)S(1)}, bf16[3,272,256]{2,1,0:T(8,128)(2,1)S(1)}, u32[]{:S(2)}, u32[]{:S(2)}) collective-permute-start(bf16[3,272,256]{2,1,0:T(8,128)(2,1)S(1)} %get-tuple-element.17), channel_id=1, source_target_pairs={{8,0},{10,2},{12,4},{14,6},{16,8},{18,10},{20,12},{22,14},{24,16},... | collective-permute-start | bytes 1253384 | tf_op jit(solution)/shard_map/ppermute | solution.py:425
  20.4 11.6 %collective-permute-start = (bf16[3,272,256]{2,1,0:T(8,128)(2,1)S(1)}, bf16[3,272,256]{2,1,0:T(8,128)(2,1)S(1)}, u32[]{:S(2)}, u32[]{:S(2)}) collective-permute-start(bf16[3,272,256]{2,1,0:T(8,128)(2,1)S(1)} %get-tuple-element.18), channel_id=1, source_target_pairs={{0,8},{2,10},{4,12},{6,14},{8,16},{10,18},{12,20},{14,22},{16,24},... | collective-permute-start | bytes 1253384 | tf_op jit(solution)/shard_map/ppermute | solution.py:422
  24.7 18.8 %copy-start.4 = (f32[128,2]{0,1:T(2,128)S(1)}, f32[128,2]{0,1:T(2,128)}, u32[]{:S(2)}) copy-start(f32[128,2]{0,1:T(2,128)} %param.25) | copy-start | bytes 3076
  24.7 20.5 %copy-start = (bf16[128,2048]{1,0:T(8,128)(2,1)S(1)}, bf16[128,2048]{1,0:T(8,128)(2,1)}, u32[]{:S(2)}) copy-start(bf16[128,2048]{1,0:T(8,128)(2,1)} %residual_ref.1) | copy-start | bytes 1572868
  24.7 24.1 %copy-start.1 = (f32[2048]{0:T(1024)S(1)}, f32[2048]{0:T(1024)}, u32[]{:S(2)}) copy-start(f32[2048]{0:T(1024)} %param.20) | copy-start | bytes 24580
  39.2 9.6 %all-to-all-start.2 = ((bf16[8,128,128]{2,1,0:T(8,128)(2,1)}), bf16[8,128,128]{2,1,0:T(8,128)(2,1)S(1)}, u32[]{:S(2)}, u32[]{:S(2)}) async-start(bf16[8,128,128]{2,1,0:T(8,128)(2,1)} %bitcast.4), calls=%async_computation.2 | async-start | bytes 524288 | tf_op jit(solution)/shard_map/all_to_all | solution.py:442
  43.6 9.4 %collective-permute-start.5 = (f32[8,128]{1,0:T(8,128)S(1)}, f32[8,128]{1,0:T(8,128)S(1)}, u32[]{:S(2)}, u32[]{:S(2)}) collective-permute-start(f32[8,128]{1,0:T(8,128)S(1)} %get-tuple-element.21), channel_id=1, source_target_pairs={{0,24},{2,26},{4,28},{6,30},{8,16},{10,18},{12,20},{14,22},{16,8},... | collective-permute-start | bytes 12296 | tf_op jit(solution)/shard_map/ppermute | solution.py:431
  45.2 36.1 %collective-permute-start.7 = (bf16[128,2048]{1,0:T(8,128)(2,1)S(1)}, bf16[128,2048]{1,0:T(8,128)(2,1)S(1)}, u32[]{:S(2)}, u32[]{:S(2)}) collective-permute-start(bf16[128,2048]{1,0:T(8,128)(2,1)S(1)} %copy-done), channel_id=1, source_target_pairs={{0,24},{2,26},{4,28},{6,30},{8,16},{10,18},{12,20},{14,22},{16,8},... | collective-permute-start | bytes 1572872 | tf_op jit(solution)/shard_map/ppermute | solution.py:433
  52.9 28.4 %collective-permute-start.6 = (bf16[8,128,128]{2,1,0:T(8,128)(2,1)S(1)}, bf16[8,128,128]{2,1,0:T(8,128)(2,1)S(1)}, u32[]{:S(2)}, u32[]{:S(2)}) collective-permute-start(bf16[8,128,128]{2,1,0:T(8,128)(2,1)S(1)} %all-to-all-done.2.heads_ref), channel_id=1, source_target_pairs={{0,24},{2,26},{4,28},{6,30},{8,16},{10,18},{12,20},{14,22},{16,8},... | collective-permute-start | bytes 786440 | tf_op jit(solution)/shard_map/ppermute | solution.py:455
  101.5 16.5 %all-to-all-start.3 = ((bf16[8,32,2048]{2,1,0:T(8,128)(2,1)}), bf16[8,32,2048]{2,1,0:T(8,128)(2,1)S(1)}, u32[]{:S(2)}, u32[]{:S(2)}) async-start(bf16[8,32,2048]{2,1,0:T(8,128)(2,1)} %bitcast.6), calls=%async_computation.3 | async-start | bytes 2097152 | tf_op jit(solution)/shard_map/all_to_all | solution.py:450
  117.9 17.3 %all-to-all-start.6 = ((bf16[8,32,2048]{2,1,0:T(8,128)(2,1)}), bf16[8,32,2048]{2,1,0:T(8,128)(2,1)S(1)}, u32[]{:S(2)}, u32[]{:S(2)}) async-start(bf16[8,32,2048]{2,1,0:T(8,128)(2,1)} %bitcast.16), calls=%async_computation.6 | async-start | bytes 2097152 | tf_op jit(solution)/shard_map/all_to_all | solution.py:450
  133.9 30.6 %copy-start.2 = (bf16[128,2048]{1,0:T(8,128)(2,1)S(1)}, bf16[128,2048]{1,0:T(8,128)(2,1)}, u32[]{:S(2)}) copy-start(bf16[128,2048]{1,0:T(8,128)(2,1)} %get-tuple-element.14.mixed_ref) | copy-start | bytes 1572868
  135.2 18.9 %all-to-all-start.4 = ((bf16[8,32,2048]{2,1,0:T(8,128)(2,1)}), bf16[8,32,2048]{2,1,0:T(8,128)(2,1)S(1)}, u32[]{:S(2)}, u32[]{:S(2)}) async-start(bf16[8,32,2048]{2,1,0:T(8,128)(2,1)} %bitcast.11), calls=%async_computation.4 | async-start | bytes 2097152 | tf_op jit(solution)/shard_map/all_to_all | solution.py:450
  141.0 23.6 %collective-permute-start.8 = (bf16[128,2048]{1,0:T(8,128)(2,1)S(1)}, bf16[128,2048]{1,0:T(8,128)(2,1)S(1)}, u32[]{:S(2)}, u32[]{:S(2)}) collective-permute-start(bf16[128,2048]{1,0:T(8,128)(2,1)S(1)} %partial_sum.1), channel_id=1, source_target_pairs={{0,24},{2,26},{4,28},{6,30},{8,16},{10,18},{12,20},{14,22},{16,8},... | collective-permute-start | bytes 1572872 | tf_op jit(solution)/shard_map/ppermute | solution.py:463
